TPU v7x, 512 devices: a whole 4x4x16 slice. The times are simulated.
512 devices in a mesh: sp: 64 (over z, y), tp: 8 (over x, core).
Axes of the slice: x: 4, y: 4, z: 16, core: 2. Of those that a mesh axis runs over, the one named last changes fastest.
Arguments:
- hidden: bfloat16 [12288, 2048], P('sp')
- norm_gain: float32 [2048], replicated, may hold values from 0.1 to 1.9
- query_weight: bfloat16 [2048, 1024], P(None, 'tp'), may hold values from -0.125 to 0.125
- key_weight: bfloat16 [2048, 256], replicated, may hold values from -0.125 to 0.125
- value_weight: bfloat16 [2048, 256], replicated, may hold values from -0.125 to 0.125
- head_bias: float32 [16], P('tp'), may hold values from -10 to -3.5
- output_weight: bfloat16 [1024, 2048], P('tp'), may hold values from -0.1875 to 0.1875
Outputs:
- mixed: bfloat16 [12288, 2048], P('sp')
All inputs are finite; a program needn't handle non-finite values.
Results may differ from a plain program's by a relative error of at most 0.014.
Values may be sent and summed in bfloat16 or wider, within the bound.
No kernel may reach another device: no remote copies, remote signals or barrier semaphores. Data moves between devices by JAX's collectives and lax.ppermute only.
A program may use at most 64 MiB of HBM per device.

v0:
```python
import math

import jax
import jax.numpy as jnp
from jax import lax
from jax.sharding import Mesh
from jax.sharding import PartitionSpec as P

HEADS = 16
KV_HEADS = 4
HEAD_DIM = 64
SP = ("sp_0", "sp_1")


def gather_axes(value, axes, dim):
    for axis in reversed(axes):
        value = lax.all_gather(value, axis, axis=dim, tiled=True)
    return value


def laid_out(blocks, dim):
    blocks = jnp.moveaxis(blocks, 0, dim)
    shape = blocks.shape
    return blocks.reshape(*shape[:dim], shape[dim] * shape[dim + 1], *shape[dim + 2 :])


def sent_to_all(value, axis):
    length = lax.axis_size(axis)
    return lax.all_to_all(
        jnp.broadcast_to(value[None], (length, *value.shape)), axis, 0, 0, tiled=True
    )


def gathered_copies(value, axis, dim):
    return laid_out(sent_to_all(value, axis), dim)


def local(hidden, norm_gain, query_weight, key_weight, value_weight, head_bias, output_weight):
    group = HEADS // KV_HEADS
    scale = HEAD_DIM ** (-0.5)
    local_heads = query_weight.shape[1] // HEAD_DIM
    kv_count = max(1, local_heads // group)
    share = min(local_heads, group)
    first = lax.axis_index("tp") * local_heads // group
    key_cols = lax.dynamic_slice_in_dim(key_weight, first * HEAD_DIM, kv_count * HEAD_DIM, 1)
    value_cols = lax.dynamic_slice_in_dim(value_weight, first * HEAD_DIM, kv_count * HEAD_DIM, 1)
    joined = jnp.concatenate([query_weight, key_cols, value_cols], axis=1)
    wide = hidden.astype(jnp.float32)
    normed = (
        wide * lax.rsqrt(jnp.mean(wide * wide, axis=-1, keepdims=True) + 1e-06) * norm_gain
    ).astype(jnp.bfloat16)
    projected = jnp.dot(normed, joined, preferred_element_type=jnp.float32).astype(jnp.bfloat16)
    query_width = local_heads * HEAD_DIM
    kv_width = kv_count * HEAD_DIM
    queries = projected[:, :query_width]
    key_value = projected[:, query_width:]
    all_pairs = gather_axes(key_value, SP, 0)
    rows = queries.shape[0]
    offset = lax.axis_index(SP) * rows
    span = math.gcd(all_pairs.shape[0], 1024)
    turns = (offset + rows + span - 1) // span
    grouped = queries.reshape(rows, kv_count, share, HEAD_DIM)
    bias = head_bias.reshape(kv_count, share)
    query_pos = offset + jnp.arange(rows, dtype=jnp.int32)
    width = 128
    pieces = span // width
    inner = jnp.arange(width, dtype=jnp.int32)
    inner_later = (inner[:, None] > inner[None, :]).astype(jnp.float32)
    outer = jnp.arange(pieces, dtype=jnp.int32)
    outer_later = (outer[:, None] > outer[None, :]).astype(jnp.float32)

    def sweep(turn, carry):
        total, kept = carry
        start = (turns - 1 - turn) * span
        pair_block = lax.dynamic_slice_in_dim(all_pairs, start, span, 0)
        key_block = pair_block[:, :kv_width].reshape(span, kv_count, HEAD_DIM)
        value_block = pair_block[:, kv_width:].reshape(span, kv_count, HEAD_DIM)
        z = (
            jnp.einsum("qgrd,kgd->grqk", grouped, key_block, preferred_element_type=jnp.float32)
            * scale
        )
        z = z + bias[:, :, None, None]
        key_pos = start + jnp.arange(span, dtype=jnp.int32)
        strict = (key_pos[None, :] < query_pos[:, None])[None, None, :, :]
        keep = jnp.where(strict, jax.nn.log_sigmoid(-z), 0.0)
        split_keep = keep.reshape(kv_count, share, rows, pieces, width)
        within = jnp.einsum("grqpj,js->grqps", split_keep, inner_later)
        piece_sums = jnp.sum(split_keep, axis=4)
        later = jnp.einsum("grqj,jp->grqp", piece_sums, outer_later)
        between = (within + later[..., None]).reshape(kv_count, share, rows, span) + kept[..., None]
        weight = jnp.where(strict, jnp.exp(jax.nn.log_sigmoid(z) + between), 0.0).astype(
            jnp.bfloat16
        )
        total = total + jnp.einsum(
            "grqk,kgd->grqd", weight, value_block, preferred_element_type=jnp.float32
        )
        kept = kept + jnp.sum(piece_sums, axis=3)
        return (total, kept)

    start_total = jnp.zeros((kv_count, share, rows, HEAD_DIM), jnp.float32)
    start_kept = jnp.zeros((kv_count, share, rows), jnp.float32)
    total, kept = lax.fori_loop(0, turns, sweep, (start_total, start_kept))
    attended = total.transpose(2, 0, 1, 3).reshape(rows, query_width).astype(jnp.bfloat16)
    every_head = gathered_copies(attended, "tp", 1)
    summed = jnp.dot(
        every_head,
        lax.all_gather(output_weight, "tp", axis=0, tiled=True),
        preferred_element_type=jnp.float32,
    )
    return summed.astype(jnp.bfloat16)


def solution(mesh):
    torus = Mesh(mesh.devices.reshape(16, 4, mesh.shape["tp"]), ("sp_0", "sp_1", "tp"))
    in_specs = (P(SP, None), P(), P(None, "tp"), P(), P(), P("tp"), P("tp", None))
    out_specs = P(SP, None)
    return jax.shard_map(local, mesh=torus, in_specs=in_specs, out_specs=out_specs, check_vma=False)
```

profile of v0, /device:TPU:480, one launch (start us, length us, event | category | flops | bytes accessed | tf_op | source)
XLA Modules:
  0.0 223.4 jit_solution(15223147251479954251)
XLA Ops:
  6.5 1.5 fusion.33
  8.0 1.6 constant_dynamic-slice_fusion
  9.6 0.6 convolution_convert_fusion.1
  10.3 13.4 %all_gather.9 = bf16[768,128]{1,0:T(8,128)(2,1)} all-gather(bf16[192,128]{1,0:T(8,128)(2,1)S(1)} %get-tuple-element.203), channel_id=1, replica_groups=mesh['sp_0'=16,'sp_1'=4,'tp'=8] {'sp_1'}, dimensions={0}, use_global_device_ids=true | all-gather | bytes 245760 | tf_op jit(solution)/shard_map/all_gather | solution.py:17
  23.7 0.7 all-gather.5.cloned.1.call-update
  24.6 71.6 %all-gather.3.cloned.1.call-done = bf16[12288,128]{1,0:T(8,128)(2,1)} async-done(((bf16[768,128]{1,0:T(8,128)(2,1)}), bf16[12288,128]{1,0:T(8,128)(2,1)}) %all-gather.3.cloned.1.call-update) | async-done | bytes 3145744 | tf_op jit(solution)/shard_map/all_gather | solution.py:17
  96.2 103.1 %while.15 = (s32[]{:T(128)}, f32[1,2,192,64]{2,3,1,0:T(8,128)S(1)}, f32[1,2,192]{2,1,0:T(2,128)S(1)}, s32[]{:T(128)}, s32[]{:T(128)}, /*index=5*/bf16[12288,128]...) while((s32[]{:T(128)}, f32[1,2,192,64]{2,3,1,0:T(8,128)S(1)}, ...), condition=%wide.region_4.5_spmd.clone, body=%wide.region_1.4_spmd.clone.sunk | while | flops 211458368 | bytes 18715880 | solution.py:102
  96.4 3.6 %fusion.72 = (f32[2,192]{1,0:T(2,128)S(1)}, f32[1,2,192,1024]{3,2,1,0:T(8,128)S(1)}, f32[1,1024,192,2]{1,2,3,0:T(8,128)}) fusion(pred[192,1024]{1,0:T(8,128)(4,1)S(1)} %broadcast_compare_fusion.2, f32[2]{0:T(128)S(1)} %get-tuple-element.303, bf16[192,1,2,64]{0,3,2,1:T(8,128)(2,1)S(1)} %get-tuple-element.302, ...), kind=kOutput, calls=%fused_computation.63.clone.1 | convolution fusion | flops 54656640 | bytes 3655180 | tf_op jit(solution)/shard_map/while/body/qgrd,kgd->grqk/dot_general | solution.py:79
  100.4 0.6 bitcast_reduce_fusion.2
  101.8 2.9 %fusion.75 = f32[1,2,192,64]{2,3,1,0:T(8,128)S(1)} fusion(f32[1,2,192,64]{2,3,1,0:T(8,128)S(1)} %get-tuple-element.283, f32[1,2,192,1024]{3,2,1,0:T(8,128)S(1)} %reshape.140, f32[1,1024,192,2]{1,2,3,0:T(8,128)} %get-tuple-element.266, f32[2,192]{1,0:T(2,128)S(1)} %bitcast.130, pred[192,1024]{1,0:T(8,128)(4,1)S(1)} %broadcast_compare_fusion.2, ...), kind=kOutput, calls=%fused_computation.25.clone.1 | convolution fusion | flops 55074816 | bytes 3802632 | tf_op jit(solution)/shard_map/while/body/grqk,kgd->grqd/dot_general | solution.py:94
  105.0 3.6 %fusion.72 = (f32[2,192]{1,0:T(2,128)S(1)}, f32[1,2,192,1024]{3,2,1,0:T(8,128)S(1)}, f32[1,1024,192,2]{1,2,3,0:T(8,128)}) fusion(pred[192,1024]{1,0:T(8,128)(4,1)S(1)} %broadcast_compare_fusion.2, f32[2]{0:T(128)S(1)} %get-tuple-element.303, bf16[192,1,2,64]{0,3,2,1:T(8,128)(2,1)S(1)} %get-tuple-element.302, ...), kind=kOutput, calls=%fused_computation.63.clone.1 | convolution fusion | flops 54656640 | bytes 3655180 | tf_op jit(solution)/shard_map/while/body/qgrd,kgd->grqk/dot_general | solution.py:79
  109.0 0.6 bitcast_reduce_fusion.2
  110.4 2.9 %fusion.75 = f32[1,2,192,64]{2,3,1,0:T(8,128)S(1)} fusion(f32[1,2,192,64]{2,3,1,0:T(8,128)S(1)} %get-tuple-element.283, f32[1,2,192,1024]{3,2,1,0:T(8,128)S(1)} %reshape.140, f32[1,1024,192,2]{1,2,3,0:T(8,128)} %get-tuple-element.266, f32[2,192]{1,0:T(2,128)S(1)} %bitcast.130, pred[192,1024]{1,0:T(8,128)(4,1)S(1)} %broadcast_compare_fusion.2, ...), kind=kOutput, calls=%fused_computation.25.clone.1 | convolution fusion | flops 55074816 | bytes 3802632 | tf_op jit(solution)/shard_map/while/body/grqk,kgd->grqd/dot_general | solution.py:94
  113.6 3.6 %fusion.72 = (f32[2,192]{1,0:T(2,128)S(1)}, f32[1,2,192,1024]{3,2,1,0:T(8,128)S(1)}, f32[1,1024,192,2]{1,2,3,0:T(8,128)}) fusion(pred[192,1024]{1,0:T(8,128)(4,1)S(1)} %broadcast_compare_fusion.2, f32[2]{0:T(128)S(1)} %get-tuple-element.303, bf16[192,1,2,64]{0,3,2,1:T(8,128)(2,1)S(1)} %get-tuple-element.302, ...), kind=kOutput, calls=%fused_computation.63.clone.1 | convolution fusion | flops 54656640 | bytes 3655180 | tf_op jit(solution)/shard_map/while/body/qgrd,kgd->grqk/dot_general | solution.py:79
  117.6 0.6 bitcast_reduce_fusion.2
  119.0 2.9 %fusion.75 = f32[1,2,192,64]{2,3,1,0:T(8,128)S(1)} fusion(f32[1,2,192,64]{2,3,1,0:T(8,128)S(1)} %get-tuple-element.283, f32[1,2,192,1024]{3,2,1,0:T(8,128)S(1)} %reshape.140, f32[1,1024,192,2]{1,2,3,0:T(8,128)} %get-tuple-element.266, f32[2,192]{1,0:T(2,128)S(1)} %bitcast.130, pred[192,1024]{1,0:T(8,128)(4,1)S(1)} %broadcast_compare_fusion.2, ...), kind=kOutput, calls=%fused_computation.25.clone.1 | convolution fusion | flops 55074816 | bytes 3802632 | tf_op jit(solution)/shard_map/while/body/grqk,kgd->grqd/dot_general | solution.py:94
  122.2 3.6 %fusion.72 = (f32[2,192]{1,0:T(2,128)S(1)}, f32[1,2,192,1024]{3,2,1,0:T(8,128)S(1)}, f32[1,1024,192,2]{1,2,3,0:T(8,128)}) fusion(pred[192,1024]{1,0:T(8,128)(4,1)S(1)} %broadcast_compare_fusion.2, f32[2]{0:T(128)S(1)} %get-tuple-element.303, bf16[192,1,2,64]{0,3,2,1:T(8,128)(2,1)S(1)} %get-tuple-element.302, ...), kind=kOutput, calls=%fused_computation.63.clone.1 | convolution fusion | flops 54656640 | bytes 3655180 | tf_op jit(solution)/shard_map/while/body/qgrd,kgd->grqk/dot_general | solution.py:79
  126.2 0.6 bitcast_reduce_fusion.2
  127.6 3.0 %fusion.75 = f32[1,2,192,64]{2,3,1,0:T(8,128)S(1)} fusion(f32[1,2,192,64]{2,3,1,0:T(8,128)S(1)} %get-tuple-element.283, f32[1,2,192,1024]{3,2,1,0:T(8,128)S(1)} %reshape.140, f32[1,1024,192,2]{1,2,3,0:T(8,128)} %get-tuple-element.266, f32[2,192]{1,0:T(2,128)S(1)} %bitcast.130, pred[192,1024]{1,0:T(8,128)(4,1)S(1)} %broadcast_compare_fusion.2, ...), kind=kOutput, calls=%fused_computation.25.clone.1 | convolution fusion | flops 55074816 | bytes 3802632 | tf_op jit(solution)/shard_map/while/body/grqk,kgd->grqd/dot_general | solution.py:94
  130.8 3.6 %fusion.72 = (f32[2,192]{1,0:T(2,128)S(1)}, f32[1,2,192,1024]{3,2,1,0:T(8,128)S(1)}, f32[1,1024,192,2]{1,2,3,0:T(8,128)}) fusion(pred[192,1024]{1,0:T(8,128)(4,1)S(1)} %broadcast_compare_fusion.2, f32[2]{0:T(128)S(1)} %get-tuple-element.303, bf16[192,1,2,64]{0,3,2,1:T(8,128)(2,1)S(1)} %get-tuple-element.302, ...), kind=kOutput, calls=%fused_computation.63.clone.1 | convolution fusion | flops 54656640 | bytes 3655180 | tf_op jit(solution)/shard_map/while/body/qgrd,kgd->grqk/dot_general | solution.py:79
  134.7 0.6 bitcast_reduce_fusion.2
  136.2 2.9 %fusion.75 = f32[1,2,192,64]{2,3,1,0:T(8,128)S(1)} fusion(f32[1,2,192,64]{2,3,1,0:T(8,128)S(1)} %get-tuple-element.283, f32[1,2,192,1024]{3,2,1,0:T(8,128)S(1)} %reshape.140, f32[1,1024,192,2]{1,2,3,0:T(8,128)} %get-tuple-element.266, f32[2,192]{1,0:T(2,128)S(1)} %bitcast.130, pred[192,1024]{1,0:T(8,128)(4,1)S(1)} %broadcast_compare_fusion.2, ...), kind=kOutput, calls=%fused_computation.25.clone.1 | convolution fusion | flops 55074816 | bytes 3802632 | tf_op jit(solution)/shard_map/while/body/grqk,kgd->grqd/dot_general | solution.py:94
  139.4 3.6 %fusion.72 = (f32[2,192]{1,0:T(2,128)S(1)}, f32[1,2,192,1024]{3,2,1,0:T(8,128)S(1)}, f32[1,1024,192,2]{1,2,3,0:T(8,128)}) fusion(pred[192,1024]{1,0:T(8,128)(4,1)S(1)} %broadcast_compare_fusion.2, f32[2]{0:T(128)S(1)} %get-tuple-element.303, bf16[192,1,2,64]{0,3,2,1:T(8,128)(2,1)S(1)} %get-tuple-element.302, ...), kind=kOutput, calls=%fused_computation.63.clone.1 | convolution fusion | flops 54656640 | bytes 3655180 | tf_op jit(solution)/shard_map/while/body/qgrd,kgd->grqk/dot_general | solution.py:79
  143.3 0.6 bitcast_reduce_fusion.2
  144.0 0.5 fusion.74
  144.8 2.9 %fusion.75 = f32[1,2,192,64]{2,3,1,0:T(8,128)S(1)} fusion(f32[1,2,192,64]{2,3,1,0:T(8,128)S(1)} %get-tuple-element.283, f32[1,2,192,1024]{3,2,1,0:T(8,128)S(1)} %reshape.140, f32[1,1024,192,2]{1,2,3,0:T(8,128)} %get-tuple-element.266, f32[2,192]{1,0:T(2,128)S(1)} %bitcast.130, pred[192,1024]{1,0:T(8,128)(4,1)S(1)} %broadcast_compare_fusion.2, ...), kind=kOutput, calls=%fused_computation.25.clone.1 | convolution fusion | flops 55074816 | bytes 3802632 | tf_op jit(solution)/shard_map/while/body/grqk,kgd->grqd/dot_general | solution.py:94
  148.0 3.6 %fusion.72 = (f32[2,192]{1,0:T(2,128)S(1)}, f32[1,2,192,1024]{3,2,1,0:T(8,128)S(1)}, f32[1,1024,192,2]{1,2,3,0:T(8,128)}) fusion(pred[192,1024]{1,0:T(8,128)(4,1)S(1)} %broadcast_compare_fusion.2, f32[2]{0:T(128)S(1)} %get-tuple-element.303, bf16[192,1,2,64]{0,3,2,1:T(8,128)(2,1)S(1)} %get-tuple-element.302, ...), kind=kOutput, calls=%fused_computation.63.clone.1 | convolution fusion | flops 54656640 | bytes 3655180 | tf_op jit(solution)/shard_map/while/body/qgrd,kgd->grqk/dot_general | solution.py:79
  151.9 0.6 bitcast_reduce_fusion.2
  153.4 2.9 %fusion.75 = f32[1,2,192,64]{2,3,1,0:T(8,128)S(1)} fusion(f32[1,2,192,64]{2,3,1,0:T(8,128)S(1)} %get-tuple-element.283, f32[1,2,192,1024]{3,2,1,0:T(8,128)S(1)} %reshape.140, f32[1,1024,192,2]{1,2,3,0:T(8,128)} %get-tuple-element.266, f32[2,192]{1,0:T(2,128)S(1)} %bitcast.130, pred[192,1024]{1,0:T(8,128)(4,1)S(1)} %broadcast_compare_fusion.2, ...), kind=kOutput, calls=%fused_computation.25.clone.1 | convolution fusion | flops 55074816 | bytes 3802632 | tf_op jit(solution)/shard_map/while/body/grqk,kgd->grqd/dot_general | solution.py:94
  156.6 3.6 %fusion.72 = (f32[2,192]{1,0:T(2,128)S(1)}, f32[1,2,192,1024]{3,2,1,0:T(8,128)S(1)}, f32[1,1024,192,2]{1,2,3,0:T(8,128)}) fusion(pred[192,1024]{1,0:T(8,128)(4,1)S(1)} %broadcast_compare_fusion.2, f32[2]{0:T(128)S(1)} %get-tuple-element.303, bf16[192,1,2,64]{0,3,2,1:T(8,128)(2,1)S(1)} %get-tuple-element.302, ...), kind=kOutput, calls=%fused_computation.63.clone.1 | convolution fusion | flops 54656640 | bytes 3655180 | tf_op jit(solution)/shard_map/while/body/qgrd,kgd->grqk/dot_general | solution.py:79
  160.5 0.6 bitcast_reduce_fusion.2
  161.2 0.5 fusion.74
  161.9 2.9 %fusion.75 = f32[1,2,192,64]{2,3,1,0:T(8,128)S(1)} fusion(f32[1,2,192,64]{2,3,1,0:T(8,128)S(1)} %get-tuple-element.283, f32[1,2,192,1024]{3,2,1,0:T(8,128)S(1)} %reshape.140, f32[1,1024,192,2]{1,2,3,0:T(8,128)} %get-tuple-element.266, f32[2,192]{1,0:T(2,128)S(1)} %bitcast.130, pred[192,1024]{1,0:T(8,128)(4,1)S(1)} %broadcast_compare_fusion.2, ...), kind=kOutput, calls=%fused_computation.25.clone.1 | convolution fusion | flops 55074816 | bytes 3802632 | tf_op jit(solution)/shard_map/while/body/grqk,kgd->grqd/dot_general | solution.py:94
  165.1 3.6 %fusion.72 = (f32[2,192]{1,0:T(2,128)S(1)}, f32[1,2,192,1024]{3,2,1,0:T(8,128)S(1)}, f32[1,1024,192,2]{1,2,3,0:T(8,128)}) fusion(pred[192,1024]{1,0:T(8,128)(4,1)S(1)} %broadcast_compare_fusion.2, f32[2]{0:T(128)S(1)} %get-tuple-element.303, bf16[192,1,2,64]{0,3,2,1:T(8,128)(2,1)S(1)} %get-tuple-element.302, ...), kind=kOutput, calls=%fused_computation.63.clone.1 | convolution fusion | flops 54656640 | bytes 3655180 | tf_op jit(solution)/shard_map/while/body/qgrd,kgd->grqk/dot_general | solution.py:79
  169.1 0.6 bitcast_reduce_fusion.2
  170.5 2.9 %fusion.75 = f32[1,2,192,64]{2,3,1,0:T(8,128)S(1)} fusion(f32[1,2,192,64]{2,3,1,0:T(8,128)S(1)} %get-tuple-element.283, f32[1,2,192,1024]{3,2,1,0:T(8,128)S(1)} %reshape.140, f32[1,1024,192,2]{1,2,3,0:T(8,128)} %get-tuple-element.266, f32[2,192]{1,0:T(2,128)S(1)} %bitcast.130, pred[192,1024]{1,0:T(8,128)(4,1)S(1)} %broadcast_compare_fusion.2, ...), kind=kOutput, calls=%fused_computation.25.clone.1 | convolution fusion | flops 55074816 | bytes 3802632 | tf_op jit(solution)/shard_map/while/body/grqk,kgd->grqd/dot_general | solution.py:94
  173.7 3.6 %fusion.72 = (f32[2,192]{1,0:T(2,128)S(1)}, f32[1,2,192,1024]{3,2,1,0:T(8,128)S(1)}, f32[1,1024,192,2]{1,2,3,0:T(8,128)}) fusion(pred[192,1024]{1,0:T(8,128)(4,1)S(1)} %broadcast_compare_fusion.2, f32[2]{0:T(128)S(1)} %get-tuple-element.303, bf16[192,1,2,64]{0,3,2,1:T(8,128)(2,1)S(1)} %get-tuple-element.302, ...), kind=kOutput, calls=%fused_computation.63.clone.1 | convolution fusion | flops 54656640 | bytes 3655180 | tf_op jit(solution)/shard_map/while/body/qgrd,kgd->grqk/dot_general | solution.py:79
  177.7 0.6 bitcast_reduce_fusion.2
  179.1 2.9 %fusion.75 = f32[1,2,192,64]{2,3,1,0:T(8,128)S(1)} fusion(f32[1,2,192,64]{2,3,1,0:T(8,128)S(1)} %get-tuple-element.283, f32[1,2,192,1024]{3,2,1,0:T(8,128)S(1)} %reshape.140, f32[1,1024,192,2]{1,2,3,0:T(8,128)} %get-tuple-element.266, f32[2,192]{1,0:T(2,128)S(1)} %bitcast.130, pred[192,1024]{1,0:T(8,128)(4,1)S(1)} %broadcast_compare_fusion.2, ...), kind=kOutput, calls=%fused_computation.25.clone.1 | convolution fusion | flops 55074816 | bytes 3802632 | tf_op jit(solution)/shard_map/while/body/grqk,kgd->grqd/dot_general | solution.py:94
  182.3 3.6 %fusion.72 = (f32[2,192]{1,0:T(2,128)S(1)}, f32[1,2,192,1024]{3,2,1,0:T(8,128)S(1)}, f32[1,1024,192,2]{1,2,3,0:T(8,128)}) fusion(pred[192,1024]{1,0:T(8,128)(4,1)S(1)} %broadcast_compare_fusion.2, f32[2]{0:T(128)S(1)} %get-tuple-element.303, bf16[192,1,2,64]{0,3,2,1:T(8,128)(2,1)S(1)} %get-tuple-element.302, ...), kind=kOutput, calls=%fused_computation.63.clone.1 | convolution fusion | flops 54656640 | bytes 3655180 | tf_op jit(solution)/shard_map/while/body/qgrd,kgd->grqk/dot_general | solution.py:79
  186.3 0.6 bitcast_reduce_fusion.2
  187.0 0.5 fusion.74
  187.7 2.9 %fusion.75 = f32[1,2,192,64]{2,3,1,0:T(8,128)S(1)} fusion(f32[1,2,192,64]{2,3,1,0:T(8,128)S(1)} %get-tuple-element.283, f32[1,2,192,1024]{3,2,1,0:T(8,128)S(1)} %reshape.140, f32[1,1024,192,2]{1,2,3,0:T(8,128)} %get-tuple-element.266, f32[2,192]{1,0:T(2,128)S(1)} %bitcast.130, pred[192,1024]{1,0:T(8,128)(4,1)S(1)} %broadcast_compare_fusion.2, ...), kind=kOutput, calls=%fused_computation.25.clone.1 | convolution fusion | flops 55074816 | bytes 3802632 | tf_op jit(solution)/shard_map/while/body/grqk,kgd->grqd/dot_general | solution.py:94
  190.9 3.6 %fusion.72 = (f32[2,192]{1,0:T(2,128)S(1)}, f32[1,2,192,1024]{3,2,1,0:T(8,128)S(1)}, f32[1,1024,192,2]{1,2,3,0:T(8,128)}) fusion(pred[192,1024]{1,0:T(8,128)(4,1)S(1)} %broadcast_compare_fusion.2, f32[2]{0:T(128)S(1)} %get-tuple-element.303, bf16[192,1,2,64]{0,3,2,1:T(8,128)(2,1)S(1)} %get-tuple-element.302, ...), kind=kOutput, calls=%fused_computation.63.clone.1 | convolution fusion | flops 54656640 | bytes 3655180 | tf_op jit(solution)/shard_map/while/body/qgrd,kgd->grqk/dot_general | solution.py:79
  194.8 0.6 bitcast_reduce_fusion.2
  196.3 2.9 %fusion.75 = f32[1,2,192,64]{2,3,1,0:T(8,128)S(1)} fusion(f32[1,2,192,64]{2,3,1,0:T(8,128)S(1)} %get-tuple-element.283, f32[1,2,192,1024]{3,2,1,0:T(8,128)S(1)} %reshape.140, f32[1,1024,192,2]{1,2,3,0:T(8,128)} %get-tuple-element.266, f32[2,192]{1,0:T(2,128)S(1)} %bitcast.130, pred[192,1024]{1,0:T(8,128)(4,1)S(1)} %broadcast_compare_fusion.2, ...), kind=kOutput, calls=%fused_computation.25.clone.1 | convolution fusion | flops 55074816 | bytes 3802632 | tf_op jit(solution)/shard_map/while/body/grqk,kgd->grqd/dot_general | solution.py:94
  199.4 13.1 %all_to_all.5 = bf16[8,192,128]{2,1,0:T(8,128)(2,1)S(1)} all-to-all(bf16[8,192,128]{2,1,0:T(8,128)(2,1)S(1)} %broadcast_in_dim.29), channel_id=1, replica_groups=mesh['sp_0'=16,'sp_1'=4,'tp'=8] {'tp'}, dimensions={0} | all-to-all | bytes 786432 | tf_op jit(solution)/shard_map/all_to_all | solution.py:29
  212.5 4.1 %convolution_convert_fusion = bf16[192,2048]{1,0:T(8,128)(2,1)} fusion(bf16[1024,2048]{1,0:T(8,128)(2,1)} %all-gather.5.cloned.1.call-done, bf16[8,192,128]{2,1,0:T(8,128)(2,1)S(1)} %all_to_all.5), kind=kOutput, calls=%fused_computation.43 | convolution fusion | flops 805699584 | bytes 5373952 | tf_op jit(solution)/shard_map/dot_general | solution.py:105
  (113 shorter events, 15.7 us)
Async XLA Ops:
  6.5 3.1 %copy-start = (bf16[192,2048]{1,0:T(8,128)(2,1)S(1)}, bf16[192,2048]{1,0:T(8,128)(2,1)}, u32[]{:S(2)}) copy-start(bf16[192,2048]{1,0:T(8,128)(2,1)} %param.9) | copy-start | bytes 2359300
  6.5 3.1 %copy-start.2 = (f32[2048]{0:T(1024)S(1)}, f32[2048]{0:T(1024)}, u32[]{:S(2)}) copy-start(f32[2048]{0:T(1024)} %param.10) | copy-start | bytes 24580
  6.5 3.1 %copy-start.1 = (bf16[2048,128]{1,0:T(8,128)(2,1)S(1)}, bf16[2048,128]{1,0:T(8,128)(2,1)}, u32[]{:S(2)}) copy-start(bf16[2048,128]{1,0:T(8,128)(2,1)} %param.11) | copy-start | bytes 1572868
  6.5 89.6 %all-gather.3.cloned.1.call-start = ((), (), s32[]{:S(2)}) async-start(), calls=%async_computation.1 | async-start | bytes 3342336 | tf_op jit(solution)/shard_map/all_gather | solution.py:17
  9.6 86.6 %copy-start.3 = (f32[2]{0:T(128)S(1)}, f32[2]{0:T(128)}, u32[]{:S(2)}) copy-start(f32[2]{0:T(128)} %param.14) | copy-start | bytes 28
  23.7 188.8 %all-gather.5.cloned.1.call-start = ((), (), s32[]{:S(2)}) async-start(), calls=%async_computation.2 | async-start | bytes 4718592 | tf_op jit(solution)/shard_map/all_gather | solution.py:107
Sparse Core Ops, SparseCore 0:
  23.8 72.3 all-gather.2
  98.3 38.0 all-gather.4
where the time goes:
time: 224 us; the launch traced here: 223 us
  matrix products  91 us (41%)
  waiting for transfers between devices  72.3 us (32%)
  blocking collectives  26.4 us (12%)
  between operations  13.5 us (6%)
  other arithmetic  10.5 us (5%)
  local copies, waits for them, and re-layouts  8.7 us (4%)
    all_gather x1, waiting for transfers between devices, gather_axes(): value = lax.all_gather(value, axis, axis=dim, tiled=True)  71.6 us
    dot_general x12, matrix products, sweep(): jnp.einsum('qgrd,kgd->grqk', grouped, key_block, preferred_element_type=j...  43.4 us
    dot_general x12, matrix products, sweep(): jnp.einsum('grqk,kgd->grqd', weight, value_block, preferred_element_type=...  35.3 us
    all_gather x1, blocking collectives, gather_axes(): value = lax.all_gather(value, axis, axis=dim, tiled=True)  13.4 us
    all_to_all x1, blocking collectives, sent_to_all(): lax.all_to_all(jnp.broadcast_to(value[None], (length, *value.shape)), axi...  13.1 us
    reduce_sum x12, other arithmetic, sweep(): piece_sums = jnp.sum(split_keep, axis=4)  6.64 us
    dot_general x12, matrix products, sweep(): within = jnp.einsum('grqpj,js->grqps', split_keep, inner_later)  5.75 us
  transfers between devices with their start and end apart: 2, of which 1 were waited for; matrix products, arithmetic and copies ran while one was open for 46% of the time, Pallas kernels for 0%

commit v1 on v0

v1 whole, which is shorter than its diff:
```python
import math

import jax
import jax.numpy as jnp
from jax import lax
from jax.experimental import pallas as pl
from jax.experimental.pallas import tpu as pltpu
from jax.sharding import Mesh
from jax.sharding import PartitionSpec as P

HEAD_DIM = 64
TILE = 256
VMEM = pltpu.VMEM
SMEM = pltpu.SMEM
LIMIT = 56 * 1024 * 1024


def project_kernel(half_ref, hidden_ref, gain_ref, wq_ref, wk_ref, wv_ref, q_ref, kv_ref):
    wide = hidden_ref[...].astype(jnp.float32)
    inv = lax.rsqrt(jnp.mean(wide * wide, axis=-1, keepdims=True) + 1e-06)
    normed = (wide * inv * gain_ref[...]).astype(jnp.bfloat16)
    q = jnp.dot(normed, wq_ref[...], preferred_element_type=jnp.float32).astype(jnp.bfloat16)
    q = q * jnp.bfloat16(HEAD_DIM**-0.5)
    for dest in range(q_ref.shape[0]):
        q_ref[dest] = q
    k = jnp.dot(normed, wk_ref[...], preferred_element_type=jnp.float32)
    v = jnp.dot(normed, wv_ref[...], preferred_element_type=jnp.float32)
    upper = half_ref[0] == 1
    lane = lax.broadcasted_iota(jnp.int32, k.shape, 1)
    k_side = jnp.where(upper, pltpu.roll(k, HEAD_DIM, 1), k)
    v_side = jnp.where(upper, v, pltpu.roll(v, HEAD_DIM, 1))
    kv_ref[...] = jnp.where(lane < HEAD_DIM, k_side, v_side).astype(jnp.bfloat16)


def attend_kernel(rel_ref, bias_ref, q_ref, kv_ref, out_ref, qs, acc, carry):
    key_tiles = kv_ref.shape[0] // TILE
    blocks, tok = q_ref.shape[0], q_ref.shape[1]
    tokens = blocks * tok
    row_tiles = tokens // TILE
    rows = 2 * TILE
    lane = lax.broadcasted_iota(jnp.int32, (tok, 2 * HEAD_DIM), 1)
    for b in range(blocks):
        q = q_ref[b].astype(jnp.float32)
        qs[0, b * tok : (b + 1) * tok, :] = jnp.where(lane < HEAD_DIM, q, 0.0).astype(jnp.bfloat16)
        turned = jnp.where(lane < HEAD_DIM, pltpu.roll(q, HEAD_DIM, 1), 0.0)
        qs[1, b * tok : (b + 1) * tok, :] = turned.astype(jnp.bfloat16)
    acc[...] = jnp.zeros_like(acc)
    carry[...] = jnp.zeros_like(carry)
    from_row = lax.broadcasted_iota(jnp.int32, (TILE, TILE), 0)
    to_col = lax.broadcasted_iota(jnp.int32, (TILE, TILE), 1)
    later = (from_row > to_col).astype(jnp.bfloat16)
    rel = rel_ref[0]

    def step(i, k, masked):
        kv = kv_ref[pl.ds(pl.multiple_of(k * TILE, TILE), TILE), :]
        q = jnp.concatenate([qs[h, i * TILE : (i + 1) * TILE, :] for h in range(2)], axis=0)
        raw = lax.dot_general(q, kv, (((1,), (1,)), ((), ())), preferred_element_type=jnp.float32)
        z = jnp.concatenate([raw[:TILE] + bias_ref[0], raw[TILE:] + bias_ref[1]], axis=0)
        soft = jnp.maximum(z, jnp.log(1.0 + jnp.exp(jnp.minimum(z, 80.0))))
        gain = z - soft
        if masked:
            t = lax.broadcasted_iota(jnp.int32, (rows, TILE), 0) & (TILE - 1)
            s = lax.broadcasted_iota(jnp.int32, (rows, TILE), 1)
            soft = jnp.where(s < t, soft, 0.0)
        between = jnp.dot(soft.astype(jnp.bfloat16), later, preferred_element_type=jnp.float32)
        held = carry[i]
        expo = gain - between - jnp.concatenate([held, held], axis=1)
        weight = jnp.exp(expo)
        if masked:
            weight = jnp.where(s < t, weight, 0.0)
        acc[i] += jnp.dot(weight.astype(jnp.bfloat16), kv, preferred_element_type=jnp.float32)
        carry[i] = held + jnp.broadcast_to(between[:, :1] + soft[:, :1], held.shape)

    for i in range(row_tiles):
        spot = rel + i

        @pl.when((spot >= 0) & (spot < key_tiles))
        def _():
            step(i, spot, True)

        whole = jnp.clip(spot, 0, key_tiles)

        @pl.loop(0, whole)
        def _(n):
            step(i, whole - 1 - n, False)

    wide_lane = lax.broadcasted_iota(jnp.int32, (TILE, 2 * HEAD_DIM), 1)
    for i in range(row_tiles):
        part = jnp.where(
            wide_lane < HEAD_DIM, pltpu.roll(acc[i, :TILE], HEAD_DIM, 1), acc[i, TILE:]
        )
        decay = jnp.exp(-jnp.where(wide_lane < HEAD_DIM, carry[i, :TILE], carry[i, TILE:]))
        out_ref[i * TILE : (i + 1) * TILE, : 2 * HEAD_DIM] = part.astype(jnp.bfloat16)
        out_ref[i * TILE : (i + 1) * TILE, 2 * HEAD_DIM :] = decay.astype(jnp.bfloat16)


def project_out_kernel(heads_ref, weight_ref, out_ref, joined):
    @pl.when(pl.program_id(0) == 0)
    def _():
        for t in range(heads_ref.shape[0]):
            joined[:, t * 128 : (t + 1) * 128] = heads_ref[t]

    out_ref[...] = jnp.dot(
        joined[...], weight_ref[...], preferred_element_type=jnp.float32
    ).astype(jnp.bfloat16)


def local(hidden, norm_gain, query_weight, key_weight, value_weight, head_bias, output_weight):
    rows, width = hidden.shape
    zs, ys, xs = lax.axis_size("z"), lax.axis_size("y"), lax.axis_size("x")
    tps = xs * lax.axis_size("c")
    z, y, x = lax.axis_index("z"), lax.axis_index("y"), lax.axis_index("x")
    mine = 2 * HEAD_DIM
    whole_out = lax.all_gather(output_weight, ("x", "c"), axis=0, tiled=True)

    whole = lambda *shape: pl.BlockSpec(shape, lambda i, pick: (0,) * len(shape))
    side = pl.BlockSpec((width, mine), lambda i, pick: (0, pick[1]))
    pick = jnp.stack([x % 2, x // 2]).astype(jnp.int32)
    q_all, kv = pl.pallas_call(
        project_kernel,
        grid_spec=pltpu.PrefetchScalarGridSpec(
            num_scalar_prefetch=1,
            grid=(1,),
            in_specs=[whole(rows, width), whole(1, width), whole(width, mine), side, side],
            out_specs=[whole(ys, rows, mine), whole(rows, mine)],
        ),
        out_shape=[
            jax.ShapeDtypeStruct((ys, rows, mine), jnp.bfloat16),
            jax.ShapeDtypeStruct((rows, mine), jnp.bfloat16),
        ],
        compiler_params=pltpu.CompilerParams(vmem_limit_bytes=LIMIT),
        cost_estimate=pl.CostEstimate(
            flops=2 * rows * width * 3 * mine, bytes_accessed=2 * width * (rows + 3 * mine), transcendentals=0
        ),
        name="project",
    )(pick, hidden, norm_gain[None, :], query_weight, key_weight, value_weight)

    moved = lax.ppermute(
        kv, ("z", "y"), [(blk, (blk % zs) * ys + blk // zs) for blk in range(zs * ys)]
    )
    row_q = lax.all_to_all(q_all, "y", 0, 0, tiled=True)
    quarter = lax.all_gather(moved, "z", axis=0, tiled=True)

    tokens = ys * rows
    row_tiles = tokens // TILE
    rel = (z * row_tiles - y * (zs * rows // TILE)).astype(jnp.int32).reshape(1)
    part = pl.pallas_call(
        attend_kernel,
        in_specs=[
            pl.BlockSpec(memory_space=SMEM),
            pl.BlockSpec(memory_space=SMEM),
            pl.BlockSpec(memory_space=VMEM),
            pl.BlockSpec(memory_space=VMEM),
        ],
        out_specs=pl.BlockSpec(memory_space=VMEM),
        out_shape=jax.ShapeDtypeStruct((tokens, 2 * mine), jnp.bfloat16),
        scratch_shapes=[
            VMEM((2, tokens, mine), jnp.bfloat16),
            VMEM((row_tiles, 2 * TILE, mine), jnp.float32),
            VMEM((row_tiles, 2 * TILE, mine), jnp.float32),
        ],
        compiler_params=pltpu.CompilerParams(vmem_limit_bytes=LIMIT),
        cost_estimate=pl.CostEstimate(flops=10**10, bytes_accessed=2 * 10**6, transcendentals=0),
        name="attend",
    )(rel, head_bias, row_q, quarter)

    parts = lax.all_to_all(part.reshape(ys, rows, 2 * mine), "y", 0, 0, tiled=True)
    parts = parts.astype(jnp.float32)
    total = parts[0, :, :mine]
    for n in range(1, ys):
        total = parts[n, :, :mine] + parts[n, :, mine:] * total
    attended = total.astype(jnp.bfloat16)
    every_head = lax.all_to_all(
        jnp.broadcast_to(attended[None], (tps, rows, mine)), ("x", "c"), 0, 0, tiled=True
    )
    depth, cols = whole_out.shape
    block = 512
    return pl.pallas_call(
        project_out_kernel,
        grid=(cols // block,),
        in_specs=[
            pl.BlockSpec((tps, rows, mine), lambda n: (0, 0, 0)),
            pl.BlockSpec((depth, block), lambda n: (0, n)),
        ],
        out_specs=pl.BlockSpec((rows, block), lambda n: (0, n)),
        out_shape=jax.ShapeDtypeStruct((rows, cols), jnp.bfloat16),
        scratch_shapes=[VMEM((rows, depth), jnp.bfloat16)],
        compiler_params=pltpu.CompilerParams(vmem_limit_bytes=LIMIT),
        cost_estimate=pl.CostEstimate(
            flops=2 * rows * depth * cols, bytes_accessed=2 * depth * cols, transcendentals=0
        ),
        name="project_out",
    )(every_head, whole_out)


def solution(mesh):
    torus = Mesh(mesh.devices.reshape(16, 4, 4, 2), ("z", "y", "x", "c"))
    sp, tp = ("z", "y"), ("x", "c")
    in_specs = (P(sp, None), P(), P(None, tp), P(), P(), P(tp), P(tp, None))
    return jax.shard_map(
        local, mesh=torus, in_specs=in_specs, out_specs=P(sp, None), check_vma=False
    )
```

time: 224 us -> 124 us (0.55)
  the two profiles are of different devices: /device:TPU:480 before, /device:TPU:96 now
where the time goes in v1:
time: 124 us; the launch traced here: 123 us
  blocking collectives  62.4 us (50%)
  Pallas kernels  30.7 us (25%)
  starting transfers between devices  14.7 us (12%)
  between operations  13.5 us (11%)
    all_gather x1, blocking collectives, local(): quarter = lax.all_gather(moved, 'z', axis=0, tiled=True)  38.6 us
    pallas_call x1, Pallas kernels, local(): pl.pallas_call(attend_kernel, in_specs=[pl.BlockSpec(memory_space=SMEM),...  21.9 us
    all_to_all x1, blocking collectives, local(): lax.all_to_all(jnp.broadcast_to(attended[None], (tps, rows, mine)), ('x',...  12.9 us
    ppermute x1, starting transfers between devices, local(): lax.ppermute(kv, ('z', 'y'), [(blk, blk % zs * ys + blk // zs) for blk in...  11.4 us
    all_to_all x1, blocking collectives, local(): lax.all_to_all(part.reshape(ys, rows, 2 * mine), 'y', 0, 0, tiled=True)  10.8 us
    pallas_call x1, Pallas kernels, local(): pl.pallas_call(project_out_kernel, grid=(cols // block,), in_specs=[pl.Bl...  4.85 us
    pallas_call x1, Pallas kernels, local(): pl.pallas_call(project_kernel, grid_spec=pltpu.PrefetchScalarGridSpec(num...  3.92 us
    all_to_all x1, starting transfers between devices, local(): row_q = lax.all_to_all(q_all, 'y', 0, 0, tiled=True)  3.38 us
  transfers between devices with their start and end apart: 3, of which 0 were waited for; matrix products, arithmetic and copies ran while one was open for 1% of the time, Pallas kernels for 21%

profile of v1, /device:TPU:96, one launch (start us, length us, event | category | flops | bytes accessed | tf_op | source)
XLA Modules:
  0.0 123.5 jit_solution(15255687859681638045)
XLA Ops:
  6.5 0.0 all-gather.2.cloned.1.call-start
  6.5 0.7 all-gather.2.cloned.1.call-update
  7.3 0.7 pad_add_fusion.half_ref
  7.9 3.9 %project.1 = (bf16[4,192,128]{2,1,0:T(8,128)(2,1)}, bf16[192,128]{1,0:T(8,128)(2,1)}) custom-call(s32[2]{0:T(128)} %pad_add_fusion.half_ref, bf16[192,2048]{1,0:T(8,128)(2,1)} %hidden_ref.1, f32[1,2048]{1,0:T(1,128)} %bitcast.8, bf16[2048,128]{1,0:T(8,128)(2,1)} %wq_ref.1, bf16[2048,256]{1,0:T(8,128)(2,1)} %wk_ref.1, bf16[2048,256]{1,0:T(8,128)(2,1)} %wv_ref.1), custom_call_target="tpu_custom_call" | custom-call | flops 301989888 | bytes 2359296 | tf_op jit(solution)/shard_map/project/pallas_call | solution.py:119
  11.8 11.4 %collective-permute-start = (bf16[192,128]{1,0:T(8,128)(2,1)}, bf16[192,128]{1,0:T(8,128)(2,1)S(1)}, u32[]{:S(2)}, u32[]{:S(2)}) collective-permute-start(bf16[192,128]{1,0:T(8,128)(2,1)} %get-tuple-element.8), channel_id=1, source_target_pairs={{0,0},{8,32},{16,64},{24,96},{32,128},{40,160},{48,192},{56,224},{... | collective-permute-start | bytes 147464 | tf_op jit(solution)/shard_map/ppermute | solution.py:138
  23.2 3.4 %all-to-all-start = ((bf16[4,192,128]{2,1,0:T(8,128)(2,1)}), bf16[4,192,128]{2,1,0:T(8,128)(2,1)S(1)}, u32[]{:S(2)}, u32[]{:S(2)}) async-start(bf16[4,192,128]{2,1,0:T(8,128)(2,1)} %get-tuple-element.7), calls=%async_computation | async-start | bytes 393216 | tf_op jit(solution)/shard_map/all_to_all | solution.py:141
  26.6 0.0 collective-permute-done
  26.6 38.6 %all_gather.6.kv_ref = bf16[3072,128]{1,0:T(8,128)(2,1)} all-gather(bf16[192,128]{1,0:T(8,128)(2,1)S(1)} %collective-permute-done), channel_id=1, replica_groups=mesh['z'=16,'y'=4,'x'=4,'c'=2] {'z'}, dimensions={0}, use_global_device_ids=true | all-gather | bytes 835584 | tf_op jit(solution)/shard_map/all_gather | solution.py:142
  65.3 0.0 all-to-all-done.q_ref
  65.3 0.0 copy-start
  65.3 0.7 copy-done
  66.0 21.9 %attend.1 = bf16[768,256]{1,0:T(8,128)(2,1)} custom-call(s32[1]{0:T(128)} %bitcast.rel_ref, f32[2]{0:T(128)} %bias_ref.1, bf16[4,192,128]{2,1,0:T(8,128)(2,1)} %copy-done, bf16[3072,128]{1,0:T(8,128)(2,1)} %all_gather.6.kv_ref), custom_call_target="tpu_custom_call" | custom-call | flops 10000000000 | bytes 2000000 | tf_op jit(solution)/shard_map/attend/pallas_call | solution.py:147
  87.9 10.8 %all_to_all.15 = bf16[4,192,256]{2,1,0:T(8,128)(2,1)S(1)} all-to-all(bf16[4,192,256]{2,1,0:T(8,128)(2,1)} %bitcast.7), channel_id=1, replica_groups=mesh['z'=16,'y'=4,'x'=4,'c'=2] {'y'}, dimensions={0} | all-to-all | bytes 786432 | tf_op jit(solution)/shard_map/all_to_all | solution.py:167
  98.7 0.1 convert_element_type.7
  98.8 0.1 broadcast_in_dim.13
  98.8 12.9 %all_to_all.16.heads_ref = bf16[8,192,128]{2,1,0:T(8,128)(2,1)} all-to-all(bf16[8,192,128]{2,1,0:T(8,128)(2,1)S(1)} %broadcast_in_dim.13), channel_id=1, replica_groups=mesh['z'=16,'y'=4,'x'=4,'c'=2] {'x','c'}, dimensions={0} | all-to-all | bytes 786432 | tf_op jit(solution)/shard_map/all_to_all | solution.py:173
  111.8 0.0 all-gather.2.cloned.1.call-done.weight_ref
  111.8 4.8 %project_out.1 = bf16[192,2048]{1,0:T(8,128)(2,1)} custom-call(bf16[8,192,128]{2,1,0:T(8,128)(2,1)} %all_to_all.16.heads_ref, bf16[1024,2048]{1,0:T(8,128)(2,1)} %all-gather.2.cloned.1.call-done.weight_ref), custom_call_target="tpu_custom_call" | custom-call | flops 805306368 | bytes 4194304 | tf_op jit(solution)/shard_map/project_out/pallas_call | solution.py:178
  (1 shorter events, 0.0 us)
Async XLA Ops:
  6.5 105.2 %all-gather.2.cloned.1.call-start = ((), (), s32[]{:S(2)}) async-start(), calls=%async_computation.3 | async-start | bytes 4718592 | tf_op jit(solution)/shard_map/all_gather | solution.py:114
  11.8 14.8 %collective-permute-start = (bf16[192,128]{1,0:T(8,128)(2,1)}, bf16[192,128]{1,0:T(8,128)(2,1)S(1)}, u32[]{:S(2)}, u32[]{:S(2)}) collective-permute-start(bf16[192,128]{1,0:T(8,128)(2,1)} %get-tuple-element.8), channel_id=1, source_target_pairs={{0,0},{8,32},{16,64},{24,96},{32,128},{40,160},{48,192},{56,224},{... | collective-permute-start | bytes 147464 | tf_op jit(solution)/shard_map/ppermute | solution.py:138
  23.2 42.1 %all-to-all-start = ((bf16[4,192,128]{2,1,0:T(8,128)(2,1)}), bf16[4,192,128]{2,1,0:T(8,128)(2,1)S(1)}, u32[]{:S(2)}, u32[]{:S(2)}) async-start(bf16[4,192,128]{2,1,0:T(8,128)(2,1)} %get-tuple-element.7), calls=%async_computation | async-start | bytes 393216 | tf_op jit(solution)/shard_map/all_to_all | solution.py:141
  65.3 0.7 copy-start
Sparse Core Ops, SparseCore 0:
  9.5 43.0 all-gather.1

commit v2 on v1

v2 whole, which is shorter than its diff:
```python
import jax
import jax.numpy as jnp
from jax import lax
from jax.experimental import pallas as pl
from jax.experimental.pallas import tpu as pltpu
from jax.sharding import Mesh
from jax.sharding import PartitionSpec as P

HEAD_DIM = 64
TILE = 256
VMEM = pltpu.VMEM
SMEM = pltpu.SMEM
LIMIT = 56 * 1024 * 1024


def project_kernel(
    hidden_ref, gain_ref, wq_hbm, wk_hbm, wv_hbm, q_ref, kv_ref, wq_ref, wk_ref, wv_ref, sems
):
    copies = [
        pltpu.make_async_copy(src, dst, sems.at[n])
        for n, (src, dst) in enumerate(((wk_hbm, wk_ref), (wv_hbm, wv_ref), (wq_hbm, wq_ref)))
    ]
    for copy in copies:
        copy.start()
    x = lax.axis_index("x")
    wide = hidden_ref[...].astype(jnp.float32)
    inv = lax.rsqrt(jnp.mean(wide * wide, axis=-1, keepdims=True) + 1e-06)
    normed = (wide * inv * gain_ref[...]).astype(jnp.bfloat16)

    def own(full):
        pair = jnp.where(x >= 2, full[:, 2 * HEAD_DIM :], full[:, : 2 * HEAD_DIM])
        return pair, pltpu.roll(pair, HEAD_DIM, 1)

    copies[0].wait()
    k, k_turned = own(jnp.dot(normed, wk_ref[...], preferred_element_type=jnp.float32))
    copies[1].wait()
    v, v_turned = own(jnp.dot(normed, wv_ref[...], preferred_element_type=jnp.float32))
    upper = x % 2 == 1
    lane = lax.broadcasted_iota(jnp.int32, k.shape, 1)
    k_side = jnp.where(upper, k_turned, k)
    v_side = jnp.where(upper, v, v_turned)
    kv_ref[...] = jnp.where(lane < HEAD_DIM, k_side, v_side).astype(jnp.bfloat16)
    copies[2].wait()
    q = jnp.dot(normed, wq_ref[...], preferred_element_type=jnp.float32).astype(jnp.bfloat16)
    q = q * jnp.bfloat16(HEAD_DIM**-0.5)
    for dest in range(q_ref.shape[0]):
        q_ref[dest] = q


def attend_kernel(rel_ref, bias_ref, q_ref, kv_ref, out_ref, qs, acc, carry):
    key_tiles = kv_ref.shape[0] // TILE
    blocks, tok = q_ref.shape[0], q_ref.shape[1]
    tokens = blocks * tok
    row_tiles = tokens // TILE
    lane = lax.broadcasted_iota(jnp.int32, (tok, 2 * HEAD_DIM), 1)
    for b in range(blocks):
        q = q_ref[b].astype(jnp.float32)
        qs[b * tok : (b + 1) * tok, :] = jnp.where(lane < HEAD_DIM, q, 0.0).astype(jnp.bfloat16)
        turned = jnp.where(lane < HEAD_DIM, pltpu.roll(q, HEAD_DIM, 1), 0.0)
        qs[tokens + b * tok : tokens + (b + 1) * tok, :] = turned.astype(jnp.bfloat16)
    acc[...] = jnp.zeros_like(acc)
    carry[...] = jnp.zeros_like(carry)
    from_row = lax.broadcasted_iota(jnp.int32, (TILE, TILE), 0)
    to_col = lax.broadcasted_iota(jnp.int32, (TILE, TILE), 1)
    later = (from_row > to_col).astype(jnp.bfloat16)
    rel = rel_ref[0]

    def step(k, masked):
        kv = kv_ref[pl.ds(pl.multiple_of(k * TILE, TILE), TILE), :]
        raw = lax.dot_general(
            qs[...], kv, (((1,), (1,)), ((), ())), preferred_element_type=jnp.float32
        )
        z = jnp.concatenate([raw[:tokens] + bias_ref[0], raw[tokens:] + bias_ref[1]], axis=0)
        soft = jnp.maximum(z, jnp.log(1.0 + jnp.exp(jnp.minimum(z, 80.0))))
        gain = z - soft
        if masked:
            t = lax.broadcasted_iota(jnp.int32, (tokens, TILE), 0)
            t = jnp.concatenate([t, t], axis=0)
            s = lax.broadcasted_iota(jnp.int32, (2 * tokens, TILE), 1) + (k - rel) * TILE
            soft = jnp.where(s < t, soft, 0.0)
        between = jnp.dot(soft.astype(jnp.bfloat16), later, preferred_element_type=jnp.float32)
        held = carry[...]
        weight = jnp.exp(gain - between - jnp.concatenate([held, held], axis=1))
        if masked:
            weight = jnp.where(s < t, weight, 0.0)
        acc[...] += jnp.dot(weight.astype(jnp.bfloat16), kv, preferred_element_type=jnp.float32)
        carry[...] = held + jnp.broadcast_to(between[:, :1] + soft[:, :1], held.shape)

    @pl.when((rel >= 0) & (rel < key_tiles))
    def _():
        @pl.loop(0, row_tiles)
        def _(n):
            step(rel + row_tiles - 1 - n, True)

    whole = jnp.clip(rel, 0, key_tiles)

    @pl.loop(0, whole)
    def _(n):
        step(whole - 1 - n, False)

    wide_lane = lax.broadcasted_iota(jnp.int32, (tokens, 2 * HEAD_DIM), 1)
    first, second = slice(0, tokens), slice(tokens, 2 * tokens)
    part = jnp.where(wide_lane < HEAD_DIM, pltpu.roll(acc[first], HEAD_DIM, 1), acc[second])
    decay = jnp.exp(-jnp.where(wide_lane < HEAD_DIM, carry[first], carry[second]))
    out_ref[:, : 2 * HEAD_DIM] = part.astype(jnp.bfloat16)
    out_ref[:, 2 * HEAD_DIM :] = decay.astype(jnp.bfloat16)


def project_out_kernel(heads_ref, own_ref, other_ref, out_ref, joined):
    c = lax.axis_index("c")
    xs, mine = own_ref.shape[0], own_ref.shape[1]
    for side, core in enumerate((c, 1 - c)):
        for x in range(xs):
            col = (side * xs + x) * mine
            joined[:, col : col + mine] = heads_ref[2 * x + core]
    half = xs * mine
    block = 512
    for n in range(out_ref.shape[1] // block):
        cols = slice(n * block, (n + 1) * block)
        total = jnp.dot(
            joined[:, :half], own_ref[:, :, cols].reshape(half, block), preferred_element_type=jnp.float32
        )
        total += jnp.dot(
            joined[:, half:], other_ref[:, :, cols].reshape(half, block), preferred_element_type=jnp.float32
        )
        out_ref[:, cols] = total.astype(jnp.bfloat16)


def local(hidden, norm_gain, query_weight, key_weight, value_weight, head_bias, output_weight):
    rows, width = hidden.shape
    zs, ys, xs = lax.axis_size("z"), lax.axis_size("y"), lax.axis_size("x")
    tps = xs * lax.axis_size("c")
    z, y = lax.axis_index("z"), lax.axis_index("y")
    mine = 2 * HEAD_DIM
    vmem = pl.BlockSpec(memory_space=VMEM)
    smem = pl.BlockSpec(memory_space=SMEM)
    anywhere = pl.BlockSpec(memory_space=pl.ANY)

    kv_cols = key_weight.shape[1]
    q_all, kv = pl.pallas_call(
        project_kernel,
        in_specs=[vmem, vmem, anywhere, anywhere, anywhere],
        out_specs=[vmem, vmem],
        out_shape=[
            jax.ShapeDtypeStruct((ys, rows, mine), jnp.bfloat16),
            jax.ShapeDtypeStruct((rows, mine), jnp.bfloat16),
        ],
        scratch_shapes=[
            VMEM((width, mine), jnp.bfloat16),
            VMEM((width, kv_cols), jnp.bfloat16),
            VMEM((width, kv_cols), jnp.bfloat16),
            pltpu.SemaphoreType.DMA((3,)),
        ],
        compiler_params=pltpu.CompilerParams(vmem_limit_bytes=LIMIT),
        cost_estimate=pl.CostEstimate(
            flops=2 * rows * width * (mine + 2 * kv_cols),
            bytes_accessed=2 * width * (rows + mine + 2 * kv_cols),
            transcendentals=0,
        ),
        name="project",
    )(hidden, norm_gain[None, :], query_weight, key_weight, value_weight)

    moved = lax.ppermute(
        kv, ("z", "y"), [(blk, (blk % zs) * ys + blk // zs) for blk in range(zs * ys)]
    )
    row_q = lax.all_to_all(q_all, "y", 0, 0, tiled=True)
    row_q, moved, output_weight = lax.optimization_barrier((row_q, moved, output_weight))
    own_rows = lax.all_to_all(
        jnp.broadcast_to(output_weight[None], (xs, *output_weight.shape)), "x", 0, 0, tiled=True
    )
    quarter = lax.all_gather(moved, "z", axis=0, tiled=True)
    quarter, own_rows = lax.optimization_barrier((quarter, own_rows))
    other_rows = lax.ppermute(own_rows, "c", [(0, 1), (1, 0)])

    tokens = ys * rows
    rel = (z * (tokens // TILE) - y * (zs * rows // TILE)).astype(jnp.int32).reshape(1)
    part = pl.pallas_call(
        attend_kernel,
        in_specs=[smem, smem, vmem, vmem],
        out_specs=vmem,
        out_shape=jax.ShapeDtypeStruct((tokens, 2 * mine), jnp.bfloat16),
        scratch_shapes=[
            VMEM((2 * tokens, mine), jnp.bfloat16),
            VMEM((2 * tokens, mine), jnp.float32),
            VMEM((2 * tokens, mine), jnp.float32),
        ],
        compiler_params=pltpu.CompilerParams(vmem_limit_bytes=LIMIT),
        cost_estimate=pl.CostEstimate(flops=10**10, bytes_accessed=2 * 10**6, transcendentals=0),
        name="attend",
    )(rel, head_bias, row_q, quarter)

    parts = lax.all_to_all(part.reshape(ys, rows, 2 * mine), "y", 0, 0, tiled=True)
    parts = parts.astype(jnp.float32)
    total = parts[0, :, :mine]
    for n in range(1, ys):
        total = parts[n, :, :mine] + parts[n, :, mine:] * total
    attended = total.astype(jnp.bfloat16)
    every_head = lax.all_to_all(
        jnp.broadcast_to(attended[None], (tps, rows, mine)), ("x", "c"), 0, 0, tiled=True
    )
    cols = output_weight.shape[1]
    return pl.pallas_call(
        project_out_kernel,
        in_specs=[vmem, vmem, vmem],
        out_specs=vmem,
        out_shape=jax.ShapeDtypeStruct((rows, cols), jnp.bfloat16),
        scratch_shapes=[VMEM((rows, tps * mine), jnp.bfloat16)],
        compiler_params=pltpu.CompilerParams(vmem_limit_bytes=20 * 1024 * 1024),
        cost_estimate=pl.CostEstimate(
            flops=2 * rows * tps * mine * cols, bytes_accessed=2 * tps * mine * cols, transcendentals=0
        ),
        name="project_out",
    )(every_head, own_rows, other_rows)


def solution(mesh):
    torus = Mesh(mesh.devices.reshape(16, 4, 4, 2), ("z", "y", "x", "c"))
    sp, tp = ("z", "y"), ("x", "c")
    in_specs = (P(sp, None), P(), P(None, tp), P(), P(), P(tp), P(tp, None))
    return jax.shard_map(
        local, mesh=torus, in_specs=in_specs, out_specs=P(sp, None), check_vma=False
    )
```

time: 124 us -> 117 us (0.944)
  between operations: 13.5 us -> 0.06 us
  starting transfers between devices: 14.7 us -> 22 us
  Pallas kernels: 30.7 us -> 24.5 us
  blocking collectives: 62.4 us -> 65.8 us
  waiting for transfers between devices: 0.72 us -> 2.05 us
    pallas_call x3, Pallas kernels: 30.7 us -> 24.5 us  [the longest x1 16.3 us: local(): pl.pallas_call(attend_kernel, in_specs=[smem, smem, vmem, vmem], out_spec...]
    all_to_all x0 -> x1, starting transfers between devices: none -> 4.29 us  [local(): lax.all_to_all(jnp.broadcast_to(output_weight[None], (xs, *output_weight....]
    ppermute x1, waiting for transfers between devices: 0.01 us -> 2.05 us  [local(): lax.ppermute(kv, ('z', 'y'), [(blk, blk % zs * ys + blk // zs) for blk in...]
    ppermute x0 -> x1, starting transfers between devices: none -> 1.91 us  [local(): other_rows = lax.ppermute(own_rows, 'c', [(0, 1), (1, 0)])]
    all_to_all x1, blocking collectives: 10.8 us -> 12.5 us  [local(): lax.all_to_all(part.reshape(ys, rows, 2 * mine), 'y', 0, 0, tiled=True)]
    broadcast_in_dim x0 -> x1, local copies, waits for them, and re-layouts: none -> 1.62 us  [local(): jnp.broadcast_to(output_weight[None], (xs, *output_weight.shape))]
  transfers between devices with their start and end apart: 3 -> 4, of which waited for: 0 -> 1; matrix products, arithmetic and copies ran while one was open for 1% -> 0% of each run, Pallas kernels for 21% -> 14%
where the time goes in v2:
time: 117 us; the launch traced here: 116 us
  blocking collectives  65.8 us (56%)
  Pallas kernels  24.5 us (21%)
  starting transfers between devices  22 us (19%)
  waiting for transfers between devices  2.05 us (2%)
  local copies, waits for them, and re-layouts  1.68 us (1%)
    all_gather x1, blocking collectives, local(): quarter = lax.all_gather(moved, 'z', axis=0, tiled=True)  39.7 us
    pallas_call x1, Pallas kernels, local(): pl.pallas_call(attend_kernel, in_specs=[smem, smem, vmem, vmem], out_spec...  16.3 us
    all_to_all x1, blocking collectives, local(): lax.all_to_all(jnp.broadcast_to(attended[None], (tps, rows, mine)), ('x',...  13.6 us
    all_to_all x1, blocking collectives, local(): lax.all_to_all(part.reshape(ys, rows, 2 * mine), 'y', 0, 0, tiled=True)  12.5 us
    ppermute x1, starting transfers between devices, local(): lax.ppermute(kv, ('z', 'y'), [(blk, blk % zs * ys + blk // zs) for blk in...  11.4 us
    pallas_call x1, Pallas kernels, local(): pl.pallas_call(project_kernel, in_specs=[vmem, vmem, anywhere, anywhere,...  4.73 us
    all_to_all x1, starting transfers between devices, local(): row_q = lax.all_to_all(q_all, 'y', 0, 0, tiled=True)  4.48 us
    all_to_all x1, starting transfers between devices, local(): lax.all_to_all(jnp.broadcast_to(output_weight[None], (xs, *output_weight....  4.29 us
  transfers between devices with their start and end apart: 4, of which 1 were waited for; matrix products, arithmetic and copies ran while one was open for 0% of the time, Pallas kernels for 14%

profile of v2, /device:TPU:96, one launch (start us, length us, event | category | flops | bytes accessed | tf_op | source)
XLA Modules:
  0.0 116.2 jit_solution(11417588776731051735)
XLA Ops:
  0.0 0.0 copy-start
  0.0 4.7 %project.1 = (bf16[4,192,128]{2,1,0:T(8,128)(2,1)}, bf16[192,128]{1,0:T(8,128)(2,1)}) custom-call(bf16[192,2048]{1,0:T(8,128)(2,1)} %hidden_ref.1, f32[1,2048]{1,0:T(1,128)} %bitcast.6, bf16[2048,128]{1,0:T(8,128)(2,1)} %wq_hbm.1, bf16[2048,256]{1,0:T(8,128)(2,1)} %wk_hbm.1, bf16[2048,256]{1,0:T(8,128)(2,1)} %wv_hbm.1), custom_call_target="tpu_custom_call" | custom-call | flops 503316480 | bytes 3407872 | tf_op jit(solution)/shard_map/project/pallas_call | solution.py:140
  4.7 4.5 %all-to-all-start = ((bf16[4,192,128]{2,1,0:T(8,128)(2,1)}), bf16[4,192,128]{2,1,0:T(8,128)(2,1)S(1)}, u32[]{:S(2)}, u32[]{:S(2)}) async-start(bf16[4,192,128]{2,1,0:T(8,128)(2,1)} %get-tuple-element.12), calls=%async_computation | async-start | bytes 393216 | tf_op jit(solution)/shard_map/all_to_all | solution.py:166
  9.2 11.4 %collective-permute-start = (bf16[192,128]{1,0:T(8,128)(2,1)}, bf16[192,128]{1,0:T(8,128)(2,1)S(1)}, u32[]{:S(2)}, u32[]{:S(2)}) collective-permute-start(bf16[192,128]{1,0:T(8,128)(2,1)} %get-tuple-element.13), channel_id=1, source_target_pairs={{0,0},{8,32},{16,64},{24,96},{32,128},{40,160},{48,192},{56,224},{... | collective-permute-start | bytes 147464 | tf_op jit(solution)/shard_map/ppermute | solution.py:163
  20.6 2.0 %collective-permute-done = bf16[192,128]{1,0:T(8,128)(2,1)S(1)} collective-permute-done((bf16[192,128]{1,0:T(8,128)(2,1)}, bf16[192,128]{1,0:T(8,128)(2,1)S(1)}, u32[]{:S(2)}, u32[]{:S(2)}) %collective-permute-start) | collective-permute-done | bytes 49184 | tf_op jit(solution)/shard_map/ppermute | solution.py:163
  22.6 0.0 all-to-all-done.q_ref
  22.6 0.0 copy-done
  22.6 0.0 copy-start.1
  22.6 1.6 %broadcast_in_dim.18 = bf16[4,128,2048]{2,1,0:T(8,128)(2,1)} broadcast(bf16[128,2048]{1,0:T(8,128)(2,1)S(1)} %copy-done), dimensions={1,2} | broadcast | bytes 2621440 | tf_op jit(solution)/shard_map/broadcast_in_dim | solution.py:169
  24.3 0.0 copy-done.1
  24.3 4.3 %all-to-all-start.1 = ((bf16[4,128,2048]{2,1,0:T(8,128)(2,1)}), bf16[4,128,2048]{2,1,0:T(8,128)(2,1)S(1)}, u32[]{:S(2)}, u32[]{:S(2)}) async-start(bf16[4,128,2048]{2,1,0:T(8,128)(2,1)} %broadcast_in_dim.18), calls=%async_computation.1 | async-start | bytes 4194304 | tf_op jit(solution)/shard_map/all_to_all | solution.py:168
  28.6 39.7 %all_gather.3.kv_ref = bf16[3072,128]{1,0:T(8,128)(2,1)} all-gather(bf16[192,128]{1,0:T(8,128)(2,1)S(1)} %collective-permute-done), channel_id=1, replica_groups=mesh['z'=16,'y'=4,'x'=4,'c'=2] {'z'}, dimensions={0}, use_global_device_ids=true | all-gather | bytes 835584 | tf_op jit(solution)/shard_map/all_gather | solution.py:171
  68.3 0.0 all-to-all-done.1.own_ref
  68.3 1.9 %collective-permute-start.1 = (bf16[4,128,2048]{2,1,0:T(8,128)(2,1)S(1)}, bf16[4,128,2048]{2,1,0:T(8,128)(2,1)}, u32[]{:S(2)}, u32[]{:S(2)}) collective-permute-start(bf16[4,128,2048]{2,1,0:T(8,128)(2,1)S(1)} %all-to-all-done.1.own_ref), channel_id=1, source_target_pairs={{0,1},{1,0},{2,3},{3,2},{4,5},{5,4},{6,7},{7,6},{8,9},{9,8},{10,11... | collective-permute-start | bytes 6291464 | tf_op jit(solution)/shard_map/ppermute | solution.py:173
  70.2 16.3 %attend.1 = bf16[768,256]{1,0:T(8,128)(2,1)} custom-call(s32[1]{0:T(128)} %bitcast.rel_ref, f32[2]{0:T(128)} %bias_ref.1, bf16[4,192,128]{2,1,0:T(8,128)(2,1)} %copy-done.1, bf16[3072,128]{1,0:T(8,128)(2,1)} %all_gather.3.kv_ref), custom_call_target="tpu_custom_call" | custom-call | flops 10000000000 | bytes 2000000 | tf_op jit(solution)/shard_map/attend/pallas_call | solution.py:177
  86.5 12.5 %all_to_all.20 = bf16[4,192,256]{2,1,0:T(8,128)(2,1)S(1)} all-to-all(bf16[4,192,256]{2,1,0:T(8,128)(2,1)} %bitcast.5), channel_id=1, replica_groups=mesh['z'=16,'y'=4,'x'=4,'c'=2] {'y'}, dimensions={0} | all-to-all | bytes 786432 | tf_op jit(solution)/shard_map/all_to_all | solution.py:192
  98.9 0.1 convert_element_type.7
  99.0 0.1 broadcast_in_dim.20
  99.1 13.6 %all_to_all.21.heads_ref = bf16[8,192,128]{2,1,0:T(8,128)(2,1)S(1)} all-to-all(bf16[8,192,128]{2,1,0:T(8,128)(2,1)S(1)} %broadcast_in_dim.20), channel_id=1, replica_groups=mesh['z'=16,'y'=4,'x'=4,'c'=2] {'x','c'}, dimensions={0} | all-to-all | bytes 786432 | tf_op jit(solution)/shard_map/all_to_all | solution.py:198
  112.8 0.0 collective-permute-done.1.other_ref
  112.8 3.5 %project_out.1 = bf16[192,2048]{1,0:T(8,128)(2,1)} custom-call(bf16[8,192,128]{2,1,0:T(8,128)(2,1)S(1)} %all_to_all.21.heads_ref, bf16[4,128,2048]{2,1,0:T(8,128)(2,1)S(1)} %all-to-all-done.1.own_ref, bf16[4,128,2048]{2,1,0:T(8,128)(2,1)} %collective-permute-done.1.other_ref), custom_call_target="tpu_custom_call" | custom-call | flops 805306368 | bytes 4194304 | tf_op jit(solution)/shard_map/project_out/pallas_call | solution.py:202
  (1 shorter events, 0.0 us)
Async XLA Ops:
  0.0 22.6 %copy-start = (bf16[128,2048]{1,0:T(8,128)(2,1)S(1)}, bf16[128,2048]{1,0:T(8,128)(2,1)}, u32[]{:S(2)}) copy-start(bf16[128,2048]{1,0:T(8,128)(2,1)} %param.13) | copy-start | bytes 1572868
  4.7 17.9 %all-to-all-start = ((bf16[4,192,128]{2,1,0:T(8,128)(2,1)}), bf16[4,192,128]{2,1,0:T(8,128)(2,1)S(1)}, u32[]{:S(2)}, u32[]{:S(2)}) async-start(bf16[4,192,128]{2,1,0:T(8,128)(2,1)} %get-tuple-element.12), calls=%async_computation | async-start | bytes 393216 | tf_op jit(solution)/shard_map/all_to_all | solution.py:166
  9.2 13.4 %collective-permute-start = (bf16[192,128]{1,0:T(8,128)(2,1)}, bf16[192,128]{1,0:T(8,128)(2,1)S(1)}, u32[]{:S(2)}, u32[]{:S(2)}) collective-permute-start(bf16[192,128]{1,0:T(8,128)(2,1)} %get-tuple-element.13), channel_id=1, source_target_pairs={{0,0},{8,32},{16,64},{24,96},{32,128},{40,160},{48,192},{56,224},{... | collective-permute-start | bytes 147464 | tf_op jit(solution)/shard_map/ppermute | solution.py:163
  22.6 1.6 %copy-start.1 = (bf16[4,192,128]{2,1,0:T(8,128)(2,1)}, bf16[4,192,128]{2,1,0:T(8,128)(2,1)S(1)}, u32[]{:S(2)}) copy-start(bf16[4,192,128]{2,1,0:T(8,128)(2,1)S(1)} %all-to-all-done.q_ref) | copy-start | bytes 589828
  24.3 44.0 %all-to-all-start.1 = ((bf16[4,128,2048]{2,1,0:T(8,128)(2,1)}), bf16[4,128,2048]{2,1,0:T(8,128)(2,1)S(1)}, u32[]{:S(2)}, u32[]{:S(2)}) async-start(bf16[4,128,2048]{2,1,0:T(8,128)(2,1)} %broadcast_in_dim.18), calls=%async_computation.1 | async-start | bytes 4194304 | tf_op jit(solution)/shard_map/all_to_all | solution.py:168
  68.3 44.5 %collective-permute-start.1 = (bf16[4,128,2048]{2,1,0:T(8,128)(2,1)S(1)}, bf16[4,128,2048]{2,1,0:T(8,128)(2,1)}, u32[]{:S(2)}, u32[]{:S(2)}) collective-permute-start(bf16[4,128,2048]{2,1,0:T(8,128)(2,1)S(1)} %all-to-all-done.1.own_ref), channel_id=1, source_target_pairs={{0,1},{1,0},{2,3},{3,2},{4,5},{5,4},{6,7},{7,6},{8,9},{9,8},{10,11... | collective-permute-start | bytes 6291464 | tf_op jit(solution)/shard_map/ppermute | solution.py:173

commit v3 on v2

v3 whole, which is shorter than its diff:
```python
import jax
import jax.numpy as jnp
from jax import lax
from jax.experimental import pallas as pl
from jax.experimental.pallas import tpu as pltpu
from jax.sharding import Mesh
from jax.sharding import PartitionSpec as P

HEAD_DIM = 64
TILE = 256
VMEM = pltpu.VMEM
SMEM = pltpu.SMEM
LIMIT = 56 * 1024 * 1024


def project_kernel(
    hidden_ref, gain_ref, wq_hbm, wk_hbm, wv_hbm, q_ref, kv_ref, wq_ref, wk_ref, wv_ref, sems
):
    copies = [
        pltpu.make_async_copy(src, dst, sems.at[n])
        for n, (src, dst) in enumerate(((wk_hbm, wk_ref), (wv_hbm, wv_ref), (wq_hbm, wq_ref)))
    ]
    for copy in copies:
        copy.start()
    x = lax.axis_index("x")
    wide = hidden_ref[...].astype(jnp.float32)
    inv = lax.rsqrt(jnp.mean(wide * wide, axis=-1, keepdims=True) + 1e-06)
    normed = (wide * inv * gain_ref[...]).astype(jnp.bfloat16)

    def own(full):
        pair = jnp.where(x >= 2, full[:, 2 * HEAD_DIM :], full[:, : 2 * HEAD_DIM])
        return pair, pltpu.roll(pair, HEAD_DIM, 1)

    copies[0].wait()
    k, k_turned = own(jnp.dot(normed, wk_ref[...], preferred_element_type=jnp.float32))
    copies[1].wait()
    v, v_turned = own(jnp.dot(normed, wv_ref[...], preferred_element_type=jnp.float32))
    upper = x % 2 == 1
    lane = lax.broadcasted_iota(jnp.int32, k.shape, 1)
    k_side = jnp.where(upper, k_turned, k)
    v_side = jnp.where(upper, v, v_turned)
    kv = jnp.where(lane < HEAD_DIM, k_side, v_side)
    half = kv_ref.shape[1]
    kv = jnp.where(lax.axis_index("c") == 0, kv[:half], kv[half:]).astype(jnp.bfloat16)
    for dest in range(kv_ref.shape[0]):
        kv_ref[dest] = kv
    copies[2].wait()
    q = jnp.dot(normed, wq_ref[...], preferred_element_type=jnp.float32).astype(jnp.bfloat16)
    q = q * jnp.bfloat16(HEAD_DIM**-0.5)
    q_ref[...] = q


def attend_kernel(bias_ref, q_ref, kv_ref, out_ref, qs, kvs, acc, carry):
    cores, places, half = kv_ref.shape[:3]
    blocks, tok = q_ref.shape[0], q_ref.shape[1]
    mine = 2 * HEAD_DIM
    tokens = blocks * tok
    key_tiles = places * tok // TILE
    a = lax.axis_index("a")
    start = (lax.axis_index("b") * lax.axis_size("y") + lax.axis_index("y")) * tok
    low, high = start // TILE, (start + tok - 1) // TILE
    lane = lax.broadcasted_iota(jnp.int32, (tok, mine), 1)
    for n in range(blocks):
        q = q_ref[n].astype(jnp.float32)
        qs[n * tok : (n + 1) * tok, :] = jnp.where(lane < HEAD_DIM, q, 0.0).astype(jnp.bfloat16)
        turned = jnp.where(lane < HEAD_DIM, pltpu.roll(q, HEAD_DIM, 1), 0.0)
        qs[tokens + n * tok : tokens + (n + 1) * tok, :] = turned.astype(jnp.bfloat16)
    for place in range(places):
        for core in range(cores):
            row = place * tok + core * half
            kvs[row : row + half, :] = kv_ref[core, place]
    acc[...] = jnp.zeros_like(acc)
    carry[...] = jnp.zeros_like(carry)
    from_row = lax.broadcasted_iota(jnp.int32, (TILE, TILE), 0)
    to_col = lax.broadcasted_iota(jnp.int32, (TILE, TILE), 1)
    later = (from_row > to_col).astype(jnp.bfloat16)
    ahead = lax.broadcasted_iota(jnp.int32, (tok, TILE), 1) - lax.broadcasted_iota(
        jnp.int32, (tok, TILE), 0
    )
    shut = jnp.float32(-1e30)

    def step(k, masked):
        kv = kvs[pl.ds(pl.multiple_of(k * TILE, TILE), TILE), :]
        raw = lax.dot_general(
            qs[...], kv, (((1,), (1,)), ((), ())), preferred_element_type=jnp.float32
        )
        groups = []
        for g in range(2 * blocks):
            head, block = divmod(g, blocks)
            closed = (block < a) | ((block == a) & (k > high))
            groups.append(
                raw[g * tok : (g + 1) * tok] + (bias_ref[head] + jnp.where(closed, shut, 0.0))
            )
            if masked:
                limit = jnp.where(block == a, start - k * TILE, 2 * TILE)
                groups[-1] = jnp.where(ahead < limit, groups[-1], shut)
        z = jnp.concatenate(groups, axis=0)
        soft = jnp.maximum(z, jnp.log(1.0 + jnp.exp(jnp.minimum(z, 80.0))))
        gain = z - soft
        between = jnp.dot(soft.astype(jnp.bfloat16), later, preferred_element_type=jnp.float32)
        held = carry[...]
        weight = jnp.exp(gain - between - jnp.concatenate([held, held], axis=1))
        acc[...] += jnp.dot(weight.astype(jnp.bfloat16), kv, preferred_element_type=jnp.float32)
        carry[...] = held + jnp.broadcast_to(between[:, :1] + soft[:, :1], held.shape)

    top = jnp.where(a == blocks - 1, high + 1, key_tiles)

    @pl.loop(0, top)
    def _(n):
        k = top - 1 - n
        edge = (k >= low) & (k <= high)

        @pl.when(edge)
        def _():
            step(k, True)

        @pl.when(jnp.logical_not(edge))
        def _():
            step(k, False)

    mark_row = lax.broadcasted_iota(jnp.int32, (16, mine), 0)
    mark_lane = lax.broadcasted_iota(jnp.int32, (16, mine), 1)
    pick = (mark_row * HEAD_DIM == mark_lane) & (mark_row < 2)
    pick = pick.astype(jnp.bfloat16)
    for n in range(blocks):
        first = slice(n * tok, (n + 1) * tok)
        second = slice(tokens + n * tok, tokens + (n + 1) * tok)
        part = jnp.where(lane < HEAD_DIM, pltpu.roll(acc[first], HEAD_DIM, 1), acc[second])
        decay = jnp.exp(-jnp.where(lane < HEAD_DIM, carry[first], carry[second]))
        out_ref[n, :tok, :] = part.astype(jnp.bfloat16)
        turned = lax.dot_general(
            pick, decay.astype(jnp.bfloat16), (((1,), (1,)), ((), ())), preferred_element_type=jnp.float32
        ).astype(jnp.bfloat16)
        out_ref[n, tok : tok + 16, :] = turned[:, :mine]
        out_ref[n, tok + 16 :, :] = jnp.zeros((16, mine), jnp.bfloat16)
        out_ref[n, tok + 16 :, : tok - mine] = turned[:, mine:]


def combine_kernel(part_ref, out_ref):
    tok, mine = out_ref.shape[1], out_ref.shape[2]
    row = lax.broadcasted_iota(jnp.int32, (16, mine), 0)
    lane = lax.broadcasted_iota(jnp.int32, (16, mine), 1)
    spread = (row == lane // HEAD_DIM).astype(jnp.bfloat16)

    def column(turned):
        return lax.dot_general(
            turned, spread, (((0,), (0,)), ((), ())), preferred_element_type=jnp.float32
        )

    total = part_ref[0, :tok].astype(jnp.float32)
    for n in range(1, part_ref.shape[0]):
        decay = jnp.concatenate(
            [
                column(part_ref[n, tok : tok + 16, :]),
                column(part_ref[n, tok + 16 :, :])[: tok - mine],
            ],
            axis=0,
        )
        total = part_ref[n, :tok].astype(jnp.float32) + decay * total
    attended = total.astype(jnp.bfloat16)
    for dest in range(out_ref.shape[0]):
        out_ref[dest] = attended


def project_out_kernel(heads_ref, own_ref, other_ref, out_ref, joined):
    c = lax.axis_index("c")
    xs, mine = own_ref.shape[0], own_ref.shape[1]
    for side, core in enumerate((c, 1 - c)):
        for x in range(xs):
            col = (side * xs + x) * mine
            joined[:, col : col + mine] = heads_ref[2 * x + core]
    half = xs * mine
    block = 512
    for n in range(out_ref.shape[1] // block):
        cols = slice(n * block, (n + 1) * block)
        total = jnp.dot(
            joined[:, :half], own_ref[:, :, cols].reshape(half, block), preferred_element_type=jnp.float32
        )
        total += jnp.dot(
            joined[:, half:], other_ref[:, :, cols].reshape(half, block), preferred_element_type=jnp.float32
        )
        out_ref[:, cols] = total.astype(jnp.bfloat16)


def local(hidden, norm_gain, query_weight, key_weight, value_weight, head_bias, output_weight):
    rows, width = hidden.shape
    supers, xs = lax.axis_size("a"), lax.axis_size("x")
    places, cores = lax.axis_size("b") * lax.axis_size("y"), lax.axis_size("c")
    tps = xs * cores
    mine = 2 * HEAD_DIM
    vmem = pl.BlockSpec(memory_space=VMEM)
    smem = pl.BlockSpec(memory_space=SMEM)
    anywhere = pl.BlockSpec(memory_space=pl.ANY)

    kv_cols = key_weight.shape[1]
    queries, kv = pl.pallas_call(
        project_kernel,
        in_specs=[vmem, vmem, anywhere, anywhere, anywhere],
        out_specs=[vmem, vmem],
        out_shape=[
            jax.ShapeDtypeStruct((rows, mine), jnp.bfloat16),
            jax.ShapeDtypeStruct((places, rows // cores, mine), jnp.bfloat16),
        ],
        scratch_shapes=[
            VMEM((width, mine), jnp.bfloat16),
            VMEM((width, kv_cols), jnp.bfloat16),
            VMEM((width, kv_cols), jnp.bfloat16),
            pltpu.SemaphoreType.DMA((3,)),
        ],
        compiler_params=pltpu.CompilerParams(vmem_limit_bytes=LIMIT),
        cost_estimate=pl.CostEstimate(
            flops=2 * rows * width * (mine + 2 * kv_cols),
            bytes_accessed=2 * width * (rows + mine + 2 * kv_cols),
            transcendentals=0,
        ),
        name="project",
    )(hidden, norm_gain[None, :], query_weight, key_weight, value_weight)

    kv_half = lax.all_to_all(kv, ("b", "y"), 0, 0, tiled=True)
    kv_half, queries, output_weight = lax.optimization_barrier((kv_half, queries, output_weight))
    own_rows = lax.all_to_all(
        jnp.broadcast_to(output_weight[None], (xs, *output_weight.shape)), "x", 0, 0, tiled=True
    )
    key_value = lax.all_gather(kv_half, "c", axis=0)
    every_q = lax.all_gather(queries, "a", axis=0)
    every_q, key_value, own_rows = lax.optimization_barrier((every_q, key_value, own_rows))
    other_rows = lax.ppermute(own_rows, "c", [(0, 1), (1, 0)])

    tokens = supers * rows
    part = pl.pallas_call(
        attend_kernel,
        in_specs=[smem, vmem, vmem],
        out_specs=vmem,
        out_shape=jax.ShapeDtypeStruct((supers, rows + 32, mine), jnp.bfloat16),
        scratch_shapes=[
            VMEM((2 * tokens, mine), jnp.bfloat16),
            VMEM((places * rows, mine), jnp.bfloat16),
            VMEM((2 * tokens, mine), jnp.float32),
            VMEM((2 * tokens, mine), jnp.float32),
        ],
        compiler_params=pltpu.CompilerParams(vmem_limit_bytes=LIMIT),
        cost_estimate=pl.CostEstimate(flops=10**10, bytes_accessed=2 * 10**6, transcendentals=0),
        name="attend",
    )(head_bias, every_q, key_value)

    parts = lax.all_to_all(part, "a", 0, 0, tiled=True)
    attended = pl.pallas_call(
        combine_kernel,
        in_specs=[vmem],
        out_specs=vmem,
        out_shape=jax.ShapeDtypeStruct((tps, rows, mine), jnp.bfloat16),
        compiler_params=pltpu.CompilerParams(vmem_limit_bytes=16 * 1024 * 1024),
        name="combine",
    )(parts)
    every_head = lax.all_to_all(attended, ("x", "c"), 0, 0, tiled=True)
    cols = output_weight.shape[1]
    return pl.pallas_call(
        project_out_kernel,
        in_specs=[vmem, vmem, vmem],
        out_specs=vmem,
        out_shape=jax.ShapeDtypeStruct((rows, cols), jnp.bfloat16),
        scratch_shapes=[VMEM((rows, tps * mine), jnp.bfloat16)],
        compiler_params=pltpu.CompilerParams(vmem_limit_bytes=20 * 1024 * 1024),
        cost_estimate=pl.CostEstimate(
            flops=2 * rows * tps * mine * cols, bytes_accessed=2 * tps * mine * cols, transcendentals=0
        ),
        name="project_out",
    )(every_head, own_rows, other_rows)


def solution(mesh):
    torus = Mesh(mesh.devices.reshape(4, 4, 4, 4, 2), ("a", "b", "y", "x", "c"))
    sp, tp = ("a", "b", "y"), ("x", "c")
    in_specs = (P(sp, None), P(), P(None, tp), P(), P(), P(tp), P(tp, None))
    return jax.shard_map(
        local, mesh=torus, in_specs=in_specs, out_specs=P(sp, None), check_vma=False
    )
```

time: 117 us -> 121 us (1.034)
  the two profiles are of different devices: /device:TPU:96 before, /device:TPU:32 now
where the time goes in v3:
time: 121 us
  blocking collectives  90 us (74%)
  Pallas kernels  22.8 us (19%)
  starting transfers between devices  6.45 us (5%)
  local copies, waits for them, and re-layouts  1.61 us (1%)
    all_to_all x1, blocking collectives, local(): parts = lax.all_to_all(part, 'a', 0, 0, tiled=True)  31 us
    all_gather x1, blocking collectives, local(): every_q = lax.all_gather(queries, 'a', axis=0)  24.3 us
    all_to_all x1, blocking collectives, local(): kv_half = lax.all_to_all(kv, ('b', 'y'), 0, 0, tiled=True)  20.8 us
    pallas_call x1, Pallas kernels, local(): pl.pallas_call(attend_kernel, in_specs=[smem, vmem, vmem], out_specs=vmem...  16 us
    all_to_all x1, blocking collectives, local(): every_head = lax.all_to_all(attended, ('x', 'c'), 0, 0, tiled=True)  11.5 us
    pallas_call x1, Pallas kernels, local(): pl.pallas_call(project_kernel, in_specs=[vmem, vmem, anywhere, anywhere,...  4.67 us
    all_to_all x1, starting transfers between devices, local(): lax.all_to_all(jnp.broadcast_to(output_weight[None], (xs, *output_weight....  4.41 us
    all_gather x1, blocking collectives, local(): key_value = lax.all_gather(kv_half, 'c', axis=0)  2.49 us
  transfers between devices with their start and end apart: 2, of which 0 were waited for; matrix products, arithmetic and copies ran while one was open for 0% of the time, Pallas kernels for 13%

profile of v3, /device:TPU:32, one launch (start us, length us, event | category | flops | bytes accessed | tf_op | source)
XLA Modules:
  0.0 120.9 jit_solution(4084314794502448908)
XLA Ops:
  0.0 0.0 copy-start
  0.0 4.7 %project.1 = (bf16[192,128]{1,0:T(8,128)(2,1)}, bf16[16,96,128]{2,1,0:T(8,128)(2,1)}) custom-call(bf16[192,2048]{1,0:T(8,128)(2,1)} %hidden_ref.1, f32[1,2048]{1,0:T(1,128)} %bitcast.5, bf16[2048,128]{1,0:T(8,128)(2,1)} %wq_hbm.1, bf16[2048,256]{1,0:T(8,128)(2,1)} %wk_hbm.1, bf16[2048,256]{1,0:T(8,128)(2,1)} %wv_hbm.1), custom_call_target="tpu_custom_call" | custom-call | flops 503316480 | bytes 3407872 | tf_op jit(solution)/shard_map/project/pallas_call | solution.py:196
  4.7 20.8 %all_to_all.20 = bf16[16,96,128]{2,1,0:T(8,128)(2,1)S(1)} all-to-all(bf16[16,96,128]{2,1,0:T(8,128)(2,1)} %get-tuple-element.13), channel_id=1, replica_groups=mesh['a'=4,'b'=4,'y'=4,'x'=4,'c'=2] {'b','y'}, dimensions={0} | all-to-all | bytes 786432 | tf_op jit(solution)/shard_map/all_to_all | solution.py:219
  25.4 0.0 copy-done
  25.5 1.6 %broadcast_in_dim.10 = bf16[4,128,2048]{2,1,0:T(8,128)(2,1)} broadcast(bf16[128,2048]{1,0:T(8,128)(2,1)S(1)} %copy-done), dimensions={1,2} | broadcast | bytes 2621440 | tf_op jit(solution)/shard_map/broadcast_in_dim | solution.py:222
  27.1 0.0 copy-start.1
  27.1 4.4 %all-to-all-start.1 = ((bf16[4,128,2048]{2,1,0:T(8,128)(2,1)}), bf16[4,128,2048]{2,1,0:T(8,128)(2,1)S(1)}, u32[]{:S(2)}, u32[]{:S(2)}) async-start(bf16[4,128,2048]{2,1,0:T(8,128)(2,1)} %broadcast_in_dim.10), calls=%async_computation.1 | async-start | bytes 4194304 | tf_op jit(solution)/shard_map/all_to_all | solution.py:221
  31.5 0.0 copy-done.1
  31.5 24.3 %all-gather = bf16[768,128]{1,0:T(8,128)(2,1)} all-gather(bf16[192,128]{1,0:T(8,128)(2,1)S(1)} %copy-done.1), channel_id=2, replica_groups=mesh['a'=4,'b'=4,'y'=4,'x'=4,'c'=2] {'a'}, dimensions={0}, use_global_device_ids=true | all-gather | bytes 245760 | tf_op jit(solution)/shard_map/all_gather | solution.py:225
  55.8 2.5 %all-gather.1 = bf16[32,96,128]{2,1,0:T(8,128)(2,1)} all-gather(bf16[16,96,128]{2,1,0:T(8,128)(2,1)S(1)} %all_to_all.20), channel_id=3, replica_groups=mesh['a'=4,'b'=4,'y'=4,'x'=4,'c'=2] {'c'}, dimensions={0}, use_global_device_ids=true | all-gather | bytes 1179648 | tf_op jit(solution)/shard_map/all_gather | solution.py:224
  58.2 0.0 all-to-all-done.1.own_ref
  58.3 2.0 %collective-permute-start = (bf16[4,128,2048]{2,1,0:T(8,128)(2,1)S(1)}, bf16[4,128,2048]{2,1,0:T(8,128)(2,1)S(1)}, u32[]{:S(2)}, u32[]{:S(2)}) collective-permute-start(bf16[4,128,2048]{2,1,0:T(8,128)(2,1)S(1)} %all-to-all-done.1.own_ref), channel_id=1, source_target_pairs={{0,1},{1,0},{2,3},{3,2},{4,5},{5,4},{6,7},{7,6},{8,9},{9,8},{10,11... | collective-permute-start | bytes 6291464 | tf_op jit(solution)/shard_map/ppermute | solution.py:227
  60.3 16.0 %attend.1 = bf16[4,224,128]{2,1,0:T(8,128)(2,1)} custom-call(f32[2]{0:T(128)} %bias_ref.1, bf16[4,192,128]{2,1,0:T(8,128)(2,1)} %bitcast.4, bf16[2,16,96,128]{3,2,1,0:T(8,128)(2,1)} %bitcast.3), custom_call_target="tpu_custom_call" | custom-call | flops 10000000000 | bytes 2000000 | tf_op jit(solution)/shard_map/attend/pallas_call | solution.py:230
  76.3 31.0 %all_to_all.21.part_ref = bf16[4,224,128]{2,1,0:T(8,128)(2,1)S(1)} all-to-all(bf16[4,224,128]{2,1,0:T(8,128)(2,1)} %attend.1), channel_id=1, replica_groups=mesh['a'=4,'b'=4,'y'=4,'x'=4,'c'=2] {'a'}, dimensions={0} | all-to-all | bytes 458752 | tf_op jit(solution)/shard_map/all_to_all | solution.py:246
  107.3 0.2 combine.1
  107.5 11.5 %all_to_all.22.heads_ref = bf16[8,192,128]{2,1,0:T(8,128)(2,1)S(1)} all-to-all(bf16[8,192,128]{2,1,0:T(8,128)(2,1)S(1)} %combine.1), channel_id=1, replica_groups=mesh['a'=4,'b'=4,'y'=4,'x'=4,'c'=2] {'x','c'}, dimensions={0} | all-to-all | bytes 786432 | tf_op jit(solution)/shard_map/all_to_all | solution.py:255
  119.0 0.0 collective-permute-done.other_ref
  119.0 1.9 %project_out.1 = bf16[192,2048]{1,0:T(8,128)(2,1)} custom-call(bf16[8,192,128]{2,1,0:T(8,128)(2,1)S(1)} %all_to_all.22.heads_ref, bf16[4,128,2048]{2,1,0:T(8,128)(2,1)S(1)} %all-to-all-done.1.own_ref, bf16[4,128,2048]{2,1,0:T(8,128)(2,1)S(1)} %collective-permute-done.other_ref), custom_call_target="tpu_custom_call" | custom-call | flops 805306368 | bytes 4194304 | tf_op jit(solution)/shard_map/project_out/pallas_call | solution.py:257
Async XLA Ops:
  0.0 25.5 %copy-start = (bf16[128,2048]{1,0:T(8,128)(2,1)S(1)}, bf16[128,2048]{1,0:T(8,128)(2,1)}, u32[]{:S(2)}) copy-start(bf16[128,2048]{1,0:T(8,128)(2,1)} %param.13) | copy-start | bytes 1572868
  27.1 4.4 %copy-start.1 = (bf16[192,128]{1,0:T(8,128)(2,1)S(1)}, bf16[192,128]{1,0:T(8,128)(2,1)}, u32[]{:S(2)}) copy-start(bf16[192,128]{1,0:T(8,128)(2,1)} %get-tuple-element.15) | copy-start | bytes 147460
  27.1 31.2 %all-to-all-start.1 = ((bf16[4,128,2048]{2,1,0:T(8,128)(2,1)}), bf16[4,128,2048]{2,1,0:T(8,128)(2,1)S(1)}, u32[]{:S(2)}, u32[]{:S(2)}) async-start(bf16[4,128,2048]{2,1,0:T(8,128)(2,1)} %broadcast_in_dim.10), calls=%async_computation.1 | async-start | bytes 4194304 | tf_op jit(solution)/shard_map/all_to_all | solution.py:221
  58.3 60.8 %collective-permute-start = (bf16[4,128,2048]{2,1,0:T(8,128)(2,1)S(1)}, bf16[4,128,2048]{2,1,0:T(8,128)(2,1)S(1)}, u32[]{:S(2)}, u32[]{:S(2)}) collective-permute-start(bf16[4,128,2048]{2,1,0:T(8,128)(2,1)S(1)} %all-to-all-done.1.own_ref), channel_id=1, source_target_pairs={{0,1},{1,0},{2,3},{3,2},{4,5},{5,4},{6,7},{7,6},{8,9},{9,8},{10,11... | collective-permute-start | bytes 6291464 | tf_op jit(solution)/shard_map/ppermute | solution.py:227

commit v4 on v3

--- a/solution.py
+++ b/solution.py
@@ -14,7 +14,7 @@
 
 
 def project_kernel(
-    hidden_ref, gain_ref, wq_hbm, wk_hbm, wv_hbm, q_ref, kv_ref, wq_ref, wk_ref, wv_ref, sems
+    hidden_ref, gain_ref, wq_hbm, wk_hbm, wv_hbm, q_ref, kv_ref, wq_ref, wk_ref, wv_ref, normed_ref, sems
 ):
     copies = [
         pltpu.make_async_copy(src, dst, sems.at[n])
@@ -23,9 +23,12 @@
     for copy in copies:
         copy.start()
     x = lax.axis_index("x")
-    wide = hidden_ref[...].astype(jnp.float32)
-    inv = lax.rsqrt(jnp.mean(wide * wide, axis=-1, keepdims=True) + 1e-06)
-    normed = (wide * inv * gain_ref[...]).astype(jnp.bfloat16)
+    piece = 32
+    for row in range(0, hidden_ref.shape[0], piece):
+        wide = hidden_ref[row : row + piece, :].astype(jnp.float32)
+        inv = lax.rsqrt(jnp.mean(wide * wide, axis=-1, keepdims=True) + 1e-06)
+        normed_ref[row : row + piece, :] = (wide * inv * gain_ref[...]).astype(jnp.bfloat16)
+    normed = normed_ref[...]
 
     def own(full):
         pair = jnp.where(x >= 2, full[:, 2 * HEAD_DIM :], full[:, : 2 * HEAD_DIM])
@@ -40,31 +43,29 @@
     k_side = jnp.where(upper, k_turned, k)
     v_side = jnp.where(upper, v, v_turned)
     kv = jnp.where(lane < HEAD_DIM, k_side, v_side)
-    half = kv_ref.shape[1]
+    half = kv_ref.shape[0]
     kv = jnp.where(lax.axis_index("c") == 0, kv[:half], kv[half:]).astype(jnp.bfloat16)
-    for dest in range(kv_ref.shape[0]):
-        kv_ref[dest] = kv
+    kv_ref[...] = kv
     copies[2].wait()
     q = jnp.dot(normed, wq_ref[...], preferred_element_type=jnp.float32).astype(jnp.bfloat16)
     q = q * jnp.bfloat16(HEAD_DIM**-0.5)
-    q_ref[...] = q
+    for dest in range(q_ref.shape[0]):
+        q_ref[dest] = q
 
 
 def attend_kernel(bias_ref, q_ref, kv_ref, out_ref, qs, kvs, acc, carry):
     cores, places, half = kv_ref.shape[:3]
     blocks, tok = q_ref.shape[0], q_ref.shape[1]
     mine = 2 * HEAD_DIM
+    key_tiles = places * tok // TILE
     tokens = blocks * tok
-    key_tiles = places * tok // TILE
-    a = lax.axis_index("a")
-    start = (lax.axis_index("b") * lax.axis_size("y") + lax.axis_index("y")) * tok
-    low, high = start // TILE, (start + tok - 1) // TILE
-    lane = lax.broadcasted_iota(jnp.int32, (tok, mine), 1)
-    for n in range(blocks):
-        q = q_ref[n].astype(jnp.float32)
-        qs[n * tok : (n + 1) * tok, :] = jnp.where(lane < HEAD_DIM, q, 0.0).astype(jnp.bfloat16)
+    row_tiles = tokens // TILE
+    lane = lax.broadcasted_iota(jnp.int32, (tok, 2 * HEAD_DIM), 1)
+    for b in range(blocks):
+        q = q_ref[b].astype(jnp.float32)
+        qs[b * tok : (b + 1) * tok, :] = jnp.where(lane < HEAD_DIM, q, 0.0).astype(jnp.bfloat16)
         turned = jnp.where(lane < HEAD_DIM, pltpu.roll(q, HEAD_DIM, 1), 0.0)
-        qs[tokens + n * tok : tokens + (n + 1) * tok, :] = turned.astype(jnp.bfloat16)
+        qs[tokens + b * tok : tokens + (b + 1) * tok, :] = turned.astype(jnp.bfloat16)
     for place in range(places):
         for core in range(cores):
             row = place * tok + core * half
@@ -74,49 +75,40 @@
     from_row = lax.broadcasted_iota(jnp.int32, (TILE, TILE), 0)
     to_col = lax.broadcasted_iota(jnp.int32, (TILE, TILE), 1)
     later = (from_row > to_col).astype(jnp.bfloat16)
-    ahead = lax.broadcasted_iota(jnp.int32, (tok, TILE), 1) - lax.broadcasted_iota(
-        jnp.int32, (tok, TILE), 0
-    )
-    shut = jnp.float32(-1e30)
+    rel = lax.axis_index("z") * row_tiles - lax.axis_index("y") * key_tiles
 
     def step(k, masked):
         kv = kvs[pl.ds(pl.multiple_of(k * TILE, TILE), TILE), :]
         raw = lax.dot_general(
             qs[...], kv, (((1,), (1,)), ((), ())), preferred_element_type=jnp.float32
         )
-        groups = []
-        for g in range(2 * blocks):
-            head, block = divmod(g, blocks)
-            closed = (block < a) | ((block == a) & (k > high))
-            groups.append(
-                raw[g * tok : (g + 1) * tok] + (bias_ref[head] + jnp.where(closed, shut, 0.0))
-            )
-            if masked:
-                limit = jnp.where(block == a, start - k * TILE, 2 * TILE)
-                groups[-1] = jnp.where(ahead < limit, groups[-1], shut)
-        z = jnp.concatenate(groups, axis=0)
+        z = jnp.concatenate([raw[:tokens] + bias_ref[0], raw[tokens:] + bias_ref[1]], axis=0)
         soft = jnp.maximum(z, jnp.log(1.0 + jnp.exp(jnp.minimum(z, 80.0))))
         gain = z - soft
+        if masked:
+            t = lax.broadcasted_iota(jnp.int32, (tokens, TILE), 0)
+            t = jnp.concatenate([t, t], axis=0)
+            s = lax.broadcasted_iota(jnp.int32, (2 * tokens, TILE), 1) + (k - rel) * TILE
+            soft = jnp.where(s < t, soft, 0.0)
         between = jnp.dot(soft.astype(jnp.bfloat16), later, preferred_element_type=jnp.float32)
         held = carry[...]
         weight = jnp.exp(gain - between - jnp.concatenate([held, held], axis=1))
+        if masked:
+            weight = jnp.where(s < t, weight, 0.0)
         acc[...] += jnp.dot(weight.astype(jnp.bfloat16), kv, preferred_element_type=jnp.float32)
         carry[...] = held + jnp.broadcast_to(between[:, :1] + soft[:, :1], held.shape)
 
-    top = jnp.where(a == blocks - 1, high + 1, key_tiles)
-
-    @pl.loop(0, top)
+    @pl.when((rel >= 0) & (rel < key_tiles))
+    def _():
+        @pl.loop(0, row_tiles)
+        def _(n):
+            step(rel + row_tiles - 1 - n, True)
+
+    whole = jnp.clip(rel, 0, key_tiles)
+
+    @pl.loop(0, whole)
     def _(n):
-        k = top - 1 - n
-        edge = (k >= low) & (k <= high)
-
-        @pl.when(edge)
-        def _():
-            step(k, True)
-
-        @pl.when(jnp.logical_not(edge))
-        def _():
-            step(k, False)
+        step(whole - 1 - n, False)
 
     mark_row = lax.broadcasted_iota(jnp.int32, (16, mine), 0)
     mark_lane = lax.broadcasted_iota(jnp.int32, (16, mine), 1)
@@ -184,8 +176,8 @@
 
 def local(hidden, norm_gain, query_weight, key_weight, value_weight, head_bias, output_weight):
     rows, width = hidden.shape
-    supers, xs = lax.axis_size("a"), lax.axis_size("x")
-    places, cores = lax.axis_size("b") * lax.axis_size("y"), lax.axis_size("c")
+    zs, ys, xs = lax.axis_size("z"), lax.axis_size("y"), lax.axis_size("x")
+    cores = lax.axis_size("c")
     tps = xs * cores
     mine = 2 * HEAD_DIM
     vmem = pl.BlockSpec(memory_space=VMEM)
@@ -198,13 +190,14 @@
         in_specs=[vmem, vmem, anywhere, anywhere, anywhere],
         out_specs=[vmem, vmem],
         out_shape=[
-            jax.ShapeDtypeStruct((rows, mine), jnp.bfloat16),
-            jax.ShapeDtypeStruct((places, rows // cores, mine), jnp.bfloat16),
+            jax.ShapeDtypeStruct((ys, rows, mine), jnp.bfloat16),
+            jax.ShapeDtypeStruct((rows // cores, mine), jnp.bfloat16),
         ],
         scratch_shapes=[
             VMEM((width, mine), jnp.bfloat16),
             VMEM((width, kv_cols), jnp.bfloat16),
             VMEM((width, kv_cols), jnp.bfloat16),
+            VMEM((rows, width), jnp.bfloat16),
             pltpu.SemaphoreType.DMA((3,)),
         ],
         compiler_params=pltpu.CompilerParams(vmem_limit_bytes=LIMIT),
@@ -216,34 +209,37 @@
         name="project",
     )(hidden, norm_gain[None, :], query_weight, key_weight, value_weight)
 
-    kv_half = lax.all_to_all(kv, ("b", "y"), 0, 0, tiled=True)
-    kv_half, queries, output_weight = lax.optimization_barrier((kv_half, queries, output_weight))
+    moved = lax.ppermute(
+        kv, ("z", "y"), [(blk, (blk % zs) * ys + blk // zs) for blk in range(zs * ys)]
+    )
+    row_q = lax.all_to_all(queries, "y", 0, 0, tiled=True)
+    row_q, moved, output_weight = lax.optimization_barrier((row_q, moved, output_weight))
     own_rows = lax.all_to_all(
         jnp.broadcast_to(output_weight[None], (xs, *output_weight.shape)), "x", 0, 0, tiled=True
     )
-    key_value = lax.all_gather(kv_half, "c", axis=0)
-    every_q = lax.all_gather(queries, "a", axis=0)
-    every_q, key_value, own_rows = lax.optimization_barrier((every_q, key_value, own_rows))
+    quarter_half = lax.all_gather(moved, "z", axis=0)
+    quarter = lax.all_gather(quarter_half, "c", axis=0)
+    quarter, own_rows = lax.optimization_barrier((quarter, own_rows))
     other_rows = lax.ppermute(own_rows, "c", [(0, 1), (1, 0)])
 
-    tokens = supers * rows
+    tokens = ys * rows
     part = pl.pallas_call(
         attend_kernel,
         in_specs=[smem, vmem, vmem],
         out_specs=vmem,
-        out_shape=jax.ShapeDtypeStruct((supers, rows + 32, mine), jnp.bfloat16),
+        out_shape=jax.ShapeDtypeStruct((ys, rows + 32, mine), jnp.bfloat16),
         scratch_shapes=[
             VMEM((2 * tokens, mine), jnp.bfloat16),
-            VMEM((places * rows, mine), jnp.bfloat16),
+            VMEM((zs * rows, mine), jnp.bfloat16),
             VMEM((2 * tokens, mine), jnp.float32),
             VMEM((2 * tokens, mine), jnp.float32),
         ],
         compiler_params=pltpu.CompilerParams(vmem_limit_bytes=LIMIT),
         cost_estimate=pl.CostEstimate(flops=10**10, bytes_accessed=2 * 10**6, transcendentals=0),
         name="attend",
-    )(head_bias, every_q, key_value)
-
-    parts = lax.all_to_all(part, "a", 0, 0, tiled=True)
+    )(head_bias, row_q, quarter)
+
+    parts = lax.all_to_all(part, "y", 0, 0, tiled=True)
     attended = pl.pallas_call(
         combine_kernel,
         in_specs=[vmem],
@@ -269,8 +265,8 @@
 
 
 def solution(mesh):
-    torus = Mesh(mesh.devices.reshape(4, 4, 4, 4, 2), ("a", "b", "y", "x", "c"))
-    sp, tp = ("a", "b", "y"), ("x", "c")
+    torus = Mesh(mesh.devices.reshape(16, 4, 4, 2), ("z", "y", "x", "c"))
+    sp, tp = ("z", "y"), ("x", "c")
     in_specs = (P(sp, None), P(), P(None, tp), P(), P(), P(tp), P(tp, None))
     return jax.shard_map(
         local, mesh=torus, in_specs=in_specs, out_specs=P(sp, None), check_vma=False

time: 121 us -> 111 us (0.917)
  the two profiles are of different devices: /device:TPU:32 before, /device:TPU:96 now
where the time goes in v4:
time: 111 us; the launch traced here: 110 us
  blocking collectives  61.7 us (56%)
  Pallas kernels  23.2 us (21%)
  starting transfers between devices  22.2 us (20%)
  waiting for transfers between devices  1.72 us (2%)
  local copies, waits for them, and re-layouts  1.63 us (1%)
    all_gather x1, blocking collectives, local(): quarter_half = lax.all_gather(moved, 'z', axis=0)  35.3 us
    pallas_call x1, Pallas kernels, local(): pl.pallas_call(attend_kernel, in_specs=[smem, vmem, vmem], out_specs=vmem...  16.3 us
    all_to_all x1, blocking collectives, local(): every_head = lax.all_to_all(attended, ('x', 'c'), 0, 0, tiled=True)  13.5 us
    ppermute x1, starting transfers between devices, local(): lax.ppermute(kv, ('z', 'y'), [(blk, blk % zs * ys + blk // zs) for blk in...  11.4 us
    all_to_all x1, blocking collectives, local(): parts = lax.all_to_all(part, 'y', 0, 0, tiled=True)  10.5 us
    pallas_call x1, Pallas kernels, local(): pl.pallas_call(project_kernel, in_specs=[vmem, vmem, anywhere, anywhere,...  4.73 us
    all_to_all x1, starting transfers between devices, local(): row_q = lax.all_to_all(queries, 'y', 0, 0, tiled=True)  4.47 us
    all_to_all x1, starting transfers between devices, local(): lax.all_to_all(jnp.broadcast_to(output_weight[None], (xs, *output_weight....  4.3 us
  transfers between devices with their start and end apart: 4, of which 1 were waited for; matrix products, arithmetic and copies ran while one was open for 0% of the time, Pallas kernels for 15%

profile of v4, /device:TPU:96, one launch (start us, length us, event | category | flops | bytes accessed | tf_op | source)
XLA Modules:
  0.0 110.4 jit_solution(16373200881660706843)
XLA Ops:
  0.0 0.0 copy-start
  0.0 4.7 %project.1 = (bf16[4,192,128]{2,1,0:T(8,128)(2,1)}, bf16[96,128]{1,0:T(8,128)(2,1)}) custom-call(bf16[192,2048]{1,0:T(8,128)(2,1)} %hidden_ref.1, f32[1,2048]{1,0:T(1,128)} %bitcast.5, bf16[2048,128]{1,0:T(8,128)(2,1)} %wq_hbm.1, bf16[2048,256]{1,0:T(8,128)(2,1)} %wk_hbm.1, bf16[2048,256]{1,0:T(8,128)(2,1)} %wv_hbm.1), custom_call_target="tpu_custom_call" | custom-call | flops 503316480 | bytes 3407872 | tf_op jit(solution)/shard_map/project/pallas_call | solution.py:188
  4.7 4.5 %all-to-all-start = ((bf16[4,192,128]{2,1,0:T(8,128)(2,1)}), bf16[4,192,128]{2,1,0:T(8,128)(2,1)S(1)}, u32[]{:S(2)}, u32[]{:S(2)}) async-start(bf16[4,192,128]{2,1,0:T(8,128)(2,1)} %get-tuple-element.12), calls=%async_computation | async-start | bytes 393216 | tf_op jit(solution)/shard_map/all_to_all | solution.py:215
  9.2 11.4 %collective-permute-start = (bf16[96,128]{1,0:T(8,128)(2,1)}, bf16[96,128]{1,0:T(8,128)(2,1)S(1)}, u32[]{:S(2)}, u32[]{:S(2)}) collective-permute-start(bf16[96,128]{1,0:T(8,128)(2,1)} %get-tuple-element.13), channel_id=1, source_target_pairs={{0,0},{8,32},{16,64},{24,96},{32,128},{40,160},{48,192},{56,224},{... | collective-permute-start | bytes 73736 | tf_op jit(solution)/shard_map/ppermute | solution.py:212
  20.6 1.7 %collective-permute-done = bf16[96,128]{1,0:T(8,128)(2,1)S(1)} collective-permute-done((bf16[96,128]{1,0:T(8,128)(2,1)}, bf16[96,128]{1,0:T(8,128)(2,1)S(1)}, u32[]{:S(2)}, u32[]{:S(2)}) %collective-permute-start) | collective-permute-done | bytes 24608 | tf_op jit(solution)/shard_map/ppermute | solution.py:212
  22.3 0.0 all-to-all-done.q_ref
  22.3 0.0 copy-done
  22.3 0.0 copy-start.1
  22.3 1.6 %broadcast_in_dim.10 = bf16[4,128,2048]{2,1,0:T(8,128)(2,1)} broadcast(bf16[128,2048]{1,0:T(8,128)(2,1)S(1)} %copy-done), dimensions={1,2} | broadcast | bytes 2621440 | tf_op jit(solution)/shard_map/broadcast_in_dim | solution.py:218
  23.9 0.0 copy-done.1
  23.9 4.3 %all-to-all-start.1 = ((bf16[4,128,2048]{2,1,0:T(8,128)(2,1)}), bf16[4,128,2048]{2,1,0:T(8,128)(2,1)S(1)}, u32[]{:S(2)}, u32[]{:S(2)}) async-start(bf16[4,128,2048]{2,1,0:T(8,128)(2,1)} %broadcast_in_dim.10), calls=%async_computation.1 | async-start | bytes 4194304 | tf_op jit(solution)/shard_map/all_to_all | solution.py:217
  28.2 35.3 %all-gather = bf16[1536,128]{1,0:T(8,128)(2,1)S(1)} all-gather(bf16[96,128]{1,0:T(8,128)(2,1)S(1)} %collective-permute-done), channel_id=2, replica_groups=mesh['z'=16,'y'=4,'x'=4,'c'=2] {'z'}, dimensions={0}, use_global_device_ids=true | all-gather | bytes 417792 | tf_op jit(solution)/shard_map/all_gather | solution.py:220
  63.5 2.5 %all-gather.1 = bf16[32,96,128]{2,1,0:T(8,128)(2,1)} all-gather(bf16[16,96,128]{2,1,0:T(8,128)(2,1)S(1)} %bitcast.3), channel_id=3, replica_groups=mesh['z'=16,'y'=4,'x'=4,'c'=2] {'c'}, dimensions={0}, use_global_device_ids=true | all-gather | bytes 1179648 | tf_op jit(solution)/shard_map/all_gather | solution.py:221
  66.0 0.0 all-to-all-done.1.own_ref
  66.0 2.0 %collective-permute-start.1 = (bf16[4,128,2048]{2,1,0:T(8,128)(2,1)S(1)}, bf16[4,128,2048]{2,1,0:T(8,128)(2,1)S(1)}, u32[]{:S(2)}, u32[]{:S(2)}) collective-permute-start(bf16[4,128,2048]{2,1,0:T(8,128)(2,1)S(1)} %all-to-all-done.1.own_ref), channel_id=1, source_target_pairs={{0,1},{1,0},{2,3},{3,2},{4,5},{5,4},{6,7},{7,6},{8,9},{9,8},{10,11... | collective-permute-start | bytes 6291464 | tf_op jit(solution)/shard_map/ppermute | solution.py:223
  68.0 16.3 %attend.1 = bf16[4,224,128]{2,1,0:T(8,128)(2,1)} custom-call(f32[2]{0:T(128)} %bias_ref.1, bf16[4,192,128]{2,1,0:T(8,128)(2,1)} %copy-done.1, bf16[2,16,96,128]{3,2,1,0:T(8,128)(2,1)} %bitcast.4), custom_call_target="tpu_custom_call" | custom-call | flops 10000000000 | bytes 2000000 | tf_op jit(solution)/shard_map/attend/pallas_call | solution.py:226
  84.3 10.5 %all_to_all.20.part_ref = bf16[4,224,128]{2,1,0:T(8,128)(2,1)S(1)} all-to-all(bf16[4,224,128]{2,1,0:T(8,128)(2,1)} %attend.1), channel_id=1, replica_groups=mesh['z'=16,'y'=4,'x'=4,'c'=2] {'y'}, dimensions={0} | all-to-all | bytes 458752 | tf_op jit(solution)/shard_map/all_to_all | solution.py:242
  94.8 0.2 combine.1
  95.1 13.5 %all_to_all.21.heads_ref = bf16[8,192,128]{2,1,0:T(8,128)(2,1)S(1)} all-to-all(bf16[8,192,128]{2,1,0:T(8,128)(2,1)S(1)} %combine.1), channel_id=1, replica_groups=mesh['z'=16,'y'=4,'x'=4,'c'=2] {'x','c'}, dimensions={0} | all-to-all | bytes 786432 | tf_op jit(solution)/shard_map/all_to_all | solution.py:251
  108.6 0.0 collective-permute-done.1.other_ref
  108.6 1.9 %project_out.1 = bf16[192,2048]{1,0:T(8,128)(2,1)} custom-call(bf16[8,192,128]{2,1,0:T(8,128)(2,1)S(1)} %all_to_all.21.heads_ref, bf16[4,128,2048]{2,1,0:T(8,128)(2,1)S(1)} %all-to-all-done.1.own_ref, bf16[4,128,2048]{2,1,0:T(8,128)(2,1)S(1)} %collective-permute-done.1.other_ref), custom_call_target="tpu_custom_call" | custom-call | flops 805306368 | bytes 4194304 | tf_op jit(solution)/shard_map/project_out/pallas_call | solution.py:253
Async XLA Ops:
  0.0 22.3 %copy-start = (bf16[128,2048]{1,0:T(8,128)(2,1)S(1)}, bf16[128,2048]{1,0:T(8,128)(2,1)}, u32[]{:S(2)}) copy-start(bf16[128,2048]{1,0:T(8,128)(2,1)} %param.13) | copy-start | bytes 1572868
  4.7 17.6 %all-to-all-start = ((bf16[4,192,128]{2,1,0:T(8,128)(2,1)}), bf16[4,192,128]{2,1,0:T(8,128)(2,1)S(1)}, u32[]{:S(2)}, u32[]{:S(2)}) async-start(bf16[4,192,128]{2,1,0:T(8,128)(2,1)} %get-tuple-element.12), calls=%async_computation | async-start | bytes 393216 | tf_op jit(solution)/shard_map/all_to_all | solution.py:215
  9.2 13.1 %collective-permute-start = (bf16[96,128]{1,0:T(8,128)(2,1)}, bf16[96,128]{1,0:T(8,128)(2,1)S(1)}, u32[]{:S(2)}, u32[]{:S(2)}) collective-permute-start(bf16[96,128]{1,0:T(8,128)(2,1)} %get-tuple-element.13), channel_id=1, source_target_pairs={{0,0},{8,32},{16,64},{24,96},{32,128},{40,160},{48,192},{56,224},{... | collective-permute-start | bytes 73736 | tf_op jit(solution)/shard_map/ppermute | solution.py:212
  22.3 1.6 %copy-start.1 = (bf16[4,192,128]{2,1,0:T(8,128)(2,1)}, bf16[4,192,128]{2,1,0:T(8,128)(2,1)S(1)}, u32[]{:S(2)}) copy-start(bf16[4,192,128]{2,1,0:T(8,128)(2,1)S(1)} %all-to-all-done.q_ref) | copy-start | bytes 589828
  23.9 42.1 %all-to-all-start.1 = ((bf16[4,128,2048]{2,1,0:T(8,128)(2,1)}), bf16[4,128,2048]{2,1,0:T(8,128)(2,1)S(1)}, u32[]{:S(2)}, u32[]{:S(2)}) async-start(bf16[4,128,2048]{2,1,0:T(8,128)(2,1)} %broadcast_in_dim.10), calls=%async_computation.1 | async-start | bytes 4194304 | tf_op jit(solution)/shard_map/all_to_all | solution.py:217
  66.0 42.6 %collective-permute-start.1 = (bf16[4,128,2048]{2,1,0:T(8,128)(2,1)S(1)}, bf16[4,128,2048]{2,1,0:T(8,128)(2,1)S(1)}, u32[]{:S(2)}, u32[]{:S(2)}) collective-permute-start(bf16[4,128,2048]{2,1,0:T(8,128)(2,1)S(1)} %all-to-all-done.1.own_ref), channel_id=1, source_target_pairs={{0,1},{1,0},{2,3},{3,2},{4,5},{5,4},{6,7},{7,6},{8,9},{9,8},{10,11... | collective-permute-start | bytes 6291464 | tf_op jit(solution)/shard_map/ppermute | solution.py:223

commit v5 on v4

--- a/solution.py
+++ b/solution.py
@@ -6,6 +6,7 @@
 from jax.sharding import Mesh
 from jax.sharding import PartitionSpec as P
 
+
 HEAD_DIM = 64
 TILE = 256
 VMEM = pltpu.VMEM
@@ -13,42 +14,73 @@
 LIMIT = 56 * 1024 * 1024
 
 
+PIECES = 4
+ROWS_AT_ONCE = 32
+NEAR = ((-6, -5, -3, -4), (-2, -1, 1, 0), (5, 4, 2, 3), (9, 8, 6, 7))
+
+
 def project_kernel(
-    hidden_ref, gain_ref, wq_hbm, wk_hbm, wv_hbm, q_ref, kv_ref, wq_ref, wk_ref, wv_ref, normed_ref, sems
+    hidden_hbm, gain_ref, wq_hbm, wk_hbm, wv_hbm, q_ref, kv_ref, hidden_ref, wq_ref, wkv_ref, normed_ref, sems
 ):
-    copies = [
-        pltpu.make_async_copy(src, dst, sems.at[n])
-        for n, (src, dst) in enumerate(((wk_hbm, wk_ref), (wv_hbm, wv_ref), (wq_hbm, wq_ref)))
-    ]
+    rows, width = hidden_ref.shape
+    mine = 2 * HEAD_DIM
+    depth = width // PIECES
+    x = lax.axis_index("x")
+    cols = pl.ds(pl.multiple_of((x // 2) * mine, mine), mine)
+    pieces = rows // ROWS_AT_ONCE
+    copies = []
+    for n in range(pieces):
+        part = slice(n * ROWS_AT_ONCE, (n + 1) * ROWS_AT_ONCE)
+        copies.append(
+            pltpu.make_async_copy(hidden_hbm.at[part, :], hidden_ref.at[part, :], sems.at[n])
+        )
+    for n in range(PIECES):
+        part = slice(n * depth, (n + 1) * depth)
+        for side, src in enumerate((wk_hbm, wv_hbm)):
+            copies.append(
+                pltpu.make_async_copy(
+                    src.at[part, cols],
+                    wkv_ref.at[part, side * mine : (side + 1) * mine],
+                    sems.at[pieces + 2 * n + side],
+                )
+            )
+    for n in range(PIECES):
+        part = slice(n * depth, (n + 1) * depth)
+        copies.append(
+            pltpu.make_async_copy(
+                wq_hbm.at[part, :], wq_ref.at[part, :], sems.at[pieces + 2 * PIECES + n]
+            )
+        )
     for copy in copies:
         copy.start()
-    x = lax.axis_index("x")
-    piece = 32
-    for row in range(0, hidden_ref.shape[0], piece):
-        wide = hidden_ref[row : row + piece, :].astype(jnp.float32)
+    for n in range(pieces):
+        part = slice(n * ROWS_AT_ONCE, (n + 1) * ROWS_AT_ONCE)
+        copies[n].wait()
+        wide = hidden_ref[part, :].astype(jnp.float32)
         inv = lax.rsqrt(jnp.mean(wide * wide, axis=-1, keepdims=True) + 1e-06)
-        normed_ref[row : row + piece, :] = (wide * inv * gain_ref[...]).astype(jnp.bfloat16)
-    normed = normed_ref[...]
-
-    def own(full):
-        pair = jnp.where(x >= 2, full[:, 2 * HEAD_DIM :], full[:, : 2 * HEAD_DIM])
-        return pair, pltpu.roll(pair, HEAD_DIM, 1)
-
-    copies[0].wait()
-    k, k_turned = own(jnp.dot(normed, wk_ref[...], preferred_element_type=jnp.float32))
-    copies[1].wait()
-    v, v_turned = own(jnp.dot(normed, wv_ref[...], preferred_element_type=jnp.float32))
+        normed_ref[part, :] = (wide * inv * gain_ref[...]).astype(jnp.bfloat16)
+
+    both = jnp.zeros((rows, 2 * mine), jnp.float32)
+    for n in range(PIECES):
+        part = slice(n * depth, (n + 1) * depth)
+        copies[pieces + 2 * n].wait()
+        copies[pieces + 2 * n + 1].wait()
+        both += jnp.dot(normed_ref[:, part], wkv_ref[part, :], preferred_element_type=jnp.float32)
+    k, v = both[:, :mine], both[:, mine:]
     upper = x % 2 == 1
     lane = lax.broadcasted_iota(jnp.int32, k.shape, 1)
-    k_side = jnp.where(upper, k_turned, k)
-    v_side = jnp.where(upper, v, v_turned)
+    k_side = jnp.where(upper, pltpu.roll(k, HEAD_DIM, 1), k)
+    v_side = jnp.where(upper, v, pltpu.roll(v, HEAD_DIM, 1))
     kv = jnp.where(lane < HEAD_DIM, k_side, v_side)
     half = kv_ref.shape[0]
-    kv = jnp.where(lax.axis_index("c") == 0, kv[:half], kv[half:]).astype(jnp.bfloat16)
-    kv_ref[...] = kv
-    copies[2].wait()
-    q = jnp.dot(normed, wq_ref[...], preferred_element_type=jnp.float32).astype(jnp.bfloat16)
-    q = q * jnp.bfloat16(HEAD_DIM**-0.5)
+    kv_ref[...] = jnp.where(lax.axis_index("c") == 0, kv[:half], kv[half:]).astype(jnp.bfloat16)
+
+    q = jnp.zeros((rows, mine), jnp.float32)
+    for n in range(PIECES):
+        part = slice(n * depth, (n + 1) * depth)
+        copies[pieces + 2 * PIECES + n].wait()
+        q += jnp.dot(normed_ref[:, part], wq_ref[part, :], preferred_element_type=jnp.float32)
+    q = q.astype(jnp.bfloat16) * jnp.bfloat16(HEAD_DIM**-0.5)
     for dest in range(q_ref.shape[0]):
         q_ref[dest] = q
 
@@ -66,16 +98,21 @@
         qs[b * tok : (b + 1) * tok, :] = jnp.where(lane < HEAD_DIM, q, 0.0).astype(jnp.bfloat16)
         turned = jnp.where(lane < HEAD_DIM, pltpu.roll(q, HEAD_DIM, 1), 0.0)
         qs[tokens + b * tok : tokens + (b + 1) * tok, :] = turned.astype(jnp.bfloat16)
-    for place in range(places):
-        for core in range(cores):
-            row = place * tok + core * half
-            kvs[row : row + half, :] = kv_ref[core, place]
+    own = lax.axis_index("y")
+    span = len(NEAR)
+    for row in range(span):
+        for turn in range(span):
+            source = lax.rem(span * own + NEAR[row][turn] + places, places)
+            place = row * span + lax.rem(own + turn, span)
+            for core in range(cores):
+                at = pl.multiple_of(place * tok + core * half, 32)
+                kvs[pl.ds(at, half), :] = kv_ref[core, source]
     acc[...] = jnp.zeros_like(acc)
     carry[...] = jnp.zeros_like(carry)
     from_row = lax.broadcasted_iota(jnp.int32, (TILE, TILE), 0)
     to_col = lax.broadcasted_iota(jnp.int32, (TILE, TILE), 1)
     later = (from_row > to_col).astype(jnp.bfloat16)
-    rel = lax.axis_index("z") * row_tiles - lax.axis_index("y") * key_tiles
+    rel = lax.axis_index("z") * row_tiles - own * key_tiles
 
     def step(k, masked):
         kv = kvs[pl.ds(pl.multiple_of(k * TILE, TILE), TILE), :]
@@ -184,39 +221,41 @@
     smem = pl.BlockSpec(memory_space=SMEM)
     anywhere = pl.BlockSpec(memory_space=pl.ANY)
 
-    kv_cols = key_weight.shape[1]
     queries, kv = pl.pallas_call(
         project_kernel,
-        in_specs=[vmem, vmem, anywhere, anywhere, anywhere],
+        in_specs=[anywhere, vmem, anywhere, anywhere, anywhere],
         out_specs=[vmem, vmem],
         out_shape=[
             jax.ShapeDtypeStruct((ys, rows, mine), jnp.bfloat16),
             jax.ShapeDtypeStruct((rows // cores, mine), jnp.bfloat16),
         ],
         scratch_shapes=[
+            VMEM((rows, width), jnp.bfloat16),
             VMEM((width, mine), jnp.bfloat16),
-            VMEM((width, kv_cols), jnp.bfloat16),
-            VMEM((width, kv_cols), jnp.bfloat16),
+            VMEM((width, 2 * mine), jnp.bfloat16),
             VMEM((rows, width), jnp.bfloat16),
-            pltpu.SemaphoreType.DMA((3,)),
+            pltpu.SemaphoreType.DMA((rows // ROWS_AT_ONCE + 3 * PIECES,)),
         ],
         compiler_params=pltpu.CompilerParams(vmem_limit_bytes=LIMIT),
         cost_estimate=pl.CostEstimate(
-            flops=2 * rows * width * (mine + 2 * kv_cols),
-            bytes_accessed=2 * width * (rows + mine + 2 * kv_cols),
+            flops=2 * rows * width * 3 * mine,
+            bytes_accessed=2 * width * (rows + 3 * mine),
             transcendentals=0,
         ),
         name="project",
     )(hidden, norm_gain[None, :], query_weight, key_weight, value_weight)
 
-    moved = lax.ppermute(
-        kv, ("z", "y"), [(blk, (blk % zs) * ys + blk // zs) for blk in range(zs * ys)]
-    )
+    pairs = []
+    for z in range(zs):
+        for y in range(ys):
+            super_row, row = divmod(z, ys)
+            near = (ys * super_row + NEAR[row][(y - super_row) % ys]) % zs
+            pairs.append((z * ys + y, near * ys + super_row))
+    moved = lax.ppermute(kv, ("z", "y"), pairs)
     row_q = lax.all_to_all(queries, "y", 0, 0, tiled=True)
-    row_q, moved, output_weight = lax.optimization_barrier((row_q, moved, output_weight))
-    own_rows = lax.all_to_all(
-        jnp.broadcast_to(output_weight[None], (xs, *output_weight.shape)), "x", 0, 0, tiled=True
-    )
+    fan = jnp.broadcast_to(output_weight[None], (xs, *output_weight.shape))
+    row_q, moved, fan = lax.optimization_barrier((row_q, moved, fan))
+    own_rows = lax.all_to_all(fan, "x", 0, 0, tiled=True)
     quarter_half = lax.all_gather(moved, "z", axis=0)
     quarter = lax.all_gather(quarter_half, "c", axis=0)
     quarter, own_rows = lax.optimization_barrier((quarter, own_rows))

time: 111 us -> 108 us (0.973)
  blocking collectives: 61.7 us -> 58 us
    all_gather x1, blocking collectives: 35.3 us -> 31.3 us  [local(): quarter_half = lax.all_gather(moved, 'z', axis=0)]
where the time goes in v5:
time: 108 us
  blocking collectives  58 us (54%)
  Pallas kernels  23.2 us (21%)
  starting transfers between devices  22.9 us (21%)
  waiting for transfers between devices  1.72 us (2%)
  local copies, waits for them, and re-layouts  1.63 us (2%)
    all_gather x1, blocking collectives, local(): quarter_half = lax.all_gather(moved, 'z', axis=0)  31.3 us
    pallas_call x1, Pallas kernels, local(): pl.pallas_call(attend_kernel, in_specs=[smem, vmem, vmem], out_specs=vmem...  16.3 us
    all_to_all x1, blocking collectives, local(): every_head = lax.all_to_all(attended, ('x', 'c'), 0, 0, tiled=True)  13.7 us
    ppermute x1, starting transfers between devices, local(): moved = lax.ppermute(kv, ('z', 'y'), pairs)  12.1 us
    all_to_all x1, blocking collectives, local(): parts = lax.all_to_all(part, 'y', 0, 0, tiled=True)  10.5 us
    pallas_call x1, Pallas kernels, local(): pl.pallas_call(project_kernel, in_specs=[anywhere, vmem, anywhere, anywhe...  4.82 us
    all_to_all x1, starting transfers between devices, local(): row_q = lax.all_to_all(queries, 'y', 0, 0, tiled=True)  4.47 us
    all_to_all x1, starting transfers between devices, local(): own_rows = lax.all_to_all(fan, 'x', 0, 0, tiled=True)  4.29 us
  transfers between devices with their start and end apart: 4, of which 1 were waited for; matrix products, arithmetic and copies ran while one was open for 0% of the time, Pallas kernels for 15%

profile of v5, /device:TPU:96, one launch (start us, length us, event | category | flops | bytes accessed | tf_op | source)
XLA Modules:
  0.0 107.6 jit_solution(6877523610344605496)
XLA Ops:
  0.0 0.0 copy-start
  0.0 4.8 %project.1 = (bf16[4,192,128]{2,1,0:T(8,128)(2,1)}, bf16[96,128]{1,0:T(8,128)(2,1)}) custom-call(bf16[192,2048]{1,0:T(8,128)(2,1)} %hidden_hbm.1, f32[1,2048]{1,0:T(1,128)} %bitcast.5, bf16[2048,128]{1,0:T(8,128)(2,1)} %wq_hbm.1, bf16[2048,256]{1,0:T(8,128)(2,1)} %wk_hbm.1, bf16[2048,256]{1,0:T(8,128)(2,1)} %wv_hbm.1), custom_call_target="tpu_custom_call" | custom-call | flops 301989888 | bytes 2359296 | tf_op jit(solution)/shard_map/project/pallas_call | solution.py:224
  4.8 4.5 %all-to-all-start = ((bf16[4,192,128]{2,1,0:T(8,128)(2,1)}), bf16[4,192,128]{2,1,0:T(8,128)(2,1)S(1)}, u32[]{:S(2)}, u32[]{:S(2)}) async-start(bf16[4,192,128]{2,1,0:T(8,128)(2,1)} %get-tuple-element.12), calls=%async_computation | async-start | bytes 393216 | tf_op jit(solution)/shard_map/all_to_all | solution.py:255
  9.3 12.1 %collective-permute-start = (bf16[96,128]{1,0:T(8,128)(2,1)}, bf16[96,128]{1,0:T(8,128)(2,1)S(1)}, u32[]{:S(2)}, u32[]{:S(2)}) collective-permute-start(bf16[96,128]{1,0:T(8,128)(2,1)} %get-tuple-element.13), channel_id=1, source_target_pairs={{0,320},{8,352},{16,416},{24,384},{32,448},{40,480},{48,32},{56,0}... | collective-permute-start | bytes 73736 | tf_op jit(solution)/shard_map/ppermute | solution.py:254
  21.4 1.7 %collective-permute-done = bf16[96,128]{1,0:T(8,128)(2,1)S(1)} collective-permute-done((bf16[96,128]{1,0:T(8,128)(2,1)}, bf16[96,128]{1,0:T(8,128)(2,1)S(1)}, u32[]{:S(2)}, u32[]{:S(2)}) %collective-permute-start) | collective-permute-done | bytes 24608 | tf_op jit(solution)/shard_map/ppermute | solution.py:254
  23.1 0.0 all-to-all-done.q_ref
  23.1 0.0 copy-done
  23.1 0.0 copy-start.1
  23.1 1.6 %broadcast_in_dim.10 = bf16[4,128,2048]{2,1,0:T(8,128)(2,1)} broadcast(bf16[128,2048]{1,0:T(8,128)(2,1)S(1)} %copy-done), dimensions={1,2} | broadcast | bytes 2621440 | tf_op jit(solution)/shard_map/broadcast_in_dim | solution.py:256
  24.8 0.0 copy-done.1
  24.8 4.3 %all-to-all-start.1 = ((bf16[4,128,2048]{2,1,0:T(8,128)(2,1)}), bf16[4,128,2048]{2,1,0:T(8,128)(2,1)S(1)}, u32[]{:S(2)}, u32[]{:S(2)}) async-start(bf16[4,128,2048]{2,1,0:T(8,128)(2,1)} %broadcast_in_dim.10), calls=%async_computation.1 | async-start | bytes 4194304 | tf_op jit(solution)/shard_map/all_to_all | solution.py:258
  29.1 31.3 %all-gather = bf16[1536,128]{1,0:T(8,128)(2,1)S(1)} all-gather(bf16[96,128]{1,0:T(8,128)(2,1)S(1)} %collective-permute-done), channel_id=2, replica_groups=mesh['z'=16,'y'=4,'x'=4,'c'=2] {'z'}, dimensions={0}, use_global_device_ids=true | all-gather | bytes 417792 | tf_op jit(solution)/shard_map/all_gather | solution.py:259
  60.4 2.5 %all-gather.1 = bf16[32,96,128]{2,1,0:T(8,128)(2,1)} all-gather(bf16[16,96,128]{2,1,0:T(8,128)(2,1)S(1)} %bitcast.3), channel_id=3, replica_groups=mesh['z'=16,'y'=4,'x'=4,'c'=2] {'c'}, dimensions={0}, use_global_device_ids=true | all-gather | bytes 1179648 | tf_op jit(solution)/shard_map/all_gather | solution.py:260
  62.9 0.0 all-to-all-done.1.own_ref
  62.9 2.0 %collective-permute-start.1 = (bf16[4,128,2048]{2,1,0:T(8,128)(2,1)S(1)}, bf16[4,128,2048]{2,1,0:T(8,128)(2,1)S(1)}, u32[]{:S(2)}, u32[]{:S(2)}) collective-permute-start(bf16[4,128,2048]{2,1,0:T(8,128)(2,1)S(1)} %all-to-all-done.1.own_ref), channel_id=1, source_target_pairs={{0,1},{1,0},{2,3},{3,2},{4,5},{5,4},{6,7},{7,6},{8,9},{9,8},{10,11... | collective-permute-start | bytes 6291464 | tf_op jit(solution)/shard_map/ppermute | solution.py:262
  64.9 16.3 %attend.1 = bf16[4,224,128]{2,1,0:T(8,128)(2,1)} custom-call(f32[2]{0:T(128)} %bias_ref.1, bf16[4,192,128]{2,1,0:T(8,128)(2,1)} %copy-done.1, bf16[2,16,96,128]{3,2,1,0:T(8,128)(2,1)} %bitcast.4), custom_call_target="tpu_custom_call" | custom-call | flops 10000000000 | bytes 2000000 | tf_op jit(solution)/shard_map/attend/pallas_call | solution.py:265
  81.2 10.5 %all_to_all.20.part_ref = bf16[4,224,128]{2,1,0:T(8,128)(2,1)S(1)} all-to-all(bf16[4,224,128]{2,1,0:T(8,128)(2,1)} %attend.1), channel_id=1, replica_groups=mesh['z'=16,'y'=4,'x'=4,'c'=2] {'y'}, dimensions={0} | all-to-all | bytes 458752 | tf_op jit(solution)/shard_map/all_to_all | solution.py:281
  91.7 0.2 combine.1
  92.0 13.7 %all_to_all.21.heads_ref = bf16[8,192,128]{2,1,0:T(8,128)(2,1)S(1)} all-to-all(bf16[8,192,128]{2,1,0:T(8,128)(2,1)S(1)} %combine.1), channel_id=1, replica_groups=mesh['z'=16,'y'=4,'x'=4,'c'=2] {'x','c'}, dimensions={0} | all-to-all | bytes 786432 | tf_op jit(solution)/shard_map/all_to_all | solution.py:290
  105.7 0.0 collective-permute-done.1.other_ref
  105.7 1.9 %project_out.1 = bf16[192,2048]{1,0:T(8,128)(2,1)} custom-call(bf16[8,192,128]{2,1,0:T(8,128)(2,1)S(1)} %all_to_all.21.heads_ref, bf16[4,128,2048]{2,1,0:T(8,128)(2,1)S(1)} %all-to-all-done.1.own_ref, bf16[4,128,2048]{2,1,0:T(8,128)(2,1)S(1)} %collective-permute-done.1.other_ref), custom_call_target="tpu_custom_call" | custom-call | flops 805306368 | bytes 4194304 | tf_op jit(solution)/shard_map/project_out/pallas_call | solution.py:292
Async XLA Ops:
  0.0 23.1 %copy-start = (bf16[128,2048]{1,0:T(8,128)(2,1)S(1)}, bf16[128,2048]{1,0:T(8,128)(2,1)}, u32[]{:S(2)}) copy-start(bf16[128,2048]{1,0:T(8,128)(2,1)} %param.13) | copy-start | bytes 1572868
  4.8 18.3 %all-to-all-start = ((bf16[4,192,128]{2,1,0:T(8,128)(2,1)}), bf16[4,192,128]{2,1,0:T(8,128)(2,1)S(1)}, u32[]{:S(2)}, u32[]{:S(2)}) async-start(bf16[4,192,128]{2,1,0:T(8,128)(2,1)} %get-tuple-element.12), calls=%async_computation | async-start | bytes 393216 | tf_op jit(solution)/shard_map/all_to_all | solution.py:255
  9.3 13.8 %collective-permute-start = (bf16[96,128]{1,0:T(8,128)(2,1)}, bf16[96,128]{1,0:T(8,128)(2,1)S(1)}, u32[]{:S(2)}, u32[]{:S(2)}) collective-permute-start(bf16[96,128]{1,0:T(8,128)(2,1)} %get-tuple-element.13), channel_id=1, source_target_pairs={{0,320},{8,352},{16,416},{24,384},{32,448},{40,480},{48,32},{56,0}... | collective-permute-start | bytes 73736 | tf_op jit(solution)/shard_map/ppermute | solution.py:254
  23.1 1.6 %copy-start.1 = (bf16[4,192,128]{2,1,0:T(8,128)(2,1)}, bf16[4,192,128]{2,1,0:T(8,128)(2,1)S(1)}, u32[]{:S(2)}) copy-start(bf16[4,192,128]{2,1,0:T(8,128)(2,1)S(1)} %all-to-all-done.q_ref) | copy-start | bytes 589828
  24.8 38.1 %all-to-all-start.1 = ((bf16[4,128,2048]{2,1,0:T(8,128)(2,1)}), bf16[4,128,2048]{2,1,0:T(8,128)(2,1)S(1)}, u32[]{:S(2)}, u32[]{:S(2)}) async-start(bf16[4,128,2048]{2,1,0:T(8,128)(2,1)} %broadcast_in_dim.10), calls=%async_computation.1 | async-start | bytes 4194304 | tf_op jit(solution)/shard_map/all_to_all | solution.py:258
  62.9 42.8 %collective-permute-start.1 = (bf16[4,128,2048]{2,1,0:T(8,128)(2,1)S(1)}, bf16[4,128,2048]{2,1,0:T(8,128)(2,1)S(1)}, u32[]{:S(2)}, u32[]{:S(2)}) collective-permute-start(bf16[4,128,2048]{2,1,0:T(8,128)(2,1)S(1)} %all-to-all-done.1.own_ref), channel_id=1, source_target_pairs={{0,1},{1,0},{2,3},{3,2},{4,5},{5,4},{6,7},{7,6},{8,9},{9,8},{10,11... | collective-permute-start | bytes 6291464 | tf_op jit(solution)/shard_map/ppermute | solution.py:262

commit v6 on v5

--- a/solution.py
+++ b/solution.py
@@ -1,3 +1,5 @@
+import math
+
 import jax
 import jax.numpy as jnp
 from jax import lax
@@ -12,6 +14,7 @@
 VMEM = pltpu.VMEM
 SMEM = pltpu.SMEM
 LIMIT = 56 * 1024 * 1024
+HELD = 64 * math.log(2.0)
 
 
 PIECES = 4
@@ -20,7 +23,7 @@
 
 
 def project_kernel(
-    hidden_hbm, gain_ref, wq_hbm, wk_hbm, wv_hbm, q_ref, kv_ref, hidden_ref, wq_ref, wkv_ref, normed_ref, sems
+    hidden_hbm, gain_ref, wq_hbm, wk_hbm, wv_hbm, q_ref, kv_ref, hidden_ref, wq_ref, wkv_ref, normed_ref, turn_ref, sems
 ):
     rows, width = hidden_ref.shape
     mine = 2 * HEAD_DIM
@@ -72,8 +75,13 @@
     k_side = jnp.where(upper, pltpu.roll(k, HEAD_DIM, 1), k)
     v_side = jnp.where(upper, v, pltpu.roll(v, HEAD_DIM, 1))
     kv = jnp.where(lane < HEAD_DIM, k_side, v_side)
-    half = kv_ref.shape[0]
-    kv_ref[...] = jnp.where(lax.axis_index("c") == 0, kv[:half], kv[half:]).astype(jnp.bfloat16)
+    turn_ref[...] = kv
+    few = kv_ref.shape[0] // 2
+    for odd in range(2):
+        first = turn_ref[pl.ds(odd, few, stride=2), :]
+        second = turn_ref[pl.ds(2 * few + odd, few, stride=2), :]
+        part = slice(odd * few, (odd + 1) * few)
+        kv_ref[part, :] = jnp.where(lax.axis_index("c") == 0, first, second).astype(jnp.bfloat16)
 
     q = jnp.zeros((rows, mine), jnp.float32)
     for n in range(PIECES):
@@ -85,14 +93,15 @@
         q_ref[dest] = q
 
 
-def attend_kernel(bias_ref, q_ref, kv_ref, out_ref, qs, kvs, acc, carry):
+def attend_kernel(bias_ref, q_ref, kv_ref, out_ref, qs, evens, odds, acc, carry):
     cores, places, half = kv_ref.shape[:3]
     blocks, tok = q_ref.shape[0], q_ref.shape[1]
     mine = 2 * HEAD_DIM
+    few, wide = half // 2, TILE // 2
     key_tiles = places * tok // TILE
     tokens = blocks * tok
     row_tiles = tokens // TILE
-    lane = lax.broadcasted_iota(jnp.int32, (tok, 2 * HEAD_DIM), 1)
+    lane = lax.broadcasted_iota(jnp.int32, (tok, mine), 1)
     for b in range(blocks):
         q = q_ref[b].astype(jnp.float32)
         qs[b * tok : (b + 1) * tok, :] = jnp.where(lane < HEAD_DIM, q, 0.0).astype(jnp.bfloat16)
@@ -105,34 +114,76 @@
             source = lax.rem(span * own + NEAR[row][turn] + places, places)
             place = row * span + lax.rem(own + turn, span)
             for core in range(cores):
-                at = pl.multiple_of(place * tok + core * half, 32)
-                kvs[pl.ds(at, half), :] = kv_ref[core, source]
+                at = pl.multiple_of(place * (tok // 2) + core * few, 16)
+                evens[pl.ds(at, few), :] = kv_ref[core, source, :few, :]
+                odds[pl.ds(at, few), :] = kv_ref[core, source, few:, :]
     acc[...] = jnp.zeros_like(acc)
-    carry[...] = jnp.zeros_like(carry)
+    carry[...] = jnp.full(carry.shape, -HELD, jnp.float32)
     from_row = lax.broadcasted_iota(jnp.int32, (TILE, TILE), 0)
     to_col = lax.broadcasted_iota(jnp.int32, (TILE, TILE), 1)
-    later = (from_row > to_col).astype(jnp.bfloat16)
+    in_half = (from_row < wide) == (to_col < wide)
+    later_pair = ((from_row > to_col) & in_half).astype(jnp.bfloat16)
+
+    def order(lanes):
+        return jnp.where(lanes < wide, 2 * lanes, 2 * (lanes - wide) + 1)
+
+    later = (order(from_row) > order(to_col)).astype(jnp.bfloat16)
     rel = lax.axis_index("z") * row_tiles - own * key_tiles
 
-    def step(k, masked):
-        kv = kvs[pl.ds(pl.multiple_of(k * TILE, TILE), TILE), :]
+    keep_row = lax.broadcasted_iota(jnp.int32, (mine, mine), 0)
+    keys_only = (keep_row < HEAD_DIM).astype(jnp.bfloat16)
+
+    def largest(rows):
+        square = rows.astype(jnp.float32)
+        square = (square * square).astype(jnp.bfloat16)
+        return jnp.max(jnp.dot(square, keys_only, preferred_element_type=jnp.float32))
+
+    key_norm = jnp.maximum(largest(evens[...]), largest(odds[...]))
+    room = 20.0 - jnp.maximum(bias_ref[0], bias_ref[1])
+    tame = (room > 0.0) & (largest(qs[...]) * key_norm * 1.03 <= room * room)
+
+    def tile(k):
+        at = pl.ds(pl.multiple_of(k * wide, wide), wide)
+        kv = jnp.concatenate([evens[at, :], odds[at, :]], axis=0)
         raw = lax.dot_general(
             qs[...], kv, (((1,), (1,)), ((), ())), preferred_element_type=jnp.float32
         )
-        z = jnp.concatenate([raw[:tokens] + bias_ref[0], raw[tokens:] + bias_ref[1]], axis=0)
-        soft = jnp.maximum(z, jnp.log(1.0 + jnp.exp(jnp.minimum(z, 80.0))))
-        gain = z - soft
+        return kv, jnp.concatenate([raw[:tokens] + bias_ref[0], raw[tokens:] + bias_ref[1]], axis=0)
+
+    def step(k, masked):
+        kv, z = tile(k)
         if masked:
             t = lax.broadcasted_iota(jnp.int32, (tokens, TILE), 0)
-            t = jnp.concatenate([t, t], axis=0)
-            s = lax.broadcasted_iota(jnp.int32, (2 * tokens, TILE), 1) + (k - rel) * TILE
-            soft = jnp.where(s < t, soft, 0.0)
+            s = order(lax.broadcasted_iota(jnp.int32, (tokens, TILE), 1)) + (k - rel) * TILE
+            seen = jnp.concatenate([s < t, s < t], axis=0)
+            z = jnp.where(seen, z, -1e30)
+        soft = jnp.maximum(z, jnp.log(1.0 + jnp.exp(jnp.minimum(z, 80.0))))
         between = jnp.dot(soft.astype(jnp.bfloat16), later, preferred_element_type=jnp.float32)
         held = carry[...]
-        weight = jnp.exp(gain - between - jnp.concatenate([held, held], axis=1))
-        if masked:
-            weight = jnp.where(s < t, weight, 0.0)
+        weight = jnp.exp((z - soft) - between - jnp.concatenate([held, held], axis=1))
         acc[...] += jnp.dot(weight.astype(jnp.bfloat16), kv, preferred_element_type=jnp.float32)
+        carry[...] = held + jnp.broadcast_to(between[:, :1] + soft[:, :1], held.shape)
+
+    def tame_step(k):
+        kv, z = tile(k)
+        u = jnp.exp(z)
+        u_even, u_odd = u[:, :wide], u[:, wide:]
+        even = 1.0 + u_even
+        pair = even * (1.0 + u_odd)
+        soft = jnp.log(pair)
+        short = soft.astype(jnp.bfloat16)
+        both = jnp.dot(
+            jnp.concatenate([short[:tokens], short[tokens:]], axis=1),
+            later_pair,
+            preferred_element_type=jnp.float32,
+        )
+        between = jnp.concatenate([both[:, :wide], both[:, wide:]], axis=0)
+        held = carry[...]
+        rest = jnp.exp(-(between + held)) / pair
+        weight = jnp.concatenate(
+            [(u_even * rest).astype(jnp.bfloat16), (u_odd * even * rest).astype(jnp.bfloat16)], axis=1
+        )
+        acc[...] += jnp.dot(weight, kv, preferred_element_type=jnp.float32)
         carry[...] = held + jnp.broadcast_to(between[:, :1] + soft[:, :1], held.shape)
 
     @pl.when((rel >= 0) & (rel < key_tiles))
@@ -143,9 +194,18 @@
 
     whole = jnp.clip(rel, 0, key_tiles)
 
-    @pl.loop(0, whole)
-    def _(n):
-        step(whole - 1 - n, False)
+    @pl.when(tame)
+    def _():
+        @pl.loop(0, whole // row_tiles)
+        def _(n):
+            for m in range(row_tiles):
+                tame_step(whole - 1 - row_tiles * n - m)
+
+    @pl.when(jnp.logical_not(tame))
+    def _():
+        @pl.loop(0, whole)
+        def _(n):
+            step(whole - 1 - n, False)
 
     mark_row = lax.broadcasted_iota(jnp.int32, (16, mine), 0)
     mark_lane = lax.broadcasted_iota(jnp.int32, (16, mine), 1)
@@ -154,8 +214,8 @@
     for n in range(blocks):
         first = slice(n * tok, (n + 1) * tok)
         second = slice(tokens + n * tok, tokens + (n + 1) * tok)
-        part = jnp.where(lane < HEAD_DIM, pltpu.roll(acc[first], HEAD_DIM, 1), acc[second])
-        decay = jnp.exp(-jnp.where(lane < HEAD_DIM, carry[first], carry[second]))
+        part = jnp.where(lane < HEAD_DIM, pltpu.roll(acc[first], HEAD_DIM, 1), acc[second]) * 2.0**-64
+        decay = jnp.exp(-(jnp.where(lane < HEAD_DIM, carry[first], carry[second]) + HELD))
         out_ref[n, :tok, :] = part.astype(jnp.bfloat16)
         turned = lax.dot_general(
             pick, decay.astype(jnp.bfloat16), (((1,), (1,)), ((), ())), preferred_element_type=jnp.float32
@@ -234,6 +294,7 @@
             VMEM((width, mine), jnp.bfloat16),
             VMEM((width, 2 * mine), jnp.bfloat16),
             VMEM((rows, width), jnp.bfloat16),
+            VMEM((rows, mine), jnp.float32),
             pltpu.SemaphoreType.DMA((rows // ROWS_AT_ONCE + 3 * PIECES,)),
         ],
         compiler_params=pltpu.CompilerParams(vmem_limit_bytes=LIMIT),
@@ -269,11 +330,12 @@
         out_shape=jax.ShapeDtypeStruct((ys, rows + 32, mine), jnp.bfloat16),
         scratch_shapes=[
             VMEM((2 * tokens, mine), jnp.bfloat16),
-            VMEM((zs * rows, mine), jnp.bfloat16),
+            VMEM((zs * rows // 2, mine), jnp.bfloat16),
+            VMEM((zs * rows // 2, mine), jnp.bfloat16),
             VMEM((2 * tokens, mine), jnp.float32),
             VMEM((2 * tokens, mine), jnp.float32),
         ],
-        compiler_params=pltpu.CompilerParams(vmem_limit_bytes=LIMIT),
+        compiler_params=pltpu.CompilerParams(vmem_limit_bytes=24 * 1024 * 1024),
         cost_estimate=pl.CostEstimate(flops=10**10, bytes_accessed=2 * 10**6, transcendentals=0),
         name="attend",
     )(head_bias, row_q, quarter)

time: 108 us -> 104 us (0.963)
  Pallas kernels: 23.2 us -> 20.3 us
  blocking collectives: 58 us -> 56.9 us
    pallas_call x1, Pallas kernels: 16.3 us -> 13.4 us  [local(): pl.pallas_call(attend_kernel, in_specs=[smem, vmem, vmem], out_specs=vmem...]
  transfers between devices with their start and end apart: 4 -> 4, of which waited for: 1 -> 1; matrix products, arithmetic and copies ran while one was open for 0% -> 0% of each run, Pallas kernels for 15% -> 13%
where the time goes in v6:
time: 104 us
  blocking collectives  56.9 us (55%)
  starting transfers between devices  23 us (22%)
  Pallas kernels  20.3 us (20%)
  waiting for transfers between devices  1.72 us (2%)
  local copies, waits for them, and re-layouts  1.63 us (2%)
    all_gather x1, blocking collectives, local(): quarter_half = lax.all_gather(moved, 'z', axis=0)  31.3 us
    all_to_all x1, blocking collectives, local(): every_head = lax.all_to_all(attended, ('x', 'c'), 0, 0, tiled=True)  13.7 us
    pallas_call x1, Pallas kernels, local(): pl.pallas_call(attend_kernel, in_specs=[smem, vmem, vmem], out_specs=vmem...  13.4 us
    ppermute x1, starting transfers between devices, local(): moved = lax.ppermute(kv, ('z', 'y'), pairs)  12.1 us
    all_to_all x1, blocking collectives, local(): parts = lax.all_to_all(part, 'y', 0, 0, tiled=True)  9.51 us
    pallas_call x1, Pallas kernels, local(): pl.pallas_call(project_kernel, in_specs=[anywhere, vmem, anywhere, anywhe...  4.84 us
    all_to_all x1, starting transfers between devices, local(): row_q = lax.all_to_all(queries, 'y', 0, 0, tiled=True)  4.48 us
    all_to_all x1, starting transfers between devices, local(): own_rows = lax.all_to_all(fan, 'x', 0, 0, tiled=True)  4.43 us
  transfers between devices with their start and end apart: 4, of which 1 were waited for; matrix products, arithmetic and copies ran while one was open for 0% of the time, Pallas kernels for 13%

profile of v6, /device:TPU:96, one launch (start us, length us, event | category | flops | bytes accessed | tf_op | source)
XLA Modules:
  0.0 103.7 jit_solution(12620137987310409570)
XLA Ops:
  0.0 0.0 copy-start.1
  0.0 4.8 %project.1 = (bf16[4,192,128]{2,1,0:T(8,128)(2,1)}, bf16[96,128]{1,0:T(8,128)(2,1)}) custom-call(bf16[192,2048]{1,0:T(8,128)(2,1)} %hidden_hbm.1, f32[1,2048]{1,0:T(1,128)} %bitcast.5, bf16[2048,128]{1,0:T(8,128)(2,1)} %wq_hbm.1, bf16[2048,256]{1,0:T(8,128)(2,1)} %wk_hbm.1, bf16[2048,256]{1,0:T(8,128)(2,1)} %wv_hbm.1), custom_call_target="tpu_custom_call" | custom-call | flops 301989888 | bytes 2359296 | tf_op jit(solution)/shard_map/project/pallas_call | solution.py:284
  4.8 4.5 %all-to-all-start = ((bf16[4,192,128]{2,1,0:T(8,128)(2,1)}), bf16[4,192,128]{2,1,0:T(8,128)(2,1)S(1)}, u32[]{:S(2)}, u32[]{:S(2)}) async-start(bf16[4,192,128]{2,1,0:T(8,128)(2,1)} %get-tuple-element.12), calls=%async_computation | async-start | bytes 393216 | tf_op jit(solution)/shard_map/all_to_all | solution.py:316
  9.3 12.1 %collective-permute-start = (bf16[96,128]{1,0:T(8,128)(2,1)}, bf16[96,128]{1,0:T(8,128)(2,1)S(1)}, u32[]{:S(2)}, u32[]{:S(2)}) collective-permute-start(bf16[96,128]{1,0:T(8,128)(2,1)} %get-tuple-element.13), channel_id=1, source_target_pairs={{0,320},{8,352},{16,416},{24,384},{32,448},{40,480},{48,32},{56,0}... | collective-permute-start | bytes 73736 | tf_op jit(solution)/shard_map/ppermute | solution.py:315
  21.4 1.7 %collective-permute-done = bf16[96,128]{1,0:T(8,128)(2,1)S(1)} collective-permute-done((bf16[96,128]{1,0:T(8,128)(2,1)}, bf16[96,128]{1,0:T(8,128)(2,1)S(1)}, u32[]{:S(2)}, u32[]{:S(2)}) %collective-permute-start) | collective-permute-done | bytes 24608 | tf_op jit(solution)/shard_map/ppermute | solution.py:315
  23.1 0.0 all-to-all-done.q_ref
  23.1 0.0 copy-done.1
  23.2 1.6 %broadcast_in_dim.10 = bf16[4,128,2048]{2,1,0:T(8,128)(2,1)} broadcast(bf16[128,2048]{1,0:T(8,128)(2,1)S(1)} %copy-done.1), dimensions={1,2} | broadcast | bytes 2621440 | tf_op jit(solution)/shard_map/broadcast_in_dim | solution.py:317
  24.8 0.0 copy-start
  24.8 4.4 %all-to-all-start.1 = ((bf16[4,128,2048]{2,1,0:T(8,128)(2,1)}), bf16[4,128,2048]{2,1,0:T(8,128)(2,1)S(1)}, u32[]{:S(2)}, u32[]{:S(2)}) async-start(bf16[4,128,2048]{2,1,0:T(8,128)(2,1)} %broadcast_in_dim.10), calls=%async_computation.1 | async-start | bytes 4194304 | tf_op jit(solution)/shard_map/all_to_all | solution.py:319
  29.2 31.3 %all-gather = bf16[1536,128]{1,0:T(8,128)(2,1)S(1)} all-gather(bf16[96,128]{1,0:T(8,128)(2,1)S(1)} %collective-permute-done), channel_id=2, replica_groups=mesh['z'=16,'y'=4,'x'=4,'c'=2] {'z'}, dimensions={0}, use_global_device_ids=true | all-gather | bytes 417792 | tf_op jit(solution)/shard_map/all_gather | solution.py:320
  60.5 2.4 %all-gather.1 = bf16[32,96,128]{2,1,0:T(8,128)(2,1)S(1)} all-gather(bf16[16,96,128]{2,1,0:T(8,128)(2,1)S(1)} %bitcast.4), channel_id=3, replica_groups=mesh['z'=16,'y'=4,'x'=4,'c'=2] {'c'}, dimensions={0}, use_global_device_ids=true | all-gather | bytes 1179648 | tf_op jit(solution)/shard_map/all_gather | solution.py:321
  62.9 0.0 all-to-all-done.1.own_ref
  62.9 2.0 %collective-permute-start.1 = (bf16[4,128,2048]{2,1,0:T(8,128)(2,1)S(1)}, bf16[4,128,2048]{2,1,0:T(8,128)(2,1)S(1)}, u32[]{:S(2)}, u32[]{:S(2)}) collective-permute-start(bf16[4,128,2048]{2,1,0:T(8,128)(2,1)S(1)} %all-to-all-done.1.own_ref), channel_id=1, source_target_pairs={{0,1},{1,0},{2,3},{3,2},{4,5},{5,4},{6,7},{7,6},{8,9},{9,8},{10,11... | collective-permute-start | bytes 6291464 | tf_op jit(solution)/shard_map/ppermute | solution.py:323
  64.9 0.0 copy-done
  64.9 13.4 %attend.1 = bf16[4,224,128]{2,1,0:T(8,128)(2,1)S(1)} custom-call(f32[2]{0:T(128)S(1)} %copy-done, bf16[4,192,128]{2,1,0:T(8,128)(2,1)S(1)} %all-to-all-done.q_ref, bf16[2,16,96,128]{3,2,1,0:T(8,128)(2,1)S(1)} %bitcast.3), custom_call_target="tpu_custom_call" | custom-call | flops 10000000000 | bytes 2000000 | tf_op jit(solution)/shard_map/attend/pallas_call | solution.py:326
  78.3 9.5 %all_to_all.20.part_ref = bf16[4,224,128]{2,1,0:T(8,128)(2,1)S(1)} all-to-all(bf16[4,224,128]{2,1,0:T(8,128)(2,1)S(1)} %attend.1), channel_id=1, replica_groups=mesh['z'=16,'y'=4,'x'=4,'c'=2] {'y'}, dimensions={0} | all-to-all | bytes 458752 | tf_op jit(solution)/shard_map/all_to_all | solution.py:343
  87.8 0.2 combine.1
  88.1 13.7 %all_to_all.21.heads_ref = bf16[8,192,128]{2,1,0:T(8,128)(2,1)S(1)} all-to-all(bf16[8,192,128]{2,1,0:T(8,128)(2,1)S(1)} %combine.1), channel_id=1, replica_groups=mesh['z'=16,'y'=4,'x'=4,'c'=2] {'x','c'}, dimensions={0} | all-to-all | bytes 786432 | tf_op jit(solution)/shard_map/all_to_all | solution.py:352
  101.8 0.0 collective-permute-done.1.other_ref
  101.8 1.9 %project_out.1 = bf16[192,2048]{1,0:T(8,128)(2,1)} custom-call(bf16[8,192,128]{2,1,0:T(8,128)(2,1)S(1)} %all_to_all.21.heads_ref, bf16[4,128,2048]{2,1,0:T(8,128)(2,1)S(1)} %all-to-all-done.1.own_ref, bf16[4,128,2048]{2,1,0:T(8,128)(2,1)S(1)} %collective-permute-done.1.other_ref), custom_call_target="tpu_custom_call" | custom-call | flops 805306368 | bytes 4194304 | tf_op jit(solution)/shard_map/project_out/pallas_call | solution.py:354
Async XLA Ops:
  0.0 23.1 %copy-start.1 = (bf16[128,2048]{1,0:T(8,128)(2,1)S(1)}, bf16[128,2048]{1,0:T(8,128)(2,1)}, u32[]{:S(2)}) copy-start(bf16[128,2048]{1,0:T(8,128)(2,1)} %param.13) | copy-start | bytes 1572868
  4.8 18.3 %all-to-all-start = ((bf16[4,192,128]{2,1,0:T(8,128)(2,1)}), bf16[4,192,128]{2,1,0:T(8,128)(2,1)S(1)}, u32[]{:S(2)}, u32[]{:S(2)}) async-start(bf16[4,192,128]{2,1,0:T(8,128)(2,1)} %get-tuple-element.12), calls=%async_computation | async-start | bytes 393216 | tf_op jit(solution)/shard_map/all_to_all | solution.py:316
  9.3 13.8 %collective-permute-start = (bf16[96,128]{1,0:T(8,128)(2,1)}, bf16[96,128]{1,0:T(8,128)(2,1)S(1)}, u32[]{:S(2)}, u32[]{:S(2)}) collective-permute-start(bf16[96,128]{1,0:T(8,128)(2,1)} %get-tuple-element.13), channel_id=1, source_target_pairs={{0,320},{8,352},{16,416},{24,384},{32,448},{40,480},{48,32},{56,0}... | collective-permute-start | bytes 73736 | tf_op jit(solution)/shard_map/ppermute | solution.py:315
  24.8 40.2 %copy-start = (f32[2]{0:T(128)S(1)}, f32[2]{0:T(128)}, u32[]{:S(2)}) copy-start(f32[2]{0:T(128)} %bias_ref.1) | copy-start | bytes 28
  24.8 38.1 %all-to-all-start.1 = ((bf16[4,128,2048]{2,1,0:T(8,128)(2,1)}), bf16[4,128,2048]{2,1,0:T(8,128)(2,1)S(1)}, u32[]{:S(2)}, u32[]{:S(2)}) async-start(bf16[4,128,2048]{2,1,0:T(8,128)(2,1)} %broadcast_in_dim.10), calls=%async_computation.1 | async-start | bytes 4194304 | tf_op jit(solution)/shard_map/all_to_all | solution.py:319
  62.9 38.9 %collective-permute-start.1 = (bf16[4,128,2048]{2,1,0:T(8,128)(2,1)S(1)}, bf16[4,128,2048]{2,1,0:T(8,128)(2,1)S(1)}, u32[]{:S(2)}, u32[]{:S(2)}) collective-permute-start(bf16[4,128,2048]{2,1,0:T(8,128)(2,1)S(1)} %all-to-all-done.1.own_ref), channel_id=1, source_target_pairs={{0,1},{1,0},{2,3},{3,2},{4,5},{5,4},{6,7},{7,6},{8,9},{9,8},{10,11... | collective-permute-start | bytes 6291464 | tf_op jit(solution)/shard_map/ppermute | solution.py:323

commit v7 on v6

--- a/solution.py
+++ b/solution.py
@@ -11,64 +11,57 @@
 
 HEAD_DIM = 64
 TILE = 256
+AT_ONCE = 6
 VMEM = pltpu.VMEM
 SMEM = pltpu.SMEM
-LIMIT = 56 * 1024 * 1024
 HELD = 64 * math.log(2.0)
 
 
-PIECES = 4
 ROWS_AT_ONCE = 32
 NEAR = ((-6, -5, -3, -4), (-2, -1, 1, 0), (5, 4, 2, 3), (9, 8, 6, 7))
 
 
 def project_kernel(
-    hidden_hbm, gain_ref, wq_hbm, wk_hbm, wv_hbm, q_ref, kv_ref, hidden_ref, wq_ref, wkv_ref, normed_ref, turn_ref, sems
+    hidden_hbm,
+    gain_hbm,
+    wq_hbm,
+    wk_hbm,
+    wv_hbm,
+    q_ref,
+    kv_ref,
+    hidden_ref,
+    gain_ref,
+    wq_ref,
+    wkv_ref,
+    normed_ref,
+    turn_ref,
+    sems,
 ):
-    rows, width = hidden_ref.shape
+    rows, _ = hidden_ref.shape
     mine = 2 * HEAD_DIM
-    depth = width // PIECES
     x = lax.axis_index("x")
     cols = pl.ds(pl.multiple_of((x // 2) * mine, mine), mine)
-    pieces = rows // ROWS_AT_ONCE
-    copies = []
-    for n in range(pieces):
-        part = slice(n * ROWS_AT_ONCE, (n + 1) * ROWS_AT_ONCE)
-        copies.append(
-            pltpu.make_async_copy(hidden_hbm.at[part, :], hidden_ref.at[part, :], sems.at[n])
-        )
-    for n in range(PIECES):
-        part = slice(n * depth, (n + 1) * depth)
-        for side, src in enumerate((wk_hbm, wv_hbm)):
-            copies.append(
-                pltpu.make_async_copy(
-                    src.at[part, cols],
-                    wkv_ref.at[part, side * mine : (side + 1) * mine],
-                    sems.at[pieces + 2 * n + side],
-                )
-            )
-    for n in range(PIECES):
-        part = slice(n * depth, (n + 1) * depth)
-        copies.append(
-            pltpu.make_async_copy(
-                wq_hbm.at[part, :], wq_ref.at[part, :], sems.at[pieces + 2 * PIECES + n]
-            )
-        )
+    pairs = (
+        (gain_hbm, gain_ref),
+        (hidden_hbm, hidden_ref),
+        (wk_hbm.at[:, cols], wkv_ref.at[:, :mine]),
+        (wv_hbm.at[:, cols], wkv_ref.at[:, mine:]),
+        (wq_hbm, wq_ref),
+    )
+    copies = [pltpu.make_async_copy(src, dst, sems.at[n]) for n, (src, dst) in enumerate(pairs)]
     for copy in copies:
         copy.start()
-    for n in range(pieces):
+    copies[0].wait()
+    copies[1].wait()
+    for n in range(rows // ROWS_AT_ONCE):
         part = slice(n * ROWS_AT_ONCE, (n + 1) * ROWS_AT_ONCE)
-        copies[n].wait()
         wide = hidden_ref[part, :].astype(jnp.float32)
         inv = lax.rsqrt(jnp.mean(wide * wide, axis=-1, keepdims=True) + 1e-06)
         normed_ref[part, :] = (wide * inv * gain_ref[...]).astype(jnp.bfloat16)
 
-    both = jnp.zeros((rows, 2 * mine), jnp.float32)
-    for n in range(PIECES):
-        part = slice(n * depth, (n + 1) * depth)
-        copies[pieces + 2 * n].wait()
-        copies[pieces + 2 * n + 1].wait()
-        both += jnp.dot(normed_ref[:, part], wkv_ref[part, :], preferred_element_type=jnp.float32)
+    copies[2].wait()
+    copies[3].wait()
+    both = jnp.dot(normed_ref[...], wkv_ref[...], preferred_element_type=jnp.float32)
     k, v = both[:, :mine], both[:, mine:]
     upper = x % 2 == 1
     lane = lax.broadcasted_iota(jnp.int32, k.shape, 1)
@@ -83,11 +76,8 @@
         part = slice(odd * few, (odd + 1) * few)
         kv_ref[part, :] = jnp.where(lax.axis_index("c") == 0, first, second).astype(jnp.bfloat16)
 
-    q = jnp.zeros((rows, mine), jnp.float32)
-    for n in range(PIECES):
-        part = slice(n * depth, (n + 1) * depth)
-        copies[pieces + 2 * PIECES + n].wait()
-        q += jnp.dot(normed_ref[:, part], wq_ref[part, :], preferred_element_type=jnp.float32)
+    copies[4].wait()
+    q = jnp.dot(normed_ref[...], wq_ref[...], preferred_element_type=jnp.float32)
     q = q.astype(jnp.bfloat16) * jnp.bfloat16(HEAD_DIM**-0.5)
     for dest in range(q_ref.shape[0]):
         q_ref[dest] = q
@@ -196,10 +186,16 @@
 
     @pl.when(tame)
     def _():
-        @pl.loop(0, whole // row_tiles)
+        @pl.loop(0, whole // AT_ONCE)
         def _(n):
-            for m in range(row_tiles):
-                tame_step(whole - 1 - row_tiles * n - m)
+            for m in range(AT_ONCE):
+                tame_step(whole - 1 - AT_ONCE * n - m)
+
+        left = lax.rem(whole, AT_ONCE)
+
+        @pl.loop(0, left)
+        def _(n):
+            tame_step(left - 1 - n)
 
     @pl.when(jnp.logical_not(tame))
     def _():
@@ -283,7 +279,7 @@
 
     queries, kv = pl.pallas_call(
         project_kernel,
-        in_specs=[anywhere, vmem, anywhere, anywhere, anywhere],
+        in_specs=[anywhere] * 5,
         out_specs=[vmem, vmem],
         out_shape=[
             jax.ShapeDtypeStruct((ys, rows, mine), jnp.bfloat16),
@@ -291,13 +287,14 @@
         ],
         scratch_shapes=[
             VMEM((rows, width), jnp.bfloat16),
+            VMEM((1, width), jnp.float32),
             VMEM((width, mine), jnp.bfloat16),
             VMEM((width, 2 * mine), jnp.bfloat16),
             VMEM((rows, width), jnp.bfloat16),
             VMEM((rows, mine), jnp.float32),
-            pltpu.SemaphoreType.DMA((rows // ROWS_AT_ONCE + 3 * PIECES,)),
+            pltpu.SemaphoreType.DMA((5,)),
         ],
-        compiler_params=pltpu.CompilerParams(vmem_limit_bytes=LIMIT),
+        compiler_params=pltpu.CompilerParams(vmem_limit_bytes=56 * 1024 * 1024),
         cost_estimate=pl.CostEstimate(
             flops=2 * rows * width * 3 * mine,
             bytes_accessed=2 * width * (rows + 3 * mine),

time: 104 us -> 103 us (level)
    pallas_call x1, Pallas kernels: 4.84 us -> 3.44 us  [local(): pl.pallas_call(project_kernel, in_specs=[anywhere] * 5, out_specs=[vmem,...]
  transfers between devices with their start and end apart: 4 -> 4, of which waited for: 1 -> 1; matrix products, arithmetic and copies ran while one was open for 0% -> 0% of each run, Pallas kernels for 13% -> 14%
where the time goes in v7:
time: 103 us
  blocking collectives  56.9 us (55%)
  starting transfers between devices  23 us (22%)
  Pallas kernels  19.4 us (19%)
  waiting for transfers between devices  1.72 us (2%)
  local copies, waits for them, and re-layouts  1.63 us (2%)
    all_gather x1, blocking collectives, local(): quarter_half = lax.all_gather(moved, 'z', axis=0)  31.3 us
    pallas_call x1, Pallas kernels, local(): pl.pallas_call(attend_kernel, in_specs=[smem, vmem, vmem], out_specs=vmem...  13.8 us
    all_to_all x1, blocking collectives, local(): every_head = lax.all_to_all(attended, ('x', 'c'), 0, 0, tiled=True)  13.7 us
    ppermute x1, starting transfers between devices, local(): moved = lax.ppermute(kv, ('z', 'y'), pairs)  12.1 us
    all_to_all x1, blocking collectives, local(): parts = lax.all_to_all(part, 'y', 0, 0, tiled=True)  9.51 us
    all_to_all x1, starting transfers between devices, local(): row_q = lax.all_to_all(queries, 'y', 0, 0, tiled=True)  4.48 us
    all_to_all x1, starting transfers between devices, local(): own_rows = lax.all_to_all(fan, 'x', 0, 0, tiled=True)  4.43 us
    pallas_call x1, Pallas kernels, local(): pl.pallas_call(project_kernel, in_specs=[anywhere] * 5, out_specs=[vmem,...  3.44 us
  transfers between devices with their start and end apart: 4, of which 1 were waited for; matrix products, arithmetic and copies ran while one was open for 0% of the time, Pallas kernels for 14%

profile of v7, /device:TPU:96, one launch (start us, length us, event | category | flops | bytes accessed | tf_op | source)
XLA Modules:
  0.0 102.7 jit_solution(17442382616796899079)
XLA Ops:
  0.0 0.0 copy-start.1
  0.0 3.4 %project.1 = (bf16[4,192,128]{2,1,0:T(8,128)(2,1)}, bf16[96,128]{1,0:T(8,128)(2,1)}) custom-call(bf16[192,2048]{1,0:T(8,128)(2,1)} %hidden_hbm.1, f32[1,2048]{1,0:T(1,128)} %bitcast.5, bf16[2048,128]{1,0:T(8,128)(2,1)} %wq_hbm.1, bf16[2048,256]{1,0:T(8,128)(2,1)} %wk_hbm.1, bf16[2048,256]{1,0:T(8,128)(2,1)} %wv_hbm.1), custom_call_target="tpu_custom_call" | custom-call | flops 301989888 | bytes 2359296 | tf_op jit(solution)/shard_map/project/pallas_call | solution.py:280
  3.4 4.5 %all-to-all-start = ((bf16[4,192,128]{2,1,0:T(8,128)(2,1)}), bf16[4,192,128]{2,1,0:T(8,128)(2,1)S(1)}, u32[]{:S(2)}, u32[]{:S(2)}) async-start(bf16[4,192,128]{2,1,0:T(8,128)(2,1)} %get-tuple-element.12), calls=%async_computation | async-start | bytes 393216 | tf_op jit(solution)/shard_map/all_to_all | solution.py:313
  7.9 12.1 %collective-permute-start = (bf16[96,128]{1,0:T(8,128)(2,1)}, bf16[96,128]{1,0:T(8,128)(2,1)S(1)}, u32[]{:S(2)}, u32[]{:S(2)}) collective-permute-start(bf16[96,128]{1,0:T(8,128)(2,1)} %get-tuple-element.13), channel_id=1, source_target_pairs={{0,320},{8,352},{16,416},{24,384},{32,448},{40,480},{48,32},{56,0}... | collective-permute-start | bytes 73736 | tf_op jit(solution)/shard_map/ppermute | solution.py:312
  20.0 1.7 %collective-permute-done = bf16[96,128]{1,0:T(8,128)(2,1)S(1)} collective-permute-done((bf16[96,128]{1,0:T(8,128)(2,1)}, bf16[96,128]{1,0:T(8,128)(2,1)S(1)}, u32[]{:S(2)}, u32[]{:S(2)}) %collective-permute-start) | collective-permute-done | bytes 24608 | tf_op jit(solution)/shard_map/ppermute | solution.py:312
  21.7 0.0 all-to-all-done.q_ref
  21.7 0.0 copy-done.1
  21.7 1.6 %broadcast_in_dim.10 = bf16[4,128,2048]{2,1,0:T(8,128)(2,1)} broadcast(bf16[128,2048]{1,0:T(8,128)(2,1)S(1)} %copy-done.1), dimensions={1,2} | broadcast | bytes 2621440 | tf_op jit(solution)/shard_map/broadcast_in_dim | solution.py:314
  23.4 0.0 copy-start
  23.4 4.4 %all-to-all-start.1 = ((bf16[4,128,2048]{2,1,0:T(8,128)(2,1)}), bf16[4,128,2048]{2,1,0:T(8,128)(2,1)S(1)}, u32[]{:S(2)}, u32[]{:S(2)}) async-start(bf16[4,128,2048]{2,1,0:T(8,128)(2,1)} %broadcast_in_dim.10), calls=%async_computation.1 | async-start | bytes 4194304 | tf_op jit(solution)/shard_map/all_to_all | solution.py:316
  27.8 31.3 %all-gather = bf16[1536,128]{1,0:T(8,128)(2,1)S(1)} all-gather(bf16[96,128]{1,0:T(8,128)(2,1)S(1)} %collective-permute-done), channel_id=2, replica_groups=mesh['z'=16,'y'=4,'x'=4,'c'=2] {'z'}, dimensions={0}, use_global_device_ids=true | all-gather | bytes 417792 | tf_op jit(solution)/shard_map/all_gather | solution.py:317
  59.1 2.4 %all-gather.1 = bf16[32,96,128]{2,1,0:T(8,128)(2,1)S(1)} all-gather(bf16[16,96,128]{2,1,0:T(8,128)(2,1)S(1)} %bitcast.4), channel_id=3, replica_groups=mesh['z'=16,'y'=4,'x'=4,'c'=2] {'c'}, dimensions={0}, use_global_device_ids=true | all-gather | bytes 1179648 | tf_op jit(solution)/shard_map/all_gather | solution.py:318
  61.5 0.0 all-to-all-done.1.own_ref
  61.5 2.0 %collective-permute-start.1 = (bf16[4,128,2048]{2,1,0:T(8,128)(2,1)S(1)}, bf16[4,128,2048]{2,1,0:T(8,128)(2,1)S(1)}, u32[]{:S(2)}, u32[]{:S(2)}) collective-permute-start(bf16[4,128,2048]{2,1,0:T(8,128)(2,1)S(1)} %all-to-all-done.1.own_ref), channel_id=1, source_target_pairs={{0,1},{1,0},{2,3},{3,2},{4,5},{5,4},{6,7},{7,6},{8,9},{9,8},{10,11... | collective-permute-start | bytes 6291464 | tf_op jit(solution)/shard_map/ppermute | solution.py:320
  63.5 0.0 copy-done
  63.5 13.8 %attend.1 = bf16[4,224,128]{2,1,0:T(8,128)(2,1)S(1)} custom-call(f32[2]{0:T(128)S(1)} %copy-done, bf16[4,192,128]{2,1,0:T(8,128)(2,1)S(1)} %all-to-all-done.q_ref, bf16[2,16,96,128]{3,2,1,0:T(8,128)(2,1)S(1)} %bitcast.3), custom_call_target="tpu_custom_call" | custom-call | flops 10000000000 | bytes 2000000 | tf_op jit(solution)/shard_map/attend/pallas_call | solution.py:323
  77.4 9.5 %all_to_all.20.part_ref = bf16[4,224,128]{2,1,0:T(8,128)(2,1)S(1)} all-to-all(bf16[4,224,128]{2,1,0:T(8,128)(2,1)S(1)} %attend.1), channel_id=1, replica_groups=mesh['z'=16,'y'=4,'x'=4,'c'=2] {'y'}, dimensions={0} | all-to-all | bytes 458752 | tf_op jit(solution)/shard_map/all_to_all | solution.py:340
  86.9 0.2 combine.1
  87.1 13.7 %all_to_all.21.heads_ref = bf16[8,192,128]{2,1,0:T(8,128)(2,1)S(1)} all-to-all(bf16[8,192,128]{2,1,0:T(8,128)(2,1)S(1)} %combine.1), channel_id=1, replica_groups=mesh['z'=16,'y'=4,'x'=4,'c'=2] {'x','c'}, dimensions={0} | all-to-all | bytes 786432 | tf_op jit(solution)/shard_map/all_to_all | solution.py:349
  100.9 0.0 collective-permute-done.1.other_ref
  100.9 1.9 %project_out.1 = bf16[192,2048]{1,0:T(8,128)(2,1)} custom-call(bf16[8,192,128]{2,1,0:T(8,128)(2,1)S(1)} %all_to_all.21.heads_ref, bf16[4,128,2048]{2,1,0:T(8,128)(2,1)S(1)} %all-to-all-done.1.own_ref, bf16[4,128,2048]{2,1,0:T(8,128)(2,1)S(1)} %collective-permute-done.1.other_ref), custom_call_target="tpu_custom_call" | custom-call | flops 805306368 | bytes 4194304 | tf_op jit(solution)/shard_map/project_out/pallas_call | solution.py:351
Async XLA Ops:
  0.0 21.7 %copy-start.1 = (bf16[128,2048]{1,0:T(8,128)(2,1)S(1)}, bf16[128,2048]{1,0:T(8,128)(2,1)}, u32[]{:S(2)}) copy-start(bf16[128,2048]{1,0:T(8,128)(2,1)} %param.13) | copy-start | bytes 1572868
  3.4 18.3 %all-to-all-start = ((bf16[4,192,128]{2,1,0:T(8,128)(2,1)}), bf16[4,192,128]{2,1,0:T(8,128)(2,1)S(1)}, u32[]{:S(2)}, u32[]{:S(2)}) async-start(bf16[4,192,128]{2,1,0:T(8,128)(2,1)} %get-tuple-element.12), calls=%async_computation | async-start | bytes 393216 | tf_op jit(solution)/shard_map/all_to_all | solution.py:313
  7.9 13.8 %collective-permute-start = (bf16[96,128]{1,0:T(8,128)(2,1)}, bf16[96,128]{1,0:T(8,128)(2,1)S(1)}, u32[]{:S(2)}, u32[]{:S(2)}) collective-permute-start(bf16[96,128]{1,0:T(8,128)(2,1)} %get-tuple-element.13), channel_id=1, source_target_pairs={{0,320},{8,352},{16,416},{24,384},{32,448},{40,480},{48,32},{56,0}... | collective-permute-start | bytes 73736 | tf_op jit(solution)/shard_map/ppermute | solution.py:312
  23.4 40.2 %copy-start = (f32[2]{0:T(128)S(1)}, f32[2]{0:T(128)}, u32[]{:S(2)}) copy-start(f32[2]{0:T(128)} %bias_ref.1) | copy-start | bytes 28
  23.4 38.1 %all-to-all-start.1 = ((bf16[4,128,2048]{2,1,0:T(8,128)(2,1)}), bf16[4,128,2048]{2,1,0:T(8,128)(2,1)S(1)}, u32[]{:S(2)}, u32[]{:S(2)}) async-start(bf16[4,128,2048]{2,1,0:T(8,128)(2,1)} %broadcast_in_dim.10), calls=%async_computation.1 | async-start | bytes 4194304 | tf_op jit(solution)/shard_map/all_to_all | solution.py:316
  61.5 39.4 %collective-permute-start.1 = (bf16[4,128,2048]{2,1,0:T(8,128)(2,1)S(1)}, bf16[4,128,2048]{2,1,0:T(8,128)(2,1)S(1)}, u32[]{:S(2)}, u32[]{:S(2)}) collective-permute-start(bf16[4,128,2048]{2,1,0:T(8,128)(2,1)S(1)} %all-to-all-done.1.own_ref), channel_id=1, source_target_pairs={{0,1},{1,0},{2,3},{3,2},{4,5},{5,4},{6,7},{7,6},{8,9},{9,8},{10,11... | collective-permute-start | bytes 6291464 | tf_op jit(solution)/shard_map/ppermute | solution.py:320

commit v8 on v7

--- a/solution.py
+++ b/solution.py
@@ -140,13 +140,16 @@
         )
         return kv, jnp.concatenate([raw[:tokens] + bias_ref[0], raw[tokens:] + bias_ref[1]], axis=0)
 
+    def shown(k, z):
+        t = lax.broadcasted_iota(jnp.int32, (tokens, TILE), 0)
+        s = order(lax.broadcasted_iota(jnp.int32, (tokens, TILE), 1))
+        seen = s - t < (rel - k) * TILE
+        return jnp.where(jnp.concatenate([seen, seen], axis=0), z, -1e30)
+
     def step(k, masked):
         kv, z = tile(k)
         if masked:
-            t = lax.broadcasted_iota(jnp.int32, (tokens, TILE), 0)
-            s = order(lax.broadcasted_iota(jnp.int32, (tokens, TILE), 1)) + (k - rel) * TILE
-            seen = jnp.concatenate([s < t, s < t], axis=0)
-            z = jnp.where(seen, z, -1e30)
+            z = shown(k, z)
         soft = jnp.maximum(z, jnp.log(1.0 + jnp.exp(jnp.minimum(z, 80.0))))
         between = jnp.dot(soft.astype(jnp.bfloat16), later, preferred_element_type=jnp.float32)
         held = carry[...]
@@ -154,8 +157,10 @@
         acc[...] += jnp.dot(weight.astype(jnp.bfloat16), kv, preferred_element_type=jnp.float32)
         carry[...] = held + jnp.broadcast_to(between[:, :1] + soft[:, :1], held.shape)
 
-    def tame_step(k):
+    def tame_step(k, masked):
         kv, z = tile(k)
+        if masked:
+            z = shown(k, z)
         u = jnp.exp(z)
         u_even, u_odd = u[:, :wide], u[:, wide:]
         even = 1.0 + u_even
@@ -176,29 +181,32 @@
         acc[...] += jnp.dot(weight, kv, preferred_element_type=jnp.float32)
         carry[...] = held + jnp.broadcast_to(between[:, :1] + soft[:, :1], held.shape)
 
-    @pl.when((rel >= 0) & (rel < key_tiles))
+    crossed = (rel >= 0) & (rel < key_tiles)
+    whole = jnp.clip(rel, 0, key_tiles)
+
+    @pl.when(tame & crossed)
     def _():
-        @pl.loop(0, row_tiles)
-        def _(n):
-            step(rel + row_tiles - 1 - n, True)
-
-    whole = jnp.clip(rel, 0, key_tiles)
+        for m in range(row_tiles):
+            tame_step(rel + row_tiles - 1 - m, True)
 
     @pl.when(tame)
     def _():
         @pl.loop(0, whole // AT_ONCE)
         def _(n):
             for m in range(AT_ONCE):
-                tame_step(whole - 1 - AT_ONCE * n - m)
-
-        left = lax.rem(whole, AT_ONCE)
-
-        @pl.loop(0, left)
-        def _(n):
-            tame_step(left - 1 - n)
+                tame_step(whole - 1 - AT_ONCE * n - m, False)
+
+        @pl.when(lax.rem(whole, AT_ONCE) > 0)
+        def _():
+            for m in range(row_tiles):
+                tame_step(row_tiles - 1 - m, False)
 
     @pl.when(jnp.logical_not(tame))
     def _():
+        @pl.loop(0, jnp.where(crossed, row_tiles, 0))
+        def _(n):
+            step(rel + row_tiles - 1 - n, True)
+
         @pl.loop(0, whole)
         def _(n):
             step(whole - 1 - n, False)

time: 103 us -> 102 us (level)
  Pallas kernels: 19.4 us -> 18 us
    pallas_call x1, Pallas kernels: 13.8 us -> 12.4 us  [local(): pl.pallas_call(attend_kernel, in_specs=[smem, vmem, vmem], out_specs=vmem...]
  transfers between devices with their start and end apart: 4 -> 4, of which waited for: 1 -> 1; matrix products, arithmetic and copies ran while one was open for 0% -> 0% of each run, Pallas kernels for 14% -> 12%
where the time goes in v8:
time: 102 us; the launch traced here: 101 us
  blocking collectives  56.9 us (56%)
  starting transfers between devices  23 us (23%)
  Pallas kernels  18 us (18%)
  waiting for transfers between devices  1.72 us (2%)
  local copies, waits for them, and re-layouts  1.63 us (2%)
    all_gather x1, blocking collectives, local(): quarter_half = lax.all_gather(moved, 'z', axis=0)  31.3 us
    all_to_all x1, blocking collectives, local(): every_head = lax.all_to_all(attended, ('x', 'c'), 0, 0, tiled=True)  13.7 us
    pallas_call x1, Pallas kernels, local(): pl.pallas_call(attend_kernel, in_specs=[smem, vmem, vmem], out_specs=vmem...  12.4 us
    ppermute x1, starting transfers between devices, local(): moved = lax.ppermute(kv, ('z', 'y'), pairs)  12.1 us
    all_to_all x1, blocking collectives, local(): parts = lax.all_to_all(part, 'y', 0, 0, tiled=True)  9.5 us
    all_to_all x1, starting transfers between devices, local(): row_q = lax.all_to_all(queries, 'y', 0, 0, tiled=True)  4.47 us
    all_to_all x1, starting transfers between devices, local(): own_rows = lax.all_to_all(fan, 'x', 0, 0, tiled=True)  4.42 us
    pallas_call x1, Pallas kernels, local(): pl.pallas_call(project_kernel, in_specs=[anywhere] * 5, out_specs=[vmem,...  3.44 us
  transfers between devices with their start and end apart: 4, of which 1 were waited for; matrix products, arithmetic and copies ran while one was open for 0% of the time, Pallas kernels for 12%

profile of v8, /device:TPU:96, one launch (start us, length us, event | category | flops | bytes accessed | tf_op | source)
XLA Modules:
  0.0 101.3 jit_solution(4340720618607682000)
XLA Ops:
  0.0 0.0 copy-start.1
  0.0 3.4 %project.1 = (bf16[4,192,128]{2,1,0:T(8,128)(2,1)}, bf16[96,128]{1,0:T(8,128)(2,1)}) custom-call(bf16[192,2048]{1,0:T(8,128)(2,1)} %hidden_hbm.1, f32[1,2048]{1,0:T(1,128)} %bitcast.5, bf16[2048,128]{1,0:T(8,128)(2,1)} %wq_hbm.1, bf16[2048,256]{1,0:T(8,128)(2,1)} %wk_hbm.1, bf16[2048,256]{1,0:T(8,128)(2,1)} %wv_hbm.1), custom_call_target="tpu_custom_call" | custom-call | flops 301989888 | bytes 2359296 | tf_op jit(solution)/shard_map/project/pallas_call | solution.py:288
  3.4 4.5 %all-to-all-start = ((bf16[4,192,128]{2,1,0:T(8,128)(2,1)}), bf16[4,192,128]{2,1,0:T(8,128)(2,1)S(1)}, u32[]{:S(2)}, u32[]{:S(2)}) async-start(bf16[4,192,128]{2,1,0:T(8,128)(2,1)} %get-tuple-element.12), calls=%async_computation | async-start | bytes 393216 | tf_op jit(solution)/shard_map/all_to_all | solution.py:321
  7.9 12.1 %collective-permute-start = (bf16[96,128]{1,0:T(8,128)(2,1)}, bf16[96,128]{1,0:T(8,128)(2,1)S(1)}, u32[]{:S(2)}, u32[]{:S(2)}) collective-permute-start(bf16[96,128]{1,0:T(8,128)(2,1)} %get-tuple-element.13), channel_id=1, source_target_pairs={{0,320},{8,352},{16,416},{24,384},{32,448},{40,480},{48,32},{56,0}... | collective-permute-start | bytes 73736 | tf_op jit(solution)/shard_map/ppermute | solution.py:320
  20.0 1.7 %collective-permute-done = bf16[96,128]{1,0:T(8,128)(2,1)S(1)} collective-permute-done((bf16[96,128]{1,0:T(8,128)(2,1)}, bf16[96,128]{1,0:T(8,128)(2,1)S(1)}, u32[]{:S(2)}, u32[]{:S(2)}) %collective-permute-start) | collective-permute-done | bytes 24608 | tf_op jit(solution)/shard_map/ppermute | solution.py:320
  21.7 0.0 all-to-all-done.q_ref
  21.7 0.0 copy-done.1
  21.8 1.6 %broadcast_in_dim.10 = bf16[4,128,2048]{2,1,0:T(8,128)(2,1)} broadcast(bf16[128,2048]{1,0:T(8,128)(2,1)S(1)} %copy-done.1), dimensions={1,2} | broadcast | bytes 2621440 | tf_op jit(solution)/shard_map/broadcast_in_dim | solution.py:322
  23.4 0.0 copy-start
  23.4 4.4 %all-to-all-start.1 = ((bf16[4,128,2048]{2,1,0:T(8,128)(2,1)}), bf16[4,128,2048]{2,1,0:T(8,128)(2,1)S(1)}, u32[]{:S(2)}, u32[]{:S(2)}) async-start(bf16[4,128,2048]{2,1,0:T(8,128)(2,1)} %broadcast_in_dim.10), calls=%async_computation.1 | async-start | bytes 4194304 | tf_op jit(solution)/shard_map/all_to_all | solution.py:324
  27.8 31.3 %all-gather = bf16[1536,128]{1,0:T(8,128)(2,1)S(1)} all-gather(bf16[96,128]{1,0:T(8,128)(2,1)S(1)} %collective-permute-done), channel_id=2, replica_groups=mesh['z'=16,'y'=4,'x'=4,'c'=2] {'z'}, dimensions={0}, use_global_device_ids=true | all-gather | bytes 417792 | tf_op jit(solution)/shard_map/all_gather | solution.py:325
  59.1 2.4 %all-gather.1 = bf16[32,96,128]{2,1,0:T(8,128)(2,1)S(1)} all-gather(bf16[16,96,128]{2,1,0:T(8,128)(2,1)S(1)} %bitcast.4), channel_id=3, replica_groups=mesh['z'=16,'y'=4,'x'=4,'c'=2] {'c'}, dimensions={0}, use_global_device_ids=true | all-gather | bytes 1179648 | tf_op jit(solution)/shard_map/all_gather | solution.py:326
  61.5 0.0 all-to-all-done.1.own_ref
  61.5 2.0 %collective-permute-start.1 = (bf16[4,128,2048]{2,1,0:T(8,128)(2,1)S(1)}, bf16[4,128,2048]{2,1,0:T(8,128)(2,1)S(1)}, u32[]{:S(2)}, u32[]{:S(2)}) collective-permute-start(bf16[4,128,2048]{2,1,0:T(8,128)(2,1)S(1)} %all-to-all-done.1.own_ref), channel_id=1, source_target_pairs={{0,1},{1,0},{2,3},{3,2},{4,5},{5,4},{6,7},{7,6},{8,9},{9,8},{10,11... | collective-permute-start | bytes 6291464 | tf_op jit(solution)/shard_map/ppermute | solution.py:328
  63.5 0.0 copy-done
  63.5 12.4 %attend.1 = bf16[4,224,128]{2,1,0:T(8,128)(2,1)S(1)} custom-call(f32[2]{0:T(128)S(1)} %copy-done, bf16[4,192,128]{2,1,0:T(8,128)(2,1)S(1)} %all-to-all-done.q_ref, bf16[2,16,96,128]{3,2,1,0:T(8,128)(2,1)S(1)} %bitcast.3), custom_call_target="tpu_custom_call" | custom-call | flops 10000000000 | bytes 2000000 | tf_op jit(solution)/shard_map/attend/pallas_call | solution.py:331
  76.0 9.5 %all_to_all.20.part_ref = bf16[4,224,128]{2,1,0:T(8,128)(2,1)S(1)} all-to-all(bf16[4,224,128]{2,1,0:T(8,128)(2,1)S(1)} %attend.1), channel_id=1, replica_groups=mesh['z'=16,'y'=4,'x'=4,'c'=2] {'y'}, dimensions={0} | all-to-all | bytes 458752 | tf_op jit(solution)/shard_map/all_to_all | solution.py:348
  85.5 0.2 combine.1
  85.7 13.7 %all_to_all.21.heads_ref = bf16[8,192,128]{2,1,0:T(8,128)(2,1)S(1)} all-to-all(bf16[8,192,128]{2,1,0:T(8,128)(2,1)S(1)} %combine.1), channel_id=1, replica_groups=mesh['z'=16,'y'=4,'x'=4,'c'=2] {'x','c'}, dimensions={0} | all-to-all | bytes 786432 | tf_op jit(solution)/shard_map/all_to_all | solution.py:357
  99.5 0.0 collective-permute-done.1.other_ref
  99.5 1.9 %project_out.1 = bf16[192,2048]{1,0:T(8,128)(2,1)} custom-call(bf16[8,192,128]{2,1,0:T(8,128)(2,1)S(1)} %all_to_all.21.heads_ref, bf16[4,128,2048]{2,1,0:T(8,128)(2,1)S(1)} %all-to-all-done.1.own_ref, bf16[4,128,2048]{2,1,0:T(8,128)(2,1)S(1)} %collective-permute-done.1.other_ref), custom_call_target="tpu_custom_call" | custom-call | flops 805306368 | bytes 4194304 | tf_op jit(solution)/shard_map/project_out/pallas_call | solution.py:359
Async XLA Ops:
  0.0 21.8 %copy-start.1 = (bf16[128,2048]{1,0:T(8,128)(2,1)S(1)}, bf16[128,2048]{1,0:T(8,128)(2,1)}, u32[]{:S(2)}) copy-start(bf16[128,2048]{1,0:T(8,128)(2,1)} %param.13) | copy-start | bytes 1572868
  3.4 18.3 %all-to-all-start = ((bf16[4,192,128]{2,1,0:T(8,128)(2,1)}), bf16[4,192,128]{2,1,0:T(8,128)(2,1)S(1)}, u32[]{:S(2)}, u32[]{:S(2)}) async-start(bf16[4,192,128]{2,1,0:T(8,128)(2,1)} %get-tuple-element.12), calls=%async_computation | async-start | bytes 393216 | tf_op jit(solution)/shard_map/all_to_all | solution.py:321
  7.9 13.8 %collective-permute-start = (bf16[96,128]{1,0:T(8,128)(2,1)}, bf16[96,128]{1,0:T(8,128)(2,1)S(1)}, u32[]{:S(2)}, u32[]{:S(2)}) collective-permute-start(bf16[96,128]{1,0:T(8,128)(2,1)} %get-tuple-element.13), channel_id=1, source_target_pairs={{0,320},{8,352},{16,416},{24,384},{32,448},{40,480},{48,32},{56,0}... | collective-permute-start | bytes 73736 | tf_op jit(solution)/shard_map/ppermute | solution.py:320
  23.4 40.2 %copy-start = (f32[2]{0:T(128)S(1)}, f32[2]{0:T(128)}, u32[]{:S(2)}) copy-start(f32[2]{0:T(128)} %bias_ref.1) | copy-start | bytes 28
  23.4 38.1 %all-to-all-start.1 = ((bf16[4,128,2048]{2,1,0:T(8,128)(2,1)}), bf16[4,128,2048]{2,1,0:T(8,128)(2,1)S(1)}, u32[]{:S(2)}, u32[]{:S(2)}) async-start(bf16[4,128,2048]{2,1,0:T(8,128)(2,1)} %broadcast_in_dim.10), calls=%async_computation.1 | async-start | bytes 4194304 | tf_op jit(solution)/shard_map/all_to_all | solution.py:324
  61.5 38.0 %collective-permute-start.1 = (bf16[4,128,2048]{2,1,0:T(8,128)(2,1)S(1)}, bf16[4,128,2048]{2,1,0:T(8,128)(2,1)S(1)}, u32[]{:S(2)}, u32[]{:S(2)}) collective-permute-start(bf16[4,128,2048]{2,1,0:T(8,128)(2,1)S(1)} %all-to-all-done.1.own_ref), channel_id=1, source_target_pairs={{0,1},{1,0},{2,3},{3,2},{4,5},{5,4},{6,7},{7,6},{8,9},{9,8},{10,11... | collective-permute-start | bytes 6291464 | tf_op jit(solution)/shard_map/ppermute | solution.py:328

commit v9 on v8

--- a/solution.py
+++ b/solution.py
@@ -120,17 +120,18 @@
     later = (order(from_row) > order(to_col)).astype(jnp.bfloat16)
     rel = lax.axis_index("z") * row_tiles - own * key_tiles
 
-    keep_row = lax.broadcasted_iota(jnp.int32, (mine, mine), 0)
-    keys_only = (keep_row < HEAD_DIM).astype(jnp.bfloat16)
-
-    def largest(rows):
-        square = rows.astype(jnp.float32)
-        square = (square * square).astype(jnp.bfloat16)
-        return jnp.max(jnp.dot(square, keys_only, preferred_element_type=jnp.float32))
-
-    key_norm = jnp.maximum(largest(evens[...]), largest(odds[...]))
+    side = lax.broadcasted_iota(jnp.int32, (2 * mine, mine), 1) // HEAD_DIM
+    place = lax.broadcasted_iota(jnp.int32, (2 * mine, mine), 0) // HEAD_DIM
+    by_head = (place == side)[:mine].astype(jnp.bfloat16)
+    by_key = (place == 2 * side).astype(jnp.bfloat16)
+
+    def largest(rows, groups):
+        return jnp.max(jnp.dot(rows * rows, groups, preferred_element_type=jnp.float32))
+
+    key_norm = largest(jnp.concatenate([evens[...], odds[...]], axis=1), by_key)
+    query_norm = largest(q_ref[...].reshape(tokens, mine), by_head)
     room = 20.0 - jnp.maximum(bias_ref[0], bias_ref[1])
-    tame = (room > 0.0) & (largest(qs[...]) * key_norm * 1.03 <= room * room)
+    tame = (room > 0.0) & (query_norm * key_norm * 1.03 <= room * room)
 
     def tile(k):
         at = pl.ds(pl.multiple_of(k * wide, wide), wide)

time: 102 us -> 102 us (level)
  no operation moved by 1% of the time
where the time goes in v9:
time: 102 us; the launch traced here: 101 us
  blocking collectives  56.9 us (56%)
  starting transfers between devices  23 us (23%)
  Pallas kernels  17.9 us (18%)
  waiting for transfers between devices  1.72 us (2%)
  local copies, waits for them, and re-layouts  1.63 us (2%)
    all_gather x1, blocking collectives, local(): quarter_half = lax.all_gather(moved, 'z', axis=0)  31.3 us
    all_to_all x1, blocking collectives, local(): every_head = lax.all_to_all(attended, ('x', 'c'), 0, 0, tiled=True)  13.7 us
    pallas_call x1, Pallas kernels, local(): pl.pallas_call(attend_kernel, in_specs=[smem, vmem, vmem], out_specs=vmem...  12.3 us
    ppermute x1, starting transfers between devices, local(): moved = lax.ppermute(kv, ('z', 'y'), pairs)  12.1 us
    all_to_all x1, blocking collectives, local(): parts = lax.all_to_all(part, 'y', 0, 0, tiled=True)  9.5 us
    all_to_all x1, starting transfers between devices, local(): row_q = lax.all_to_all(queries, 'y', 0, 0, tiled=True)  4.47 us
    all_to_all x1, starting transfers between devices, local(): own_rows = lax.all_to_all(fan, 'x', 0, 0, tiled=True)  4.42 us
    pallas_call x1, Pallas kernels, local(): pl.pallas_call(project_kernel, in_specs=[anywhere] * 5, out_specs=[vmem,...  3.44 us
  transfers between devices with their start and end apart: 4, of which 1 were waited for; matrix products, arithmetic and copies ran while one was open for 0% of the time, Pallas kernels for 12%

profile of v9, /device:TPU:96, one launch (start us, length us, event | category | flops | bytes accessed | tf_op | source)
XLA Modules:
  0.0 101.2 jit_solution(18384827618450442490)
XLA Ops:
  0.0 0.0 copy-start.1
  0.0 3.4 %project.1 = (bf16[4,192,128]{2,1,0:T(8,128)(2,1)}, bf16[96,128]{1,0:T(8,128)(2,1)}) custom-call(bf16[192,2048]{1,0:T(8,128)(2,1)} %hidden_hbm.1, f32[1,2048]{1,0:T(1,128)} %bitcast.5, bf16[2048,128]{1,0:T(8,128)(2,1)} %wq_hbm.1, bf16[2048,256]{1,0:T(8,128)(2,1)} %wk_hbm.1, bf16[2048,256]{1,0:T(8,128)(2,1)} %wv_hbm.1), custom_call_target="tpu_custom_call" | custom-call | flops 301989888 | bytes 2359296 | tf_op jit(solution)/shard_map/project/pallas_call | solution.py:289
  3.4 4.5 %all-to-all-start = ((bf16[4,192,128]{2,1,0:T(8,128)(2,1)}), bf16[4,192,128]{2,1,0:T(8,128)(2,1)S(1)}, u32[]{:S(2)}, u32[]{:S(2)}) async-start(bf16[4,192,128]{2,1,0:T(8,128)(2,1)} %get-tuple-element.12), calls=%async_computation | async-start | bytes 393216 | tf_op jit(solution)/shard_map/all_to_all | solution.py:322
  7.9 12.1 %collective-permute-start = (bf16[96,128]{1,0:T(8,128)(2,1)}, bf16[96,128]{1,0:T(8,128)(2,1)S(1)}, u32[]{:S(2)}, u32[]{:S(2)}) collective-permute-start(bf16[96,128]{1,0:T(8,128)(2,1)} %get-tuple-element.13), channel_id=1, source_target_pairs={{0,320},{8,352},{16,416},{24,384},{32,448},{40,480},{48,32},{56,0}... | collective-permute-start | bytes 73736 | tf_op jit(solution)/shard_map/ppermute | solution.py:321
  20.0 1.7 %collective-permute-done = bf16[96,128]{1,0:T(8,128)(2,1)S(1)} collective-permute-done((bf16[96,128]{1,0:T(8,128)(2,1)}, bf16[96,128]{1,0:T(8,128)(2,1)S(1)}, u32[]{:S(2)}, u32[]{:S(2)}) %collective-permute-start) | collective-permute-done | bytes 24608 | tf_op jit(solution)/shard_map/ppermute | solution.py:321
  21.7 0.0 all-to-all-done.q_ref
  21.7 0.0 copy-done.1
  21.8 1.6 %broadcast_in_dim.10 = bf16[4,128,2048]{2,1,0:T(8,128)(2,1)} broadcast(bf16[128,2048]{1,0:T(8,128)(2,1)S(1)} %copy-done.1), dimensions={1,2} | broadcast | bytes 2621440 | tf_op jit(solution)/shard_map/broadcast_in_dim | solution.py:323
  23.4 0.0 copy-start
  23.4 4.4 %all-to-all-start.1 = ((bf16[4,128,2048]{2,1,0:T(8,128)(2,1)}), bf16[4,128,2048]{2,1,0:T(8,128)(2,1)S(1)}, u32[]{:S(2)}, u32[]{:S(2)}) async-start(bf16[4,128,2048]{2,1,0:T(8,128)(2,1)} %broadcast_in_dim.10), calls=%async_computation.1 | async-start | bytes 4194304 | tf_op jit(solution)/shard_map/all_to_all | solution.py:325
  27.8 31.3 %all-gather = bf16[1536,128]{1,0:T(8,128)(2,1)S(1)} all-gather(bf16[96,128]{1,0:T(8,128)(2,1)S(1)} %collective-permute-done), channel_id=2, replica_groups=mesh['z'=16,'y'=4,'x'=4,'c'=2] {'z'}, dimensions={0}, use_global_device_ids=true | all-gather | bytes 417792 | tf_op jit(solution)/shard_map/all_gather | solution.py:326
  59.1 2.4 %all-gather.1 = bf16[32,96,128]{2,1,0:T(8,128)(2,1)S(1)} all-gather(bf16[16,96,128]{2,1,0:T(8,128)(2,1)S(1)} %bitcast.4), channel_id=3, replica_groups=mesh['z'=16,'y'=4,'x'=4,'c'=2] {'c'}, dimensions={0}, use_global_device_ids=true | all-gather | bytes 1179648 | tf_op jit(solution)/shard_map/all_gather | solution.py:327
  61.5 0.0 all-to-all-done.1.own_ref
  61.5 2.0 %collective-permute-start.1 = (bf16[4,128,2048]{2,1,0:T(8,128)(2,1)S(1)}, bf16[4,128,2048]{2,1,0:T(8,128)(2,1)S(1)}, u32[]{:S(2)}, u32[]{:S(2)}) collective-permute-start(bf16[4,128,2048]{2,1,0:T(8,128)(2,1)S(1)} %all-to-all-done.1.own_ref), channel_id=1, source_target_pairs={{0,1},{1,0},{2,3},{3,2},{4,5},{5,4},{6,7},{7,6},{8,9},{9,8},{10,11... | collective-permute-start | bytes 6291464 | tf_op jit(solution)/shard_map/ppermute | solution.py:329
  63.5 0.0 copy-done
  63.5 12.3 %attend.1 = bf16[4,224,128]{2,1,0:T(8,128)(2,1)S(1)} custom-call(f32[2]{0:T(128)S(1)} %copy-done, bf16[4,192,128]{2,1,0:T(8,128)(2,1)S(1)} %all-to-all-done.q_ref, bf16[2,16,96,128]{3,2,1,0:T(8,128)(2,1)S(1)} %bitcast.3), custom_call_target="tpu_custom_call" | custom-call | flops 10000000000 | bytes 2000000 | tf_op jit(solution)/shard_map/attend/pallas_call | solution.py:332
  75.9 9.5 %all_to_all.20.part_ref = bf16[4,224,128]{2,1,0:T(8,128)(2,1)S(1)} all-to-all(bf16[4,224,128]{2,1,0:T(8,128)(2,1)S(1)} %attend.1), channel_id=1, replica_groups=mesh['z'=16,'y'=4,'x'=4,'c'=2] {'y'}, dimensions={0} | all-to-all | bytes 458752 | tf_op jit(solution)/shard_map/all_to_all | solution.py:349
  85.4 0.2 combine.1
  85.6 13.7 %all_to_all.21.heads_ref = bf16[8,192,128]{2,1,0:T(8,128)(2,1)S(1)} all-to-all(bf16[8,192,128]{2,1,0:T(8,128)(2,1)S(1)} %combine.1), channel_id=1, replica_groups=mesh['z'=16,'y'=4,'x'=4,'c'=2] {'x','c'}, dimensions={0} | all-to-all | bytes 786432 | tf_op jit(solution)/shard_map/all_to_all | solution.py:358
  99.4 0.0 collective-permute-done.1.other_ref
  99.4 1.9 %project_out.1 = bf16[192,2048]{1,0:T(8,128)(2,1)} custom-call(bf16[8,192,128]{2,1,0:T(8,128)(2,1)S(1)} %all_to_all.21.heads_ref, bf16[4,128,2048]{2,1,0:T(8,128)(2,1)S(1)} %all-to-all-done.1.own_ref, bf16[4,128,2048]{2,1,0:T(8,128)(2,1)S(1)} %collective-permute-done.1.other_ref), custom_call_target="tpu_custom_call" | custom-call | flops 805306368 | bytes 4194304 | tf_op jit(solution)/shard_map/project_out/pallas_call | solution.py:360
Async XLA Ops:
  0.0 21.8 %copy-start.1 = (bf16[128,2048]{1,0:T(8,128)(2,1)S(1)}, bf16[128,2048]{1,0:T(8,128)(2,1)}, u32[]{:S(2)}) copy-start(bf16[128,2048]{1,0:T(8,128)(2,1)} %param.13) | copy-start | bytes 1572868
  3.4 18.3 %all-to-all-start = ((bf16[4,192,128]{2,1,0:T(8,128)(2,1)}), bf16[4,192,128]{2,1,0:T(8,128)(2,1)S(1)}, u32[]{:S(2)}, u32[]{:S(2)}) async-start(bf16[4,192,128]{2,1,0:T(8,128)(2,1)} %get-tuple-element.12), calls=%async_computation | async-start | bytes 393216 | tf_op jit(solution)/shard_map/all_to_all | solution.py:322
  7.9 13.8 %collective-permute-start = (bf16[96,128]{1,0:T(8,128)(2,1)}, bf16[96,128]{1,0:T(8,128)(2,1)S(1)}, u32[]{:S(2)}, u32[]{:S(2)}) collective-permute-start(bf16[96,128]{1,0:T(8,128)(2,1)} %get-tuple-element.13), channel_id=1, source_target_pairs={{0,320},{8,352},{16,416},{24,384},{32,448},{40,480},{48,32},{56,0}... | collective-permute-start | bytes 73736 | tf_op jit(solution)/shard_map/ppermute | solution.py:321
  23.4 40.2 %copy-start = (f32[2]{0:T(128)S(1)}, f32[2]{0:T(128)}, u32[]{:S(2)}) copy-start(f32[2]{0:T(128)} %bias_ref.1) | copy-start | bytes 28
  23.4 38.1 %all-to-all-start.1 = ((bf16[4,128,2048]{2,1,0:T(8,128)(2,1)}), bf16[4,128,2048]{2,1,0:T(8,128)(2,1)S(1)}, u32[]{:S(2)}, u32[]{:S(2)}) async-start(bf16[4,128,2048]{2,1,0:T(8,128)(2,1)} %broadcast_in_dim.10), calls=%async_computation.1 | async-start | bytes 4194304 | tf_op jit(solution)/shard_map/all_to_all | solution.py:325
  61.5 37.9 %collective-permute-start.1 = (bf16[4,128,2048]{2,1,0:T(8,128)(2,1)S(1)}, bf16[4,128,2048]{2,1,0:T(8,128)(2,1)S(1)}, u32[]{:S(2)}, u32[]{:S(2)}) collective-permute-start(bf16[4,128,2048]{2,1,0:T(8,128)(2,1)S(1)} %all-to-all-done.1.own_ref), channel_id=1, source_target_pairs={{0,1},{1,0},{2,3},{3,2},{4,5},{5,4},{6,7},{7,6},{8,9},{9,8},{10,11... | collective-permute-start | bytes 6291464 | tf_op jit(solution)/shard_map/ppermute | solution.py:329

commit v10 on v9

--- a/solution.py
+++ b/solution.py
@@ -185,22 +185,28 @@
     crossed = (rel >= 0) & (rel < key_tiles)
     whole = jnp.clip(rel, 0, key_tiles)
 
-    @pl.when(tame & crossed)
+    left = lax.rem(whole, AT_ONCE)
+
+    @pl.when(tame & crossed & (left == 0))
     def _():
         for m in range(row_tiles):
             tame_step(rel + row_tiles - 1 - m, True)
 
+    @pl.when(tame & crossed & (left > 0))
+    def _():
+        for m in range(row_tiles):
+            tame_step(rel + row_tiles - 1 - m, True)
+        for m in range(row_tiles):
+            tame_step(rel - 1 - m, False)
+
     @pl.when(tame)
     def _():
+        start = whole - left
+
         @pl.loop(0, whole // AT_ONCE)
         def _(n):
             for m in range(AT_ONCE):
-                tame_step(whole - 1 - AT_ONCE * n - m, False)
-
-        @pl.when(lax.rem(whole, AT_ONCE) > 0)
-        def _():
-            for m in range(row_tiles):
-                tame_step(row_tiles - 1 - m, False)
+                tame_step(start - 1 - AT_ONCE * n - m, False)
 
     @pl.when(jnp.logical_not(tame))
     def _():

time: 102 us -> 101 us (level)
  no operation moved by 1% of the time
where the time goes in v10:
time: 101 us
  blocking collectives  56.9 us (56%)
  starting transfers between devices  23 us (23%)
  Pallas kernels  17.3 us (17%)
  waiting for transfers between devices  1.72 us (2%)
  local copies, waits for them, and re-layouts  1.63 us (2%)
    all_gather x1, blocking collectives, local(): quarter_half = lax.all_gather(moved, 'z', axis=0)  31.3 us
    all_to_all x1, blocking collectives, local(): every_head = lax.all_to_all(attended, ('x', 'c'), 0, 0, tiled=True)  13.7 us
    ppermute x1, starting transfers between devices, local(): moved = lax.ppermute(kv, ('z', 'y'), pairs)  12.1 us
    pallas_call x1, Pallas kernels, local(): pl.pallas_call(attend_kernel, in_specs=[smem, vmem, vmem], out_specs=vmem...  11.8 us
    all_to_all x1, blocking collectives, local(): parts = lax.all_to_all(part, 'y', 0, 0, tiled=True)  9.5 us
    all_to_all x1, starting transfers between devices, local(): row_q = lax.all_to_all(queries, 'y', 0, 0, tiled=True)  4.47 us
    all_to_all x1, starting transfers between devices, local(): own_rows = lax.all_to_all(fan, 'x', 0, 0, tiled=True)  4.42 us
    pallas_call x1, Pallas kernels, local(): pl.pallas_call(project_kernel, in_specs=[anywhere] * 5, out_specs=[vmem,...  3.44 us
  transfers between devices with their start and end apart: 4, of which 1 were waited for; matrix products, arithmetic and copies ran while one was open for 0% of the time, Pallas kernels for 12%

profile of v10, /device:TPU:96, one launch (start us, length us, event | category | flops | bytes accessed | tf_op | source)
XLA Modules:
  0.0 100.7 jit_solution(13139382358226023751)
XLA Ops:
  0.0 0.0 copy-start.1
  0.0 3.4 %project.1 = (bf16[4,192,128]{2,1,0:T(8,128)(2,1)}, bf16[96,128]{1,0:T(8,128)(2,1)}) custom-call(bf16[192,2048]{1,0:T(8,128)(2,1)} %hidden_hbm.1, f32[1,2048]{1,0:T(1,128)} %bitcast.5, bf16[2048,128]{1,0:T(8,128)(2,1)} %wq_hbm.1, bf16[2048,256]{1,0:T(8,128)(2,1)} %wk_hbm.1, bf16[2048,256]{1,0:T(8,128)(2,1)} %wv_hbm.1), custom_call_target="tpu_custom_call" | custom-call | flops 301989888 | bytes 2359296 | tf_op jit(solution)/shard_map/project/pallas_call | solution.py:295
  3.4 4.5 %all-to-all-start = ((bf16[4,192,128]{2,1,0:T(8,128)(2,1)}), bf16[4,192,128]{2,1,0:T(8,128)(2,1)S(1)}, u32[]{:S(2)}, u32[]{:S(2)}) async-start(bf16[4,192,128]{2,1,0:T(8,128)(2,1)} %get-tuple-element.12), calls=%async_computation | async-start | bytes 393216 | tf_op jit(solution)/shard_map/all_to_all | solution.py:328
  7.9 12.1 %collective-permute-start = (bf16[96,128]{1,0:T(8,128)(2,1)}, bf16[96,128]{1,0:T(8,128)(2,1)S(1)}, u32[]{:S(2)}, u32[]{:S(2)}) collective-permute-start(bf16[96,128]{1,0:T(8,128)(2,1)} %get-tuple-element.13), channel_id=1, source_target_pairs={{0,320},{8,352},{16,416},{24,384},{32,448},{40,480},{48,32},{56,0}... | collective-permute-start | bytes 73736 | tf_op jit(solution)/shard_map/ppermute | solution.py:327
  20.0 1.7 %collective-permute-done = bf16[96,128]{1,0:T(8,128)(2,1)S(1)} collective-permute-done((bf16[96,128]{1,0:T(8,128)(2,1)}, bf16[96,128]{1,0:T(8,128)(2,1)S(1)}, u32[]{:S(2)}, u32[]{:S(2)}) %collective-permute-start) | collective-permute-done | bytes 24608 | tf_op jit(solution)/shard_map/ppermute | solution.py:327
  21.7 0.0 all-to-all-done.q_ref
  21.7 0.0 copy-done.1
  21.8 1.6 %broadcast_in_dim.10 = bf16[4,128,2048]{2,1,0:T(8,128)(2,1)} broadcast(bf16[128,2048]{1,0:T(8,128)(2,1)S(1)} %copy-done.1), dimensions={1,2} | broadcast | bytes 2621440 | tf_op jit(solution)/shard_map/broadcast_in_dim | solution.py:329
  23.4 0.0 copy-start
  23.4 4.4 %all-to-all-start.1 = ((bf16[4,128,2048]{2,1,0:T(8,128)(2,1)}), bf16[4,128,2048]{2,1,0:T(8,128)(2,1)S(1)}, u32[]{:S(2)}, u32[]{:S(2)}) async-start(bf16[4,128,2048]{2,1,0:T(8,128)(2,1)} %broadcast_in_dim.10), calls=%async_computation.1 | async-start | bytes 4194304 | tf_op jit(solution)/shard_map/all_to_all | solution.py:331
  27.8 31.3 %all-gather = bf16[1536,128]{1,0:T(8,128)(2,1)S(1)} all-gather(bf16[96,128]{1,0:T(8,128)(2,1)S(1)} %collective-permute-done), channel_id=2, replica_groups=mesh['z'=16,'y'=4,'x'=4,'c'=2] {'z'}, dimensions={0}, use_global_device_ids=true | all-gather | bytes 417792 | tf_op jit(solution)/shard_map/all_gather | solution.py:332
  59.1 2.4 %all-gather.1 = bf16[32,96,128]{2,1,0:T(8,128)(2,1)S(1)} all-gather(bf16[16,96,128]{2,1,0:T(8,128)(2,1)S(1)} %bitcast.4), channel_id=3, replica_groups=mesh['z'=16,'y'=4,'x'=4,'c'=2] {'c'}, dimensions={0}, use_global_device_ids=true | all-gather | bytes 1179648 | tf_op jit(solution)/shard_map/all_gather | solution.py:333
  61.5 0.0 all-to-all-done.1.own_ref
  61.5 2.0 %collective-permute-start.1 = (bf16[4,128,2048]{2,1,0:T(8,128)(2,1)S(1)}, bf16[4,128,2048]{2,1,0:T(8,128)(2,1)S(1)}, u32[]{:S(2)}, u32[]{:S(2)}) collective-permute-start(bf16[4,128,2048]{2,1,0:T(8,128)(2,1)S(1)} %all-to-all-done.1.own_ref), channel_id=1, source_target_pairs={{0,1},{1,0},{2,3},{3,2},{4,5},{5,4},{6,7},{7,6},{8,9},{9,8},{10,11... | collective-permute-start | bytes 6291464 | tf_op jit(solution)/shard_map/ppermute | solution.py:335
  63.5 0.0 copy-done
  63.5 11.8 %attend.1 = bf16[4,224,128]{2,1,0:T(8,128)(2,1)S(1)} custom-call(f32[2]{0:T(128)S(1)} %copy-done, bf16[4,192,128]{2,1,0:T(8,128)(2,1)S(1)} %all-to-all-done.q_ref, bf16[2,16,96,128]{3,2,1,0:T(8,128)(2,1)S(1)} %bitcast.3), custom_call_target="tpu_custom_call" | custom-call | flops 10000000000 | bytes 2000000 | tf_op jit(solution)/shard_map/attend/pallas_call | solution.py:338
  75.3 9.5 %all_to_all.20.part_ref = bf16[4,224,128]{2,1,0:T(8,128)(2,1)S(1)} all-to-all(bf16[4,224,128]{2,1,0:T(8,128)(2,1)S(1)} %attend.1), channel_id=1, replica_groups=mesh['z'=16,'y'=4,'x'=4,'c'=2] {'y'}, dimensions={0} | all-to-all | bytes 458752 | tf_op jit(solution)/shard_map/all_to_all | solution.py:355
  84.8 0.2 combine.1
  85.1 13.7 %all_to_all.21.heads_ref = bf16[8,192,128]{2,1,0:T(8,128)(2,1)S(1)} all-to-all(bf16[8,192,128]{2,1,0:T(8,128)(2,1)S(1)} %combine.1), channel_id=1, replica_groups=mesh['z'=16,'y'=4,'x'=4,'c'=2] {'x','c'}, dimensions={0} | all-to-all | bytes 786432 | tf_op jit(solution)/shard_map/all_to_all | solution.py:364
  98.8 0.0 collective-permute-done.1.other_ref
  98.8 1.9 %project_out.1 = bf16[192,2048]{1,0:T(8,128)(2,1)} custom-call(bf16[8,192,128]{2,1,0:T(8,128)(2,1)S(1)} %all_to_all.21.heads_ref, bf16[4,128,2048]{2,1,0:T(8,128)(2,1)S(1)} %all-to-all-done.1.own_ref, bf16[4,128,2048]{2,1,0:T(8,128)(2,1)S(1)} %collective-permute-done.1.other_ref), custom_call_target="tpu_custom_call" | custom-call | flops 805306368 | bytes 4194304 | tf_op jit(solution)/shard_map/project_out/pallas_call | solution.py:366
Async XLA Ops:
  0.0 21.8 %copy-start.1 = (bf16[128,2048]{1,0:T(8,128)(2,1)S(1)}, bf16[128,2048]{1,0:T(8,128)(2,1)}, u32[]{:S(2)}) copy-start(bf16[128,2048]{1,0:T(8,128)(2,1)} %param.13) | copy-start | bytes 1572868
  3.4 18.3 %all-to-all-start = ((bf16[4,192,128]{2,1,0:T(8,128)(2,1)}), bf16[4,192,128]{2,1,0:T(8,128)(2,1)S(1)}, u32[]{:S(2)}, u32[]{:S(2)}) async-start(bf16[4,192,128]{2,1,0:T(8,128)(2,1)} %get-tuple-element.12), calls=%async_computation | async-start | bytes 393216 | tf_op jit(solution)/shard_map/all_to_all | solution.py:328
  7.9 13.8 %collective-permute-start = (bf16[96,128]{1,0:T(8,128)(2,1)}, bf16[96,128]{1,0:T(8,128)(2,1)S(1)}, u32[]{:S(2)}, u32[]{:S(2)}) collective-permute-start(bf16[96,128]{1,0:T(8,128)(2,1)} %get-tuple-element.13), channel_id=1, source_target_pairs={{0,320},{8,352},{16,416},{24,384},{32,448},{40,480},{48,32},{56,0}... | collective-permute-start | bytes 73736 | tf_op jit(solution)/shard_map/ppermute | solution.py:327
  23.4 40.2 %copy-start = (f32[2]{0:T(128)S(1)}, f32[2]{0:T(128)}, u32[]{:S(2)}) copy-start(f32[2]{0:T(128)} %bias_ref.1) | copy-start | bytes 28
  23.4 38.1 %all-to-all-start.1 = ((bf16[4,128,2048]{2,1,0:T(8,128)(2,1)}), bf16[4,128,2048]{2,1,0:T(8,128)(2,1)S(1)}, u32[]{:S(2)}, u32[]{:S(2)}) async-start(bf16[4,128,2048]{2,1,0:T(8,128)(2,1)} %broadcast_in_dim.10), calls=%async_computation.1 | async-start | bytes 4194304 | tf_op jit(solution)/shard_map/all_to_all | solution.py:331
  61.5 37.3 %collective-permute-start.1 = (bf16[4,128,2048]{2,1,0:T(8,128)(2,1)S(1)}, bf16[4,128,2048]{2,1,0:T(8,128)(2,1)S(1)}, u32[]{:S(2)}, u32[]{:S(2)}) collective-permute-start(bf16[4,128,2048]{2,1,0:T(8,128)(2,1)S(1)} %all-to-all-done.1.own_ref), channel_id=1, source_target_pairs={{0,1},{1,0},{2,3},{3,2},{4,5},{5,4},{6,7},{7,6},{8,9},{9,8},{10,11... | collective-permute-start | bytes 6291464 | tf_op jit(solution)/shard_map/ppermute | solution.py:335
